TPU v7x, 1024 devices: a whole 8x8x8 slice. The times are simulated.
1024 devices in a mesh: ep: 64 (over z, y), tp: 16 (over x, core).
Axes of the slice: x: 8, y: 8, z: 8, core: 2. Of those that a mesh axis runs over, the one named last changes fastest.
Arguments:
- tokens: bfloat16 [16384, 2048], P('ep', 'tp'), may hold values from -400 to 400
- expert_ids: int32 [16384, 2], P('ep'), may hold values from 0 to 63, all different within a row; in each aligned block of 256 rows (0 to 255, 256 to 511, ...) at most 10 rows name the same one
- route_weights: float32 [16384, 2], P('ep'), may hold values from 0.1 to 1
- pre_gain: float32 [2048], P('tp'), may hold values from 0.1 to 1.9
- post_gain: float32 [2048], P('tp'), may hold values from 0.1 to 1.9
- gate_weight: bfloat16 [64, 2048, 4096], P('ep', None, 'tp'), may hold values from -0.125 to 0.125
- up_weight: bfloat16 [64, 2048, 4096], P('ep', None, 'tp'), may hold values from -0.125 to 0.125
- down_weight: bfloat16 [64, 4096, 2048], P('ep', None, 'tp'), may hold values from -0.71875 to 0.71875
Outputs:
- layer_out: bfloat16 [16384, 2048], P('ep', 'tp')
Inputs may be any that keep to these rules, and one draw needn't show every extreme that they name: `expert_ids`: the 2 experts of a token are distinct. Within the rows of one device along ep, no expert is named more than 10 times, a bound that some block reaches.
All inputs are finite; a program needn't handle non-finite values.
Results may differ from a plain program's by a relative error of at most 0.007.
Values may be sent and summed in bfloat16 or wider, within the bound.
No kernel may reach another device: no remote copies, remote signals or barrier semaphores. Data moves between devices by JAX's collectives and lax.ppermute only.
A program may use at most 64 MiB of HBM per device.

v0:
```python
import jax
import jax.numpy as jnp
from jax import lax
from jax.sharding import PartitionSpec as P

epsilon = 1e-06


def from_everyone(value, axis):
    devices = lax.axis_size(axis)
    return lax.all_to_all(
        jnp.broadcast_to(value[None], (devices, *value.shape)), axis, 0, 0, tiled=True
    )


def over_copies(value, axis):
    everything = from_everyone(value, axis)
    return jnp.sum(everything, axis=0)


def on_device(
    tokens, expert_ids, route_weights, pre_gain, post_gain, gate_weight, up_weight, down_weight
):
    tok_rows, width_part = tokens.shape
    width_full = width_part * lax.axis_size("tp")
    ep_count = lax.axis_size("ep")
    local_count = gate_weight.shape[0]
    experts_all = local_count * ep_count
    top_count = expert_ids.shape[1]
    capacity = max(2, tok_rows * top_count * 5 // (4 * experts_all))
    slot_total = experts_all * capacity
    tok_float = tokens.astype(jnp.float32)
    square_sum = over_copies(jnp.sum(tok_float * tok_float, axis=1), "tp")
    inv_scale = lax.rsqrt(square_sum / width_full + epsilon)
    normed = (tok_float * inv_scale[:, None] * pre_gain[None, :]).astype(jnp.bfloat16)
    flat_ids = expert_ids.reshape(-1)
    onehot = (flat_ids[:, None] == jnp.arange(experts_all, dtype=jnp.int32)[None, :]).astype(
        jnp.int32
    )
    slot = jnp.sum((jnp.cumsum(onehot, axis=0) - 1) * onehot, axis=1)
    target = (flat_ids * capacity + slot).reshape(tok_rows, top_count)
    slot_index = jnp.arange(slot_total, dtype=jnp.int32)
    pick_map = (jnp.transpose(target).reshape(-1)[:, None] == slot_index[None, :]).astype(
        jnp.bfloat16
    )
    dispatch_map = jnp.sum(pick_map.reshape(top_count, tok_rows, slot_total), axis=0)
    outgoing = jnp.dot(
        jnp.transpose(dispatch_map), normed, preferred_element_type=jnp.float32
    ).astype(jnp.bfloat16)
    outgoing = outgoing.reshape(ep_count, local_count, capacity, width_part)
    arrived = lax.all_to_all(outgoing, "ep", split_axis=0, concat_axis=2, tiled=True)
    arrived = arrived.reshape(local_count, ep_count * capacity, width_part)
    row_total = ep_count * capacity
    features = lax.all_gather(arrived, "tp", axis=2, tiled=True)
    gate = jnp.einsum("erd,edh->erh", features, gate_weight, preferred_element_type=jnp.float32)
    upper = jnp.einsum("erd,edh->erh", features, up_weight, preferred_element_type=jnp.float32)
    hidden = (jax.nn.silu(gate) * upper).astype(jnp.bfloat16)
    hidden_whole = lax.all_gather(hidden, "tp", axis=2, tiled=True)
    result = jnp.einsum(
        "erh,ehd->erd", hidden_whole, down_weight, preferred_element_type=jnp.float32
    )
    expert_out = result.astype(jnp.bfloat16).reshape(1, local_count, row_total, width_part)
    returned = lax.all_to_all(expert_out, "ep", split_axis=2, concat_axis=0, tiled=True)
    returned = returned.reshape(slot_total, width_part)
    picked = jnp.dot(pick_map, returned, preferred_element_type=jnp.float32).reshape(
        top_count, tok_rows, width_part
    )
    mixed = jnp.sum(picked * jnp.transpose(route_weights)[:, :, None], axis=0)
    out_sum = over_copies(jnp.sum(mixed * mixed, axis=1), "tp")
    out_scale = lax.rsqrt(out_sum / width_full + epsilon)
    return (mixed * out_scale[:, None] * post_gain[None, :]).astype(jnp.bfloat16)


def solution(mesh):
    return jax.shard_map(
        on_device,
        mesh=mesh,
        in_specs=(
            P("ep", "tp"),
            P("ep", None),
            P("ep", None),
            P("tp"),
            P("tp"),
            P("ep", None, "tp"),
            P("ep", None, "tp"),
            P("ep", None, "tp"),
        ),
        out_specs=P("ep", "tp"),
        check_vma=False,
    )
```

profile of v0, /device:TPU:1, one launch (start us, length us, event | category | flops | bytes accessed | tf_op | source)
XLA Modules:
  0.0 217.9 jit_solution(9618720549256336493)
XLA Ops:
  6.5 1.0 fusion.28
  7.6 0.6 broadcast_in_dim.4
  8.2 17.4 %all-to-all-start = ((f32[16,1,256]{2,1,0:T(1,128)}), f32[16,1,256]{2,1,0:T(1,128)S(1)}, u32[]{:S(2)}, u32[]{:S(2)}) async-start(f32[16,1,256]{2,1,0:T(1,128)} %broadcast_in_dim.4), calls=%async_computation | async-start | bytes 32768 | tf_op jit(solution)/shard_map/all_to_all | solution.py:11
  25.6 0.8 copy.54
  26.5 0.1 eq.65
  26.6 0.1 eq.61
  26.8 1.2 reduce-window.6
  28.0 0.2 slice_reduce_fusion
  28.2 0.1 fusion.32
  28.4 0.1 reduce_sum.69
  28.5 0.1 copy.57
  28.6 0.7 add_bitcast_fusion.1
  29.3 0.2 fusion.24
  29.5 3.5 %all-to-all-done = f32[16,1,256]{2,1,0:T(1,128)S(1)} async-done(((f32[16,1,256]{2,1,0:T(1,128)}), f32[16,1,256]{2,1,0:T(1,128)S(1)}, u32[]{:S(2)}, u32[]{:S(2)}) %all-to-all-start) | async-done | bytes 16416 | tf_op jit(solution)/shard_map/all_to_all | solution.py:11
  33.0 1.2 convolution_convert_fusion
  34.3 26.8 %all_to_all.30 = bf16[64,1,10,128]{3,2,1,0:T(8,128)(2,1)S(1)} all-to-all(bf16[64,1,10,128]{3,2,1,0:T(8,128)(2,1)S(1)} %bitcast.56), channel_id=1, replica_groups=mesh['ep'=64,'tp'=16] {'ep'}, dimensions={0} | all-to-all | bytes 327680 | tf_op jit(solution)/shard_map/all_to_all | solution.py:51
  61.1 0.7 reshape.132
  61.9 39.1 %all-gather.4.cloned.1.call-done = bf16[1,640,2048]{2,1,0:T(8,128)(2,1)} async-done(((bf16[1,640,128]{2,1,0:T(8,128)(2,1)}), bf16[1,640,2048]{2,1,0:T(8,128)(2,1)}) %all-gather.4.cloned.1.call-update) | async-done | bytes 2621456 | tf_op jit(solution)/shard_map/all_gather | solution.py:54
  101.0 2.7 %fusion.2 = f32[640,256]{1,0:T(8,128)S(1)} fusion(bf16[1,640,2048]{2,1,0:T(8,128)(2,1)} %all-gather.4.cloned.1.call-done, bf16[1,2048,256]{2,1,0:T(8,128)(2,1)S(1)} %copy-done), kind=kOutput, calls=%fused_computation.2 | convolution fusion | flops 671088640 | bytes 4325376 | tf_op jit(solution)/shard_map/erd,edh->erh/dot_general | solution.py:55
  103.7 1.6 fusion.11
  105.3 59.9 %all-gather.6.cloned.1.call-done = bf16[640,4096]{1,0:T(8,128)(2,1)} async-done(((bf16[640,256]{1,0:T(8,128)(2,1)}), bf16[640,4096]{1,0:T(8,128)(2,1)}) %all-gather.6.cloned.1.call-update) | async-done | bytes 5242896 | tf_op jit(solution)/shard_map/all_gather | solution.py:58
  165.2 4.0 %fusion.20 = bf16[1,1,640,128]{3,2,1,0:T(8,128)(2,1)S(1)} fusion(bf16[640,4096]{1,0:T(8,128)(2,1)} %all-gather.6.cloned.1.call-done, bf16[1,4096,128]{2,1,0:T(8,128)(2,1)S(1)} %copy-done.4), kind=kOutput, calls=%fused_computation.15 | convolution fusion | flops 671170560 | bytes 6455296 | tf_op jit(solution)/shard_map/erh,ehd->erd/dot_general | solution.py:59
  169.2 0.3 copy.72
  169.5 0.5 broadcast.99
  170.0 1.6 reduce.5
  171.6 0.1 reshape.145
  171.7 23.7 %all_to_all.31 = bf16[64,2,640]{2,1,0:T(2,128)(2,1)S(1)} all-to-all(bf16[64,2,640]{2,1,0:T(2,128)(2,1)S(1)} %reshape.145), channel_id=1, replica_groups=mesh['ep'=64,'tp'=16] {'ep'}, dimensions={0} | all-to-all | bytes 327680 | tf_op jit(solution)/shard_map/all_to_all | solution.py:63
  195.4 0.1 reshape.146
  195.5 0.4 fusion.17
  195.9 0.1 multiply_reduce_fusion
  196.1 14.2 %all_to_all.32 = f32[16,1,256]{2,1,0:T(1,128)S(1)} all-to-all(f32[16,1,256]{2,1,0:T(1,128)S(1)} %broadcast_in_dim.5), channel_id=1, replica_groups=mesh['ep'=64,'tp'=16] {'tp'}, dimensions={0} | all-to-all | bytes 32768 | tf_op jit(solution)/shard_map/all_to_all | solution.py:11
  210.3 0.7 multiply_convert_fusion
  (25 shorter events, 0.4 us)
Async XLA Ops:
  6.5 94.4 %copy-start = (bf16[1,2048,256]{2,1,0:T(8,128)(2,1)S(1)}, bf16[1,2048,256]{2,1,0:T(8,128)(2,1)}, u32[]{:S(2)}) copy-start(bf16[1,2048,256]{2,1,0:T(8,128)(2,1)} %param.13) | copy-start | bytes 3145732
  8.2 24.8 %all-to-all-start = ((f32[16,1,256]{2,1,0:T(1,128)}), f32[16,1,256]{2,1,0:T(1,128)S(1)}, u32[]{:S(2)}, u32[]{:S(2)}) async-start(f32[16,1,256]{2,1,0:T(1,128)} %broadcast_in_dim.4), calls=%async_computation | async-start | bytes 32768 | tf_op jit(solution)/shard_map/all_to_all | solution.py:11
  25.6 75.3 %all-gather.4.cloned.1.call-start = ((), (), s32[]{:S(2)}) async-start(), calls=%async_computation.4 | async-start | bytes 2785280 | tf_op jit(solution)/shard_map/all_gather | solution.py:54
  61.8 41.9 %copy-start.3 = (bf16[1,2048,256]{2,1,0:T(8,128)(2,1)S(1)}, bf16[1,2048,256]{2,1,0:T(8,128)(2,1)}, u32[]{:S(2)}) copy-start(bf16[1,2048,256]{2,1,0:T(8,128)(2,1)} %param.14) | copy-start | bytes 3145732
  61.8 103.4 %all-gather.6.cloned.1.call-start = ((), (), s32[]{:S(2)}) async-start(), calls=%async_computation.5 | async-start | bytes 5570560 | tf_op jit(solution)/shard_map/all_gather | solution.py:58
  100.9 2.8 %copy-start.2 = (bf16[1,640,2048]{2,1,0:T(8,128)(2,1)S(1)}, bf16[1,640,2048]{2,1,0:T(8,128)(2,1)}, u32[]{:S(2)}) copy-start(bf16[1,640,2048]{2,1,0:T(8,128)(2,1)} %all-gather.4.cloned.1.call-done) | copy-start | bytes 7864324
  103.7 61.5 %copy-start.4 = (bf16[1,4096,128]{2,1,0:T(8,128)(2,1)S(1)}, bf16[1,4096,128]{2,1,0:T(8,128)(2,1)}, u32[]{:S(2)}) copy-start(bf16[1,4096,128]{2,1,0:T(8,128)(2,1)} %param.15) | copy-start | bytes 3145732
  105.3 90.2 %copy-start.5 = (f32[256,2]{0,1:T(2,128)S(1)}, f32[256,2]{0,1:T(2,128)}, u32[]{:S(2)}) copy-start(f32[256,2]{0,1:T(2,128)} %param.10) | copy-start | bytes 6148
  169.2 41.1 %copy-start.1 = (f32[128]{0:T(128)S(1)}, f32[128]{0:T(128)}, u32[]{:S(2)}) copy-start(f32[128]{0:T(128)} %param.12) | copy-start | bytes 1540
Sparse Core Ops, SparseCore 0:
  61.9 38.9 all-gather.3
  105.4 59.7 all-gather.5
where the time goes:
time: 218 us
  waiting for transfers between devices  102 us (47%)
  blocking collectives  64.7 us (30%)
  starting transfers between devices  17.5 us (8%)
  between operations  13.6 us (6%)
  matrix products  9.91 us (5%)
  other arithmetic  5.88 us (3%)
  local copies, waits for them, and re-layouts  3.95 us (2%)
    all_gather x1, waiting for transfers between devices, on_device(): hidden_whole = lax.all_gather(hidden, 'tp', axis=2, tiled=True)  59.9 us
    all_gather x1, waiting for transfers between devices, on_device(): features = lax.all_gather(arrived, 'tp', axis=2, tiled=True)  39.1 us
    all_to_all x1, blocking collectives, on_device(): lax.all_to_all(outgoing, 'ep', split_axis=0, concat_axis=2, tiled=True)  26.8 us
    all_to_all x1, blocking collectives, on_device(): lax.all_to_all(expert_out, 'ep', split_axis=2, concat_axis=0, tiled=True)  23.7 us
    all_to_all x1, starting transfers between devices, from_everyone(): lax.all_to_all(jnp.broadcast_to(value[None], (devices, *value.shape)), ax...  17.4 us
    all_to_all x1, blocking collectives, from_everyone(): lax.all_to_all(jnp.broadcast_to(value[None], (devices, *value.shape)), ax...  14.2 us
  transfers between devices with their start and end apart: 3, of which 3 were waited for; matrix products, arithmetic and copies ran while one was open for 2% of the time, Pallas kernels for 0%

commit v1 on v0

v1 whole, which is shorter than its diff:
```python
import jax
import jax.numpy as jnp
from jax import lax
from jax.experimental import pallas as pl
from jax.experimental.pallas import tpu as pltpu
from jax.sharding import PartitionSpec as P

epsilon = 1e-06
PAD = 16
EXTRA = 16


def dispatch_kernel(tok_ref, ids_ref, weights_ref, out_ref, cols_ref):
    rows = tok_ref.shape[0]
    slots = out_ref.shape[0]
    experts = slots // PAD
    ids = ids_ref[...]
    expert_index = lax.broadcasted_iota(jnp.int32, (experts, rows), 0)
    hot0 = jnp.where(expert_index == ids[0:1, :], 1.0, 0.0)
    hot1 = jnp.where(expert_index == ids[1:2, :], 1.0, 0.0)
    earlier = lax.broadcasted_iota(jnp.int32, (rows, rows), 0) < lax.broadcasted_iota(
        jnp.int32, (rows, rows), 1
    )
    earlier = jnp.where(earlier, 1.0, 0.0).astype(jnp.bfloat16)
    counts = jnp.dot((hot0 + hot1).astype(jnp.bfloat16), earlier, preferred_element_type=jnp.float32)
    slot0 = jnp.sum(hot0 * counts, axis=0, keepdims=True)
    slot1 = jnp.sum(hot1 * counts, axis=0, keepdims=True)
    target0 = ids[0:1, :] * PAD + slot0.astype(jnp.int32)
    target1 = ids[1:2, :] * PAD + slot1.astype(jnp.int32)
    slot_index = lax.broadcasted_iota(jnp.int32, (slots, rows), 0)
    chosen = jnp.logical_or(slot_index == target0, slot_index == target1)
    chosen = jnp.where(chosen, 1.0, 0.0).astype(jnp.bfloat16)
    out_ref[...] = jnp.dot(chosen, tok_ref[...], preferred_element_type=jnp.float32).astype(
        jnp.bfloat16
    )
    weights = weights_ref[...]
    lines = jnp.concatenate(
        [
            target0.astype(jnp.float32),
            target1.astype(jnp.float32),
            weights,
            jnp.zeros((4, rows), jnp.float32),
        ],
        axis=0,
    )
    cols_ref[...] = jnp.transpose(lines)


def dispatch(tokens, ids, weights, slots):
    rows, width = tokens.shape
    return pl.pallas_call(
        dispatch_kernel,
        out_shape=(
            jax.ShapeDtypeStruct((slots, width), jnp.bfloat16),
            jax.ShapeDtypeStruct((rows, 8), jnp.float32),
        ),
        name="dispatch",
    )(tokens, ids, weights)


def hidden_kernel(feat_ref, gain_ref, gate_ref, up_ref, out_ref, normed_ref):
    parts, rows, width = feat_ref.shape
    full = parts * width
    total = jnp.zeros((rows, width), jnp.float32)
    for j in range(parts):
        part = feat_ref[j].astype(jnp.float32)
        total = total + part * part
    scale = lax.rsqrt(jnp.sum(total, axis=1, keepdims=True) / full + epsilon)
    for j in range(parts):
        pieces = gain_ref[j].astype(jnp.float32)
        gain = pieces[0:1, :] + pieces[1:2, :] + pieces[2:3, :]
        part = feat_ref[j].astype(jnp.float32)
        normed_ref[:, j * width : (j + 1) * width] = (part * scale * gain).astype(jnp.bfloat16)
    normed = normed_ref[...]
    gate = jnp.dot(normed, gate_ref[...], preferred_element_type=jnp.float32)
    upper = jnp.dot(normed, up_ref[...], preferred_element_type=jnp.float32)
    out_ref[...] = (gate / (1.0 + jnp.exp(-gate)) * upper).astype(jnp.bfloat16)


def hidden_of(features, gate_weight, up_weight, row_total, tile):
    parts, _, width = features.shape
    full, units = gate_weight.shape
    return pl.pallas_call(
        hidden_kernel,
        grid=(row_total // tile,),
        in_specs=[
            pl.BlockSpec((parts, tile, width), lambda i: (0, i, 0)),
            pl.BlockSpec((parts, EXTRA, width), lambda i: (0, row_total // EXTRA, 0)),
            pl.BlockSpec((full, units), lambda i: (0, 0)),
            pl.BlockSpec((full, units), lambda i: (0, 0)),
        ],
        out_specs=pl.BlockSpec((tile, units), lambda i: (i, 0)),
        out_shape=jax.ShapeDtypeStruct((row_total, units), jnp.bfloat16),
        scratch_shapes=[pltpu.VMEM((tile, full), jnp.bfloat16)],
        name="hidden",
    )(features, features, gate_weight, up_weight)


def down_kernel(hidden_ref, down_ref, out_ref):
    parts, rows, units = hidden_ref.shape
    blocks, _, width = out_ref.shape
    capacity = rows // blocks
    total = jnp.zeros((rows, width), jnp.float32)
    for j in range(parts):
        total = total + jnp.dot(
            hidden_ref[j],
            down_ref[j * units : (j + 1) * units, :],
            preferred_element_type=jnp.float32,
        )
    empty = jnp.zeros((PAD - capacity, width), jnp.float32)
    for b in range(blocks):
        block = jnp.concatenate([total[b * capacity : (b + 1) * capacity, :], empty], axis=0)
        out_ref[b] = block.astype(jnp.bfloat16)


def down_of(hidden, down_weight, blocks_total, tile_blocks):
    parts, row_total, units = hidden.shape
    full, width = down_weight.shape
    tile = row_total // blocks_total * tile_blocks
    return pl.pallas_call(
        down_kernel,
        grid=(row_total // tile,),
        in_specs=[
            pl.BlockSpec((parts, tile, units), lambda i: (0, i, 0)),
            pl.BlockSpec((full, width), lambda i: (0, 0)),
        ],
        out_specs=pl.BlockSpec((tile_blocks, PAD, width), lambda i: (i, 0, 0)),
        out_shape=jax.ShapeDtypeStruct((blocks_total, PAD, width), jnp.bfloat16),
        name="down",
    )(hidden, down_weight)


def combine_kernel(returned_ref, cols_ref, mixed_ref, sums_ref):
    rows, width = mixed_ref.shape
    slots = returned_ref.shape[0]
    cols = cols_ref[...]
    targets = cols[:, 0:2].astype(jnp.int32)
    slot_index = lax.broadcasted_iota(jnp.int32, (rows, slots), 1)
    returned = returned_ref[...]
    mixed = jnp.zeros((rows, width), jnp.float32)
    for k in range(2):
        chosen = jnp.where(slot_index == targets[:, k : k + 1], 1.0, 0.0).astype(jnp.bfloat16)
        picked = jnp.dot(chosen, returned, preferred_element_type=jnp.float32)
        mixed = mixed + picked * cols[:, 2 + k : 3 + k]
    mixed_ref[...] = mixed
    sums = jnp.sum(mixed * mixed, axis=1, keepdims=True)
    line = jnp.transpose(jnp.broadcast_to(sums, (rows, 128)))[0:1, :]
    for j in range(sums_ref.shape[0]):
        sums_ref[j] = line


def combine(returned, cols, peers):
    width = returned.shape[1]
    rows = cols.shape[0]
    return pl.pallas_call(
        combine_kernel,
        out_shape=(
            jax.ShapeDtypeStruct((rows, width), jnp.float32),
            jax.ShapeDtypeStruct((peers, 1, rows), jnp.float32),
        ),
        name="combine",
    )(returned, cols)


def final_kernel(mixed_ref, sums_ref, gain_ref, out_ref):
    rows, width = mixed_ref.shape
    peers = sums_ref.shape[0]
    total = sums_ref[0]
    for j in range(1, peers):
        total = total + sums_ref[j]
    scale = lax.rsqrt(total / (peers * width) + epsilon)
    column = jnp.transpose(jnp.broadcast_to(scale, (8, rows)))[:, 0:1]
    out_ref[...] = (mixed_ref[...] * column * gain_ref[...]).astype(jnp.bfloat16)


def final(mixed, sums, gain):
    return pl.pallas_call(
        final_kernel,
        out_shape=jax.ShapeDtypeStruct(mixed.shape, jnp.bfloat16),
        name="final",
    )(mixed, sums, gain)


def gain_rows(gain):
    first = lax.reduce_precision(gain, 8, 7)
    second = lax.reduce_precision(gain - first, 8, 7)
    third = gain - first - second
    rows = jnp.stack([first, second, third])
    return jnp.pad(rows, ((0, EXTRA - 3), (0, 0))).astype(jnp.bfloat16)


def on_device(
    tokens, expert_ids, route_weights, pre_gain, post_gain, gate_weight, up_weight, down_weight
):
    tok_rows, width = tokens.shape
    ep_count = lax.axis_size("ep")
    tp_count = lax.axis_size("tp")
    top_count = expert_ids.shape[1]
    capacity = max(2, tok_rows * top_count * 5 // (4 * ep_count))
    row_total = ep_count * capacity
    outgoing, cols = dispatch(
        tokens, jnp.transpose(expert_ids), jnp.transpose(route_weights), ep_count * PAD
    )
    arrived = lax.all_to_all(
        outgoing.reshape(ep_count, PAD, width), "ep", split_axis=0, concat_axis=0, tiled=True
    )
    arrived = arrived[:, :capacity, :].reshape(row_total, width)
    arrived = jnp.concatenate([arrived, gain_rows(pre_gain)], axis=0)
    features = lax.all_gather(arrived, "tp", axis=0, tiled=False)
    hidden = hidden_of(features, gate_weight[0], up_weight[0], row_total, 160)
    hidden_whole = lax.all_gather(hidden, "tp", axis=0, tiled=False)
    expert_out = down_of(hidden_whole, down_weight[0], ep_count, 16)
    returned = lax.all_to_all(expert_out, "ep", split_axis=0, concat_axis=0, tiled=True)
    mixed, sums = combine(returned.reshape(ep_count * PAD, width), cols, tp_count)
    sums = lax.all_to_all(sums, "tp", split_axis=0, concat_axis=0, tiled=True)
    return final(mixed, sums, post_gain[None, :])


def solution(mesh):
    return jax.shard_map(
        on_device,
        mesh=mesh,
        in_specs=(
            P("ep", "tp"),
            P("ep", None),
            P("ep", None),
            P("tp"),
            P("tp"),
            P("ep", None, "tp"),
            P("ep", None, "tp"),
            P("ep", None, "tp"),
        ),
        out_specs=P("ep", "tp"),
        check_vma=False,
    )
```

time: 218 us -> 198 us (0.908)
  blocking collectives: 64.7 us -> 41.3 us
  Pallas kernels: 0 us -> 17.1 us
  matrix products: 9.91 us -> 0 us
  starting transfers between devices: 17.5 us -> 24 us
  other arithmetic: 5.88 us -> 1.35 us
  local copies, waits for them, and re-layouts: 3.95 us -> 0.06 us
    all_to_all x3 -> x2, blocking collectives: 64.7 us -> 41.3 us  [the longest x1 27.1 us: on_device(): lax.all_to_all(expert_out, 'ep', split_axis=0, concat_axis=0, tiled=True)]
    pallas_call x0 -> x5, Pallas kernels: none -> 17.1 us  [the longest x1 5.67 us: hidden_of(): pl.pallas_call(hidden_kernel, grid=(row_total // tile,), in_specs=[pl.Blo...]
    all_gather x2, waiting for transfers between devices: 98.9 us -> 88 us  [the longest x1 48.2 us: on_device(): hidden_whole = lax.all_gather(hidden, 'tp', axis=0, tiled=False)]
    dot_general x5 -> x0, matrix products: 9.91 us -> none  [the longest x1 4.01 us: on_device(): jnp.einsum('erh,ehd->erd', hidden_whole, down_weight, preferred_element_t...]
    all_to_all x1, waiting for transfers between devices: 3.48 us -> 12.1 us  [on_device(): lax.all_to_all(outgoing.reshape(ep_count, PAD, width), 'ep', split_axis=0...]
    all_to_all x1, starting transfers between devices: 17.4 us -> 23.9 us  [on_device(): lax.all_to_all(outgoing.reshape(ep_count, PAD, width), 'ep', split_axis=0...]
  transfers between devices with their start and end apart: 3 -> 3, of which waited for: 3 -> 3; matrix products, arithmetic and copies ran while one was open for 2% -> 0% of each run, Pallas kernels for 0% -> 0%
where the time goes in v1:
time: 198 us; the launch traced here: 197 us
  waiting for transfers between devices  100 us (51%)
  blocking collectives  41.3 us (21%)
  starting transfers between devices  24 us (12%)
  Pallas kernels  17.1 us (9%)
  between operations  13.4 us (7%)
    all_gather x1, waiting for transfers between devices, on_device(): hidden_whole = lax.all_gather(hidden, 'tp', axis=0, tiled=False)  48.2 us
    all_gather x1, waiting for transfers between devices, on_device(): features = lax.all_gather(arrived, 'tp', axis=0, tiled=False)  39.8 us
    all_to_all x1, blocking collectives, on_device(): lax.all_to_all(expert_out, 'ep', split_axis=0, concat_axis=0, tiled=True)  27.1 us
    all_to_all x1, starting transfers between devices, on_device(): lax.all_to_all(outgoing.reshape(ep_count, PAD, width), 'ep', split_axis=0...  23.9 us
    all_to_all x1, blocking collectives, on_device(): sums = lax.all_to_all(sums, 'tp', split_axis=0, concat_axis=0, tiled=True)  14.2 us
    all_to_all x1, waiting for transfers between devices, on_device(): lax.all_to_all(outgoing.reshape(ep_count, PAD, width), 'ep', split_axis=0...  12.1 us
    pallas_call x1, Pallas kernels, hidden_of(): pl.pallas_call(hidden_kernel, grid=(row_total // tile,), in_specs=[pl.Blo...  5.67 us
    pallas_call x1, Pallas kernels, down_of(): pl.pallas_call(down_kernel, grid=(row_total // tile,), in_specs=[pl.Block...  5.29 us
  transfers between devices with their start and end apart: 3, of which 3 were waited for; matrix products, arithmetic and copies ran while one was open for 0% of the time, Pallas kernels for 0%

profile of v1, /device:TPU:1, one launch (start us, length us, event | category | flops | bytes accessed | tf_op | source)
XLA Modules:
  0.0 197.4 jit_solution(17672187654815395420)
XLA Ops:
  6.5 2.1 %dispatch.1 = (bf16[1024,128]{1,0:T(8,128)(2,1)}, f32[256,8]{1,0:T(8,128)}) custom-call(bf16[256,128]{1,0:T(8,128)(2,1)} %tok_ref.1, s32[2,256]{1,0:T(2,128)} %bitcast.26, f32[2,256]{1,0:T(2,128)} %bitcast.27), custom_call_target="tpu_custom_call" | custom-call | tf_op jit(solution)/shard_map/dispatch/pallas_call | solution.py:51
  8.6 23.9 %all-to-all-start = ((bf16[64,16,128]{2,1,0:T(8,128)(2,1)}), bf16[64,16,128]{2,1,0:T(8,128)(2,1)S(1)}, u32[]{:S(2)}, u32[]{:S(2)}) async-start(bf16[64,16,128]{2,1,0:T(8,128)(2,1)} %bitcast.25), calls=%async_computation | async-start | bytes 524288 | tf_op jit(solution)/shard_map/all_to_all | solution.py:204
  32.6 0.0 all-gather.5.cloned.1.call-start
  32.6 0.7 fusion.5
  33.3 12.1 %all-to-all-done = bf16[64,16,128]{2,1,0:T(8,128)(2,1)S(1)} async-done(((bf16[64,16,128]{2,1,0:T(8,128)(2,1)}), bf16[64,16,128]{2,1,0:T(8,128)(2,1)S(1)}, u32[]{:S(2)}, u32[]{:S(2)}) %all-to-all-start) | async-done | bytes 262176 | tf_op jit(solution)/shard_map/all_to_all | solution.py:204
  45.4 0.1 reshape.10
  45.5 0.7 pad_maximum_fusion
  46.2 0.0 all-gather.5.cloned.1.call-update
  46.2 0.0 all-gather.7.cloned.1.call-start
  46.2 39.8 %all-gather.5.cloned.1.call-done = bf16[10496,128]{1,0:T(8,128)(2,1)} async-done(((bf16[656,128]{1,0:T(8,128)(2,1)}), bf16[10496,128]{1,0:T(8,128)(2,1)}) %all-gather.5.cloned.1.call-update) | async-done | bytes 2686992 | tf_op jit(solution)/shard_map/all_gather | solution.py:209
  86.0 5.7 %hidden.1 = bf16[640,256]{1,0:T(8,128)(2,1)} custom-call(bf16[16,656,128]{2,1,0:T(8,128)(2,1)} %bitcast.17, bf16[16,656,128]{2,1,0:T(8,128)(2,1)} %bitcast.18, bf16[2048,256]{1,0:T(8,128)(2,1)} %bitcast.23, bf16[2048,256]{1,0:T(8,128)(2,1)} %bitcast.24), custom_call_target="tpu_custom_call" | custom-call | tf_op jit(solution)/shard_map/hidden/pallas_call | solution.py:83
  91.7 0.0 all-gather.7.cloned.1.call-update
  91.7 48.2 %all-gather.7.cloned.1.call-done = bf16[10240,256]{1,0:T(8,128)(2,1)} async-done(((bf16[640,256]{1,0:T(8,128)(2,1)}), bf16[10240,256]{1,0:T(8,128)(2,1)}) %all-gather.7.cloned.1.call-update) | async-done | bytes 5242896 | tf_op jit(solution)/shard_map/all_gather | solution.py:211
  139.9 5.3 %down.1 = bf16[64,16,128]{2,1,0:T(8,128)(2,1)} custom-call(bf16[16,640,256]{2,1,0:T(8,128)(2,1)} %bitcast.19, bf16[4096,128]{1,0:T(8,128)(2,1)} %bitcast.20), custom_call_target="tpu_custom_call" | custom-call | tf_op jit(solution)/shard_map/down/pallas_call | solution.py:120
  145.2 27.1 %all_to_all.15 = bf16[64,16,128]{2,1,0:T(8,128)(2,1)} all-to-all(bf16[64,16,128]{2,1,0:T(8,128)(2,1)} %down.1), channel_id=1, replica_groups=mesh['ep'=64,'tp'=16] {'ep'}, dimensions={0} | all-to-all | bytes 524288 | tf_op jit(solution)/shard_map/all_to_all | solution.py:213
  172.3 2.2 %combine.1 = (f32[256,128]{1,0:T(8,128)}, f32[16,1,256]{2,1,0:T(1,128)}) custom-call(bf16[1024,128]{1,0:T(8,128)(2,1)} %bitcast.21, f32[256,8]{1,0:T(8,128)} %get-tuple-element.10.cols_ref), custom_call_target="tpu_custom_call" | custom-call | tf_op jit(solution)/shard_map/combine/pallas_call | solution.py:155
  174.5 14.2 %all_to_all.16.sums_ref = f32[16,1,256]{2,1,0:T(1,128)} all-to-all(f32[16,1,256]{2,1,0:T(1,128)} %get-tuple-element.12), channel_id=1, replica_groups=mesh['ep'=64,'tp'=16] {'tp'}, dimensions={0} | all-to-all | bytes 32768 | tf_op jit(solution)/shard_map/all_to_all | solution.py:215
  188.7 1.8 final.1
  (1 shorter events, 0.0 us)
Async XLA Ops:
  8.6 36.8 %all-to-all-start = ((bf16[64,16,128]{2,1,0:T(8,128)(2,1)}), bf16[64,16,128]{2,1,0:T(8,128)(2,1)S(1)}, u32[]{:S(2)}, u32[]{:S(2)}) async-start(bf16[64,16,128]{2,1,0:T(8,128)(2,1)} %bitcast.25), calls=%async_computation | async-start | bytes 524288 | tf_op jit(solution)/shard_map/all_to_all | solution.py:204
  32.6 53.4 %all-gather.5.cloned.1.call-start = ((), (), s32[]{:S(2)}) async-start(), calls=%async_computation.3 | async-start | bytes 2854912 | tf_op jit(solution)/shard_map/all_gather | solution.py:209
  46.2 93.7 %all-gather.7.cloned.1.call-start = ((), (), s32[]{:S(2)}) async-start(), calls=%async_computation.4 | async-start | bytes 5570560 | tf_op jit(solution)/shard_map/all_gather | solution.py:211
Sparse Core Ops, SparseCore 0:
  46.3 39.6 all-gather.4
  91.8 48.0 all-gather.6

commit v2 on v1

--- a/solution.py
+++ b/solution.py
@@ -8,6 +8,11 @@
 epsilon = 1e-06
 PAD = 16
 EXTRA = 16
+FIRST = 224
+
+
+def params(mebibytes):
+    return pltpu.CompilerParams(vmem_limit_bytes=mebibytes << 20)
 
 
 def dispatch_kernel(tok_ref, ids_ref, weights_ref, out_ref, cols_ref):
@@ -54,80 +59,226 @@
             jax.ShapeDtypeStruct((slots, width), jnp.bfloat16),
             jax.ShapeDtypeStruct((rows, 8), jnp.float32),
         ),
+        compiler_params=params(8),
         name="dispatch",
     )(tokens, ids, weights)
 
 
-def hidden_kernel(feat_ref, gain_ref, gate_ref, up_ref, out_ref, normed_ref):
-    parts, rows, width = feat_ref.shape
+GROUP = 16
+
+
+def packed_place(shape, slot_axis, capacity):
+    padded = lax.broadcasted_iota(jnp.int32, shape, slot_axis)
+    packed = lax.broadcasted_iota(jnp.int32, shape, 1 - slot_axis)
+    block = padded // PAD
+    slot = padded - block * PAD
+    same = jnp.logical_and(slot < capacity, packed == block * capacity + slot)
+    return jnp.where(same, 1.0, 0.0).astype(jnp.bfloat16)
+
+
+def arrange_kernel(arrived_ref, gain_ref, first_ref, second_ref):
+    total = first_ref.shape[0] - EXTRA + second_ref.shape[0]
+    blocks = arrived_ref.shape[0] // PAD
+    capacity = total // blocks
+    step = GROUP * capacity
+    place = packed_place((step, GROUP * PAD), 1, capacity)
+    for g in range(blocks // GROUP):
+        rows = jnp.dot(
+            place,
+            arrived_ref[g * GROUP * PAD : (g + 1) * GROUP * PAD, :],
+            preferred_element_type=jnp.float32,
+        ).astype(jnp.bfloat16)
+        begin = g * step
+        cut = min(max(FIRST - begin, 0), step)
+        if cut > 0:
+            first_ref[begin : begin + cut, :] = rows[:cut, :]
+        if cut < step:
+            second_ref[begin + cut - FIRST : begin + step - FIRST, :] = rows[cut:, :]
+    gain = gain_ref[...]
+    piece0 = gain.astype(jnp.bfloat16)
+    rest = gain - piece0.astype(jnp.float32)
+    piece1 = rest.astype(jnp.bfloat16)
+    rest = rest - piece1.astype(jnp.float32)
+    piece2 = rest.astype(jnp.bfloat16)
+    empty = jnp.zeros((EXTRA - 3, gain.shape[1]), jnp.float32)
+    lines = jnp.concatenate(
+        [
+            piece0.astype(jnp.float32),
+            piece1.astype(jnp.float32),
+            piece2.astype(jnp.float32),
+            empty,
+        ],
+        axis=0,
+    )
+    first_ref[FIRST : FIRST + EXTRA, :] = lines.astype(jnp.bfloat16)
+
+
+def arrange(arrived, gain, row_total):
+    width = arrived.shape[1]
+    return pl.pallas_call(
+        arrange_kernel,
+        out_shape=(
+            jax.ShapeDtypeStruct((FIRST + EXTRA, width), jnp.bfloat16),
+            jax.ShapeDtypeStruct((row_total - FIRST, width), jnp.bfloat16),
+        ),
+        compiler_params=params(8),
+        name="arrange",
+    )(arrived, gain)
+
+
+def hidden_rows(feat_ref, gain_ref, gate_ref, up_ref, normed_ref, rows):
+    parts, _, width = feat_ref.shape
     full = parts * width
     total = jnp.zeros((rows, width), jnp.float32)
     for j in range(parts):
-        part = feat_ref[j].astype(jnp.float32)
+        part = feat_ref[j, 0:rows, :].astype(jnp.float32)
         total = total + part * part
     scale = lax.rsqrt(jnp.sum(total, axis=1, keepdims=True) / full + epsilon)
     for j in range(parts):
         pieces = gain_ref[j].astype(jnp.float32)
         gain = pieces[0:1, :] + pieces[1:2, :] + pieces[2:3, :]
-        part = feat_ref[j].astype(jnp.float32)
+        part = feat_ref[j, 0:rows, :].astype(jnp.float32)
         normed_ref[:, j * width : (j + 1) * width] = (part * scale * gain).astype(jnp.bfloat16)
     normed = normed_ref[...]
     gate = jnp.dot(normed, gate_ref[...], preferred_element_type=jnp.float32)
     upper = jnp.dot(normed, up_ref[...], preferred_element_type=jnp.float32)
-    out_ref[...] = (gate / (1.0 + jnp.exp(-gate)) * upper).astype(jnp.bfloat16)
-
-
-def hidden_of(features, gate_weight, up_weight, row_total, tile):
+    return (gate / (1.0 + jnp.exp(-gate)) * upper).astype(jnp.bfloat16)
+
+
+def hidden_first_kernel(feat_ref, gain_ref, gate_ref, up_ref, out_ref, normed_ref):
+    rows = out_ref.shape[0]
+    out_ref[...] = hidden_rows(feat_ref, gain_ref, gate_ref, up_ref, normed_ref, rows)
+
+
+def hidden_first(features, gate_weight, up_weight):
     parts, _, width = features.shape
     full, units = gate_weight.shape
-    return pl.pallas_call(
-        hidden_kernel,
-        grid=(row_total // tile,),
+    tile = FIRST // 2
+    return pl.pallas_call(
+        hidden_first_kernel,
+        grid=(2,),
         in_specs=[
             pl.BlockSpec((parts, tile, width), lambda i: (0, i, 0)),
-            pl.BlockSpec((parts, EXTRA, width), lambda i: (0, row_total // EXTRA, 0)),
+            pl.BlockSpec((parts, EXTRA, width), lambda i: (0, FIRST // EXTRA, 0)),
             pl.BlockSpec((full, units), lambda i: (0, 0)),
             pl.BlockSpec((full, units), lambda i: (0, 0)),
         ],
         out_specs=pl.BlockSpec((tile, units), lambda i: (i, 0)),
-        out_shape=jax.ShapeDtypeStruct((row_total, units), jnp.bfloat16),
+        out_shape=jax.ShapeDtypeStruct((FIRST, units), jnp.bfloat16),
         scratch_shapes=[pltpu.VMEM((tile, full), jnp.bfloat16)],
-        name="hidden",
+        compiler_params=params(16),
+        name="hidden_first",
     )(features, features, gate_weight, up_weight)
 
 
-def down_kernel(hidden_ref, down_ref, out_ref):
+def hidden_second_kernel(
+    feat_ref, gain_ref, gate_ref, up_ref, first_ref, out_ref, half0_ref, half1_ref, normed_ref
+):
+    rows = out_ref.shape[0]
+    half = half0_ref.shape[0]
+    half0_ref[...] = first_ref[0:half, :]
+    half1_ref[...] = first_ref[half : 2 * half, :]
+    out_ref[...] = hidden_rows(feat_ref, gain_ref, gate_ref, up_ref, normed_ref, rows)
+
+
+def hidden_second(features, gains, gate_weight, up_weight, first):
+    parts, row_total, width = features.shape
+    full, units = gate_weight.shape
+    tile = row_total // 2
+    half = FIRST // 2
+    return pl.pallas_call(
+        hidden_second_kernel,
+        grid=(2,),
+        in_specs=[
+            pl.BlockSpec((parts, tile, width), lambda i: (0, i, 0)),
+            pl.BlockSpec((parts, EXTRA, width), lambda i: (0, FIRST // EXTRA, 0)),
+            pl.BlockSpec((full, units), lambda i: (0, 0)),
+            pl.BlockSpec((full, units), lambda i: (0, 0)),
+            pl.BlockSpec((FIRST, units), lambda i: (0, 0)),
+        ],
+        out_specs=(
+            pl.BlockSpec((tile, units), lambda i: (i, 0)),
+            pl.BlockSpec((half, units), lambda i: (0, 0)),
+            pl.BlockSpec((half, units), lambda i: (0, 0)),
+        ),
+        out_shape=(
+            jax.ShapeDtypeStruct((row_total, units), jnp.bfloat16),
+            jax.ShapeDtypeStruct((half, units), jnp.bfloat16),
+            jax.ShapeDtypeStruct((half, units), jnp.bfloat16),
+        ),
+        scratch_shapes=[pltpu.VMEM((tile, full), jnp.bfloat16)],
+        compiler_params=params(16),
+        name="hidden_second",
+    )(features, gains, gate_weight, up_weight, first)
+
+
+def down_rows(hidden_ref, down_ref):
     parts, rows, units = hidden_ref.shape
-    blocks, _, width = out_ref.shape
-    capacity = rows // blocks
-    total = jnp.zeros((rows, width), jnp.float32)
+    total = jnp.zeros((rows, down_ref.shape[1]), jnp.float32)
     for j in range(parts):
         total = total + jnp.dot(
             hidden_ref[j],
             down_ref[j * units : (j + 1) * units, :],
             preferred_element_type=jnp.float32,
         )
-    empty = jnp.zeros((PAD - capacity, width), jnp.float32)
-    for b in range(blocks):
-        block = jnp.concatenate([total[b * capacity : (b + 1) * capacity, :], empty], axis=0)
-        out_ref[b] = block.astype(jnp.bfloat16)
-
-
-def down_of(hidden, down_weight, blocks_total, tile_blocks):
-    parts, row_total, units = hidden.shape
+    return total.astype(jnp.bfloat16)
+
+
+def down_first_kernel(half0_ref, half1_ref, down_ref, out_ref):
+    half = half0_ref.shape[1]
+    out_ref[0:half, :] = down_rows(half0_ref, down_ref)
+    out_ref[half : 2 * half, :] = down_rows(half1_ref, down_ref)
+
+
+def down_first(half0, half1, down_weight):
+    return pl.pallas_call(
+        down_first_kernel,
+        out_shape=jax.ShapeDtypeStruct((FIRST, down_weight.shape[1]), jnp.bfloat16),
+        compiler_params=params(16),
+        name="down_first",
+    )(half0, half1, down_weight)
+
+
+def down_second_kernel(hidden_ref, down_ref, first_ref, out_ref, result_ref):
+    rows = hidden_ref.shape[1]
+    total = result_ref.shape[0]
+    blocks = out_ref.shape[0] // PAD
+    capacity = total // blocks
+    step = GROUP * capacity
+    i = pl.program_id(0)
+    begin = pl.multiple_of(FIRST + i * rows, 16)
+    result_ref[pl.ds(begin, rows), :] = down_rows(hidden_ref, down_ref)
+
+    @pl.when(i == pl.num_programs(0) - 1)
+    def _():
+        result_ref[0:FIRST, :] = first_ref[...]
+        place = packed_place((GROUP * PAD, step), 0, capacity)
+        for g in range(blocks // GROUP):
+            out_ref[g * GROUP * PAD : (g + 1) * GROUP * PAD, :] = jnp.dot(
+                place,
+                result_ref[g * step : (g + 1) * step, :],
+                preferred_element_type=jnp.float32,
+            ).astype(jnp.bfloat16)
+
+
+def down_second(hidden, down_weight, first, blocks):
+    parts, rest, units = hidden.shape
     full, width = down_weight.shape
-    tile = row_total // blocks_total * tile_blocks
-    return pl.pallas_call(
-        down_kernel,
-        grid=(row_total // tile,),
+    tile = rest // 2
+    return pl.pallas_call(
+        down_second_kernel,
+        grid=(2,),
         in_specs=[
             pl.BlockSpec((parts, tile, units), lambda i: (0, i, 0)),
             pl.BlockSpec((full, width), lambda i: (0, 0)),
+            pl.BlockSpec((FIRST, width), lambda i: (0, 0)),
         ],
-        out_specs=pl.BlockSpec((tile_blocks, PAD, width), lambda i: (i, 0, 0)),
-        out_shape=jax.ShapeDtypeStruct((blocks_total, PAD, width), jnp.bfloat16),
-        name="down",
-    )(hidden, down_weight)
+        out_specs=pl.BlockSpec((blocks * PAD, width), lambda i: (0, 0)),
+        out_shape=jax.ShapeDtypeStruct((blocks * PAD, width), jnp.bfloat16),
+        scratch_shapes=[pltpu.VMEM((FIRST + rest, width), jnp.bfloat16)],
+        compiler_params=params(16),
+        name="down_second",
+    )(hidden, down_weight, first)
 
 
 def combine_kernel(returned_ref, cols_ref, mixed_ref, sums_ref):
@@ -158,6 +309,7 @@
             jax.ShapeDtypeStruct((rows, width), jnp.float32),
             jax.ShapeDtypeStruct((peers, 1, rows), jnp.float32),
         ),
+        compiler_params=params(8),
         name="combine",
     )(returned, cols)
 
@@ -177,43 +329,56 @@
     return pl.pallas_call(
         final_kernel,
         out_shape=jax.ShapeDtypeStruct(mixed.shape, jnp.bfloat16),
+        compiler_params=params(4),
         name="final",
     )(mixed, sums, gain)
 
 
-def gain_rows(gain):
-    first = lax.reduce_precision(gain, 8, 7)
-    second = lax.reduce_precision(gain - first, 8, 7)
-    third = gain - first - second
-    rows = jnp.stack([first, second, third])
-    return jnp.pad(rows, ((0, EXTRA - 3), (0, 0))).astype(jnp.bfloat16)
+def in_hbm(value):
+    return pltpu.with_memory_space_constraint(value, pltpu.HBM)
+
+
+def everyones(value):
+    return lax.all_gather(value, "tp", axis=0, tiled=False)
+
+
+def exchange(value):
+    width = value.shape[1]
+    blocks = value.reshape(-1, PAD, width)
+    blocks = lax.all_to_all(blocks, "ep", split_axis=0, concat_axis=0, tiled=True)
+    return blocks.reshape(-1, width)
 
 
 def on_device(
     tokens, expert_ids, route_weights, pre_gain, post_gain, gate_weight, up_weight, down_weight
 ):
-    tok_rows, width = tokens.shape
+    tok_rows = tokens.shape[0]
     ep_count = lax.axis_size("ep")
     tp_count = lax.axis_size("tp")
     top_count = expert_ids.shape[1]
     capacity = max(2, tok_rows * top_count * 5 // (4 * ep_count))
     row_total = ep_count * capacity
     outgoing, cols = dispatch(
-        tokens, jnp.transpose(expert_ids), jnp.transpose(route_weights), ep_count * PAD
-    )
-    arrived = lax.all_to_all(
-        outgoing.reshape(ep_count, PAD, width), "ep", split_axis=0, concat_axis=0, tiled=True
-    )
-    arrived = arrived[:, :capacity, :].reshape(row_total, width)
-    arrived = jnp.concatenate([arrived, gain_rows(pre_gain)], axis=0)
-    features = lax.all_gather(arrived, "tp", axis=0, tiled=False)
-    hidden = hidden_of(features, gate_weight[0], up_weight[0], row_total, 160)
-    hidden_whole = lax.all_gather(hidden, "tp", axis=0, tiled=False)
-    expert_out = down_of(hidden_whole, down_weight[0], ep_count, 16)
-    returned = lax.all_to_all(expert_out, "ep", split_axis=0, concat_axis=0, tiled=True)
-    mixed, sums = combine(returned.reshape(ep_count * PAD, width), cols, tp_count)
+        in_hbm(tokens),
+        in_hbm(jnp.transpose(expert_ids)),
+        in_hbm(jnp.transpose(route_weights)),
+        ep_count * PAD,
+    )
+    arrived = exchange(outgoing)
+    part0, part1 = arrange(arrived, in_hbm(pre_gain[None, :]), row_total)
+    features0 = everyones(part0)
+    features1 = in_hbm(everyones(part1))
+    hidden0 = hidden_first(features0, gate_weight[0], up_weight[0])
+    hidden1, half0, half1 = hidden_second(
+        features1, features0, gate_weight[0], up_weight[0], hidden0
+    )
+    whole1 = in_hbm(everyones(hidden1))
+    result0 = down_first(everyones(half0), everyones(half1), down_weight[0])
+    expert_out = down_second(whole1, down_weight[0], result0, ep_count)
+    returned = exchange(expert_out)
+    mixed, sums = combine(returned, cols, tp_count)
     sums = lax.all_to_all(sums, "tp", split_axis=0, concat_axis=0, tiled=True)
-    return final(mixed, sums, post_gain[None, :])
+    return final(mixed, sums, in_hbm(post_gain[None, :]))
 
 
 def solution(mesh):

time: 198 us -> 190 us (0.960)
  blocking collectives: 41.3 us -> 141 us
  waiting for transfers between devices: 100 us -> 16.8 us
  starting transfers between devices: 24 us -> 0.04 us
  local copies, waits for them, and re-layouts: 0.06 us -> 3.71 us
  Pallas kernels: 17.1 us -> 13.7 us
    all_gather x2, waiting for transfers between devices: 88 us -> 16.8 us  [everyones(): return lax.all_gather(value, 'tp', axis=0, tiled=False)]
    all_gather x0 -> x3, blocking collectives: none -> 64.1 us  [everyones(): return lax.all_gather(value, 'tp', axis=0, tiled=False)]
    all_to_all x1 -> x2, blocking collectives: 27.1 us -> 63.3 us  [exchange(): lax.all_to_all(blocks, 'ep', split_axis=0, concat_axis=0, tiled=True)]
    all_to_all x1 -> x0, starting transfers between devices: 23.9 us -> none  [on_device(): lax.all_to_all(outgoing.reshape(ep_count, PAD, width), 'ep', split_axis=0...]
    all_to_all x1 -> x0, waiting for transfers between devices: 12.1 us -> none  [on_device(): lax.all_to_all(outgoing.reshape(ep_count, PAD, width), 'ep', split_axis=0...]
    unnamed x0 -> x12, local copies, waits for them, and re-layouts: none -> 3.71 us
    pallas_call x2 -> x5, Pallas kernels: 11 us -> 10 us  [the longest x1 3.46 us: hidden_second(): pl.pallas_call(hidden_second_kernel, grid=(2,), in_specs=[pl.BlockSpec((p...]
  transfers between devices with their start and end apart: 3 -> 2, of which waited for: 3 -> 2; matrix products, arithmetic and copies ran while one was open for 0% -> 0% of each run, Pallas kernels for 0% -> 1%
where the time goes in v2:
time: 190 us; the launch traced here: 189 us
  blocking collectives  141 us (74%)
  waiting for transfers between devices  16.8 us (9%)
  Pallas kernels  13.7 us (7%)
  between operations  13.4 us (7%)
  local copies, waits for them, and re-layouts  3.71 us (2%)
    all_gather x3, blocking collectives, everyones(): return lax.all_gather(value, 'tp', axis=0, tiled=False)  64.1 us
    all_to_all x2, blocking collectives, exchange(): lax.all_to_all(blocks, 'ep', split_axis=0, concat_axis=0, tiled=True)  63.3 us
    all_gather x2, waiting for transfers between devices, everyones(): return lax.all_gather(value, 'tp', axis=0, tiled=False)  16.8 us
    all_to_all x1, blocking collectives, on_device(): sums = lax.all_to_all(sums, 'tp', split_axis=0, concat_axis=0, tiled=True)  14.1 us
  transfers between devices with their start and end apart: 2, of which 2 were waited for; matrix products, arithmetic and copies ran while one was open for 0% of the time, Pallas kernels for 1%

profile of v2, /device:TPU:1, one launch (start us, length us, event | category | flops | bytes accessed | tf_op | source)
XLA Modules:
  0.0 189.1 jit_solution(11146948849003032525)
XLA Ops:
  6.5 0.0 copy-start.1
  6.5 0.0 all-gather.8.cloned.1.call-start
  6.5 1.5 dispatch.1
  8.0 36.6 %all_to_all.15 = bf16[64,16,128]{2,1,0:T(8,128)(2,1)S(1)} all-to-all(bf16[64,16,128]{2,1,0:T(8,128)(2,1)S(1)} %bitcast.30), channel_id=1, replica_groups=mesh['ep'=64,'tp'=16] {'ep'}, dimensions={0} | all-to-all | bytes 524288 | tf_op jit(solution)/shard_map/all_to_all | solution.py:348
  44.6 1.5 arrange.1
  46.1 0.0 all-gather.8.cloned.1.call-update
  46.1 0.0 all-gather.10.cloned.1.call-start
  46.2 22.9 %all-gather.1 = bf16[3840,128]{1,0:T(8,128)(2,1)S(1)} all-gather(bf16[240,128]{1,0:T(8,128)(2,1)S(1)} %get-tuple-element.16), channel_id=3, replica_groups=mesh['ep'=64,'tp'=16] {'tp'}, dimensions={0}, use_global_device_ids=true | all-gather | bytes 1044480 | tf_op jit(solution)/shard_map/all_gather | solution.py:342
  69.1 0.0 copy-start
  69.1 1.2 copy-done
  70.3 0.0 copy-start.2
  70.3 1.2 copy-done.2
  71.6 0.0 copy-start.3
  71.6 1.4 hidden_first.1.first_ref
  73.0 12.0 %all-gather.8.cloned.1.call-done = bf16[6656,128]{1,0:T(8,128)(2,1)} async-done(((bf16[416,128]{1,0:T(8,128)(2,1)}), bf16[6656,128]{1,0:T(8,128)(2,1)}) %all-gather.8.cloned.1.call-update) | async-done | bytes 1703952 | tf_op jit(solution)/shard_map/all_gather | solution.py:342
  85.0 0.0 copy-done.1
  85.0 0.0 copy-done.3
  85.0 3.5 %hidden_second.1 = (bf16[416,256]{1,0:T(8,128)(2,1)}, bf16[112,256]{1,0:T(8,128)(2,1)S(1)}, bf16[112,256]{1,0:T(8,128)(2,1)S(1)}) custom-call(bf16[16,416,128]{2,1,0:T(8,128)(2,1)} %bitcast.32, bf16[16,240,128]{2,1,0:T(8,128)(2,1)S(1)} %bitcast.18, bf16[2048,256]{1,0:T(8,128)(2,1)S(1)} %bitcast.20, bf16[2048,256]{1,0:T(8,128)(2,1)S(1)} %bitcast.22, ...), custom_call_target="tpu_custom_call" | custom-call | tf_op jit(solution)/shard_map/hidden_second/pallas_call | solution.py:189
  88.5 0.0 copy-start.5
  88.5 0.0 all-gather.10.cloned.1.call-update
  88.5 19.8 %all-gather.3 = bf16[1792,256]{1,0:T(8,128)(2,1)S(1)} all-gather(bf16[112,256]{1,0:T(8,128)(2,1)S(1)} %get-tuple-element.18), channel_id=5, replica_groups=mesh['ep'=64,'tp'=16] {'tp'}, dimensions={0}, use_global_device_ids=true | all-gather | bytes 974848 | tf_op jit(solution)/shard_map/all_gather | solution.py:342
  108.3 21.4 %all-gather.4 = bf16[1792,256]{1,0:T(8,128)(2,1)S(1)} all-gather(bf16[112,256]{1,0:T(8,128)(2,1)S(1)} %get-tuple-element.19), channel_id=6, replica_groups=mesh['ep'=64,'tp'=16] {'tp'}, dimensions={0}, use_global_device_ids=true | all-gather | bytes 974848 | tf_op jit(solution)/shard_map/all_gather | solution.py:342
  129.7 0.0 copy-start.4
  129.7 1.2 copy-done.4
  130.9 0.6 down_first.1.first_ref
  131.6 4.8 %all-gather.10.cloned.1.call-done = bf16[6656,256]{1,0:T(8,128)(2,1)} async-done(((bf16[416,256]{1,0:T(8,128)(2,1)}), bf16[6656,256]{1,0:T(8,128)(2,1)}) %all-gather.10.cloned.1.call-update) | async-done | bytes 3407888 | tf_op jit(solution)/shard_map/all_gather | solution.py:342
  136.3 0.0 copy-done.5
  136.4 3.0 %down_second.1 = bf16[1024,128]{1,0:T(8,128)(2,1)S(1)} custom-call(bf16[16,416,256]{2,1,0:T(8,128)(2,1)} %bitcast.31, bf16[4096,128]{1,0:T(8,128)(2,1)S(1)} %bitcast.24, bf16[224,128]{1,0:T(8,128)(2,1)S(1)} %down_first.1.first_ref), custom_call_target="tpu_custom_call" | custom-call | tf_op jit(solution)/shard_map/down_second/pallas_call | solution.py:268
  139.3 26.7 %all_to_all.16 = bf16[64,16,128]{2,1,0:T(8,128)(2,1)S(1)} all-to-all(bf16[64,16,128]{2,1,0:T(8,128)(2,1)S(1)} %bitcast.27), channel_id=1, replica_groups=mesh['ep'=64,'tp'=16] {'ep'}, dimensions={0} | all-to-all | bytes 524288 | tf_op jit(solution)/shard_map/all_to_all | solution.py:348
  166.0 0.6 combine.1
  166.6 14.1 %all_to_all.17.sums_ref = f32[16,1,256]{2,1,0:T(1,128)S(1)} all-to-all(f32[16,1,256]{2,1,0:T(1,128)S(1)} %get-tuple-element.22), channel_id=1, replica_groups=mesh['ep'=64,'tp'=16] {'tp'}, dimensions={0} | all-to-all | bytes 32768 | tf_op jit(solution)/shard_map/all_to_all | solution.py:380
  180.7 1.6 final.1
Async XLA Ops:
  6.5 78.5 %copy-start.1 = (bf16[1,2048,256]{2,1,0:T(8,128)(2,1)S(1)}, bf16[1,2048,256]{2,1,0:T(8,128)(2,1)}, u32[]{:S(2)}) copy-start(bf16[1,2048,256]{2,1,0:T(8,128)(2,1)} %param.13) | copy-start | bytes 3145732
  6.5 78.5 %all-gather.8.cloned.1.call-start = ((), (), s32[]{:S(2)}) async-start(), calls=%async_computation.3 | async-start | bytes 1810432 | tf_op jit(solution)/shard_map/all_gather | solution.py:342
  46.1 90.2 %all-gather.10.cloned.1.call-start = ((), (), s32[]{:S(2)}) async-start(), calls=%async_computation.4 | async-start | bytes 3620864 | tf_op jit(solution)/shard_map/all_gather | solution.py:342
  69.1 1.2 copy-start
  70.3 1.2 copy-start.2
  71.6 13.4 %copy-start.3 = (bf16[1,2048,256]{2,1,0:T(8,128)(2,1)S(1)}, bf16[1,2048,256]{2,1,0:T(8,128)(2,1)}, u32[]{:S(2)}) copy-start(bf16[1,2048,256]{2,1,0:T(8,128)(2,1)} %param.14) | copy-start | bytes 3145732
  88.5 47.9 %copy-start.5 = (bf16[1,4096,128]{2,1,0:T(8,128)(2,1)S(1)}, bf16[1,4096,128]{2,1,0:T(8,128)(2,1)}, u32[]{:S(2)}) copy-start(bf16[1,4096,128]{2,1,0:T(8,128)(2,1)} %param.15) | copy-start | bytes 3145732
  129.7 1.2 copy-start.4
Sparse Core Ops, SparseCore 0:
  46.3 38.6 all-gather.7
  88.6 47.6 all-gather.9

commit v3 on v1

v3 whole, which is shorter than its diff:
```python
import jax
import jax.numpy as jnp
from jax import lax
from jax.experimental import pallas as pl
from jax.experimental.pallas import tpu as pltpu
from jax.sharding import Mesh, PartitionSpec as P

epsilon = 1e-06
CORES = 2
PAD = 8
EXTRA = 16
GROUP = 16
TAKEN = 120
GATHERED = 3


def params(mebibytes):
    return pltpu.CompilerParams(vmem_limit_bytes=mebibytes << 20)


def in_hbm(value):
    return pltpu.with_memory_space_constraint(value, pltpu.HBM)


def whole(memory_space=pltpu.VMEM):
    return pl.BlockSpec(memory_space=memory_space)


def prepare_kernel(tok_ref, gain_ref, out_ref):
    rows = tok_ref.shape[0]
    out_ref[0:rows, :] = tok_ref[...]
    gain = gain_ref[...]
    piece0 = gain.astype(jnp.bfloat16).astype(jnp.float32)
    piece1 = (gain - piece0).astype(jnp.bfloat16).astype(jnp.float32)
    piece2 = gain - piece0 - piece1
    empty = jnp.zeros((EXTRA - 3, gain.shape[1]), jnp.float32)
    lines = jnp.concatenate([piece0, piece1, piece2, empty], axis=0)
    out_ref[rows : rows + EXTRA, :] = lines.astype(jnp.bfloat16)


def prepare(tokens, gain):
    rows, width = tokens.shape
    return pl.pallas_call(
        prepare_kernel,
        out_shape=jax.ShapeDtypeStruct((rows + EXTRA, width), jnp.bfloat16),
        compiler_params=params(4),
        name="prepare",
    )(tokens, gain)


def dispatch_kernel(core_ref, tok_ref, ids_ref, weights_ref, out_ref, cols_ref, *, capacity):
    rows = ids_ref.shape[1]
    slots = out_ref.shape[0]
    experts = slots // PAD
    ids = ids_ref[...]
    expert_index = lax.broadcasted_iota(jnp.int32, (experts, rows), 0)
    hot0 = jnp.where(expert_index == ids[0:1, :], 1.0, 0.0)
    hot1 = jnp.where(expert_index == ids[1:2, :], 1.0, 0.0)
    earlier = lax.broadcasted_iota(jnp.int32, (rows, rows), 0) < lax.broadcasted_iota(
        jnp.int32, (rows, rows), 1
    )
    earlier = jnp.where(earlier, 1.0, 0.0).astype(jnp.bfloat16)
    counts = jnp.dot((hot0 + hot1).astype(jnp.bfloat16), earlier, preferred_element_type=jnp.float32)
    half = capacity // CORES
    targets = []
    for k, hot in enumerate((hot0, hot1)):
        slot = jnp.sum(hot * counts, axis=0, keepdims=True).astype(jnp.int32)
        slot = slot - core_ref[0] * half
        mine = jnp.logical_and(slot >= 0, slot < half)
        targets.append(jnp.where(mine, ids[k : k + 1, :] * PAD + slot, -1))
    slot_index = lax.broadcasted_iota(jnp.int32, (slots, rows), 0)
    chosen = jnp.logical_or(slot_index == targets[0], slot_index == targets[1])
    chosen = jnp.where(chosen, 1.0, 0.0).astype(jnp.bfloat16)
    width = tok_ref.shape[2]
    for c in range(CORES):
        out_ref[:, c * width : (c + 1) * width] = jnp.dot(
            chosen, tok_ref[c, 0:rows, :], preferred_element_type=jnp.float32
        ).astype(jnp.bfloat16)
    lines = jnp.concatenate(
        [
            targets[0].astype(jnp.float32),
            targets[1].astype(jnp.float32),
            weights_ref[...],
            jnp.zeros((4, rows), jnp.float32),
        ],
        axis=0,
    )
    cols_ref[...] = jnp.transpose(lines)


def dispatch(core, tokens, ids, weights, experts, capacity):
    rows = ids.shape[1]
    width = tokens.shape[2]

    def body(*refs):
        dispatch_kernel(*refs, capacity=capacity)

    return pl.pallas_call(
        body,
        in_specs=[whole(pltpu.SMEM), whole(), whole(), whole()],
        out_shape=(
            jax.ShapeDtypeStruct((experts * PAD, CORES * width), jnp.bfloat16),
            jax.ShapeDtypeStruct((rows, 8), jnp.float32),
        ),
        compiler_params=params(8),
        name="dispatch",
    )(core, tokens, ids, weights)


def packed_place(shape, slot_axis, capacity):
    padded = lax.broadcasted_iota(jnp.int32, shape, slot_axis)
    packed = lax.broadcasted_iota(jnp.int32, shape, 1 - slot_axis)
    block = padded // PAD
    slot = padded - block * PAD
    same = jnp.logical_and(slot < capacity, packed == block * capacity + slot)
    return jnp.where(same, 1.0, 0.0).astype(jnp.bfloat16)


def arrange_kernel(arrived_ref, tok_ref, first_ref, second_ref, *, half):
    step = GROUP * half
    width = tok_ref.shape[2]
    first = tok_ref.shape[1] - EXTRA
    place = packed_place((step, GROUP * PAD), 1, half)
    groups = arrived_ref.shape[0] // (GROUP * PAD)
    for g in range(groups):
        rows = jnp.dot(
            place,
            arrived_ref[g * GROUP * PAD : (g + 1) * GROUP * PAD, :],
            preferred_element_type=jnp.float32,
        ).astype(jnp.bfloat16)
        if g < GATHERED:
            first_ref[g * step : (g + 1) * step, :] = rows
        else:
            begin = (g - GATHERED) * step
            for j in range(second_ref.shape[0]):
                second_ref[j, begin : begin + step, :] = rows
    last = (groups - GATHERED) * step
    for j in range(second_ref.shape[0]):
        for c in range(CORES):
            second_ref[j, last : last + EXTRA, c * width : (c + 1) * width] = tok_ref[
                c, first : first + EXTRA, :
            ]


def arrange(arrived, tokens, chips, half):
    groups = arrived.shape[0] // (GROUP * PAD)
    width = arrived.shape[1]
    step = GROUP * half

    def body(*refs):
        arrange_kernel(*refs, half=half)

    return pl.pallas_call(
        body,
        out_shape=(
            jax.ShapeDtypeStruct((GATHERED * step, width), jnp.bfloat16),
            jax.ShapeDtypeStruct(
                (chips, (groups - GATHERED) * step + EXTRA, width), jnp.bfloat16
            ),
        ),
        compiler_params=params(8),
        name="arrange",
    )(arrived, tokens)


def hidden_kernel(
    core_ref,
    first_ref,
    second_ref,
    gate0_ref,
    up0_ref,
    gate1_ref,
    up1_ref,
    out0_ref,
    out1_ref,
    normed_ref,
    hidden_ref,
):
    chips, _, wide = first_ref.shape
    full = chips * wide
    units = gate0_ref.shape[1]
    first = first_ref.shape[1]
    last = second_ref.shape[1] - EXTRA
    for at, ref, rows in ((0, first_ref, first), (first, second_ref, last)):
        total = jnp.zeros((rows, wide), jnp.float32)
        for j in range(chips):
            part = ref[j, 0:rows, :].astype(jnp.float32)
            total = total + part * part
        scale = lax.rsqrt(jnp.sum(total, axis=1, keepdims=True) / full + epsilon)
        for j in range(chips):
            pieces = second_ref[j, last : last + EXTRA, :].astype(jnp.float32)
            gain = pieces[0:1, :] + pieces[1:2, :] + pieces[2:3, :]
            part = ref[j, 0:rows, :].astype(jnp.float32)
            normed_ref[at : at + rows, j * wide : (j + 1) * wide] = (part * scale * gain).astype(
                jnp.bfloat16
            )

    def hidden_of(gate_ref, up_ref):
        normed = normed_ref[...]
        gate = jnp.dot(normed, gate_ref[...], preferred_element_type=jnp.float32)
        upper = jnp.dot(normed, up_ref[...], preferred_element_type=jnp.float32)
        return (gate / (1.0 + jnp.exp(-gate)) * upper).astype(jnp.bfloat16)

    own = hidden_of(gate0_ref, up0_ref)
    other = hidden_of(gate1_ref, up1_ref)
    for c in range(CORES):

        @pl.when(core_ref[0] == c)
        def _():
            hidden_ref[:, c * units : (c + 1) * units] = own
            hidden_ref[:, (1 - c) * units : (2 - c) * units] = other

    rows0 = out0_ref.shape[0]
    out0_ref[...] = hidden_ref[0:rows0, :]
    for j in range(chips):
        out1_ref[j] = hidden_ref[rows0:, :]


def hidden_of(core, first, second, gate0, up0, gate1, up1):
    chips, _, wide = first.shape
    rows = first.shape[1] + second.shape[1] - EXTRA
    units = gate0.shape[1]
    return pl.pallas_call(
        hidden_kernel,
        in_specs=[whole(pltpu.SMEM)] + [whole()] * 6,
        out_shape=(
            jax.ShapeDtypeStruct((TAKEN, CORES * units), jnp.bfloat16),
            jax.ShapeDtypeStruct((chips, rows - TAKEN, CORES * units), jnp.bfloat16),
        ),
        scratch_shapes=[
            pltpu.VMEM((rows, chips * wide), jnp.bfloat16),
            pltpu.VMEM((rows, CORES * units), jnp.bfloat16),
        ],
        compiler_params=params(24),
        name="hidden",
    )(core, first, second, gate0, up0, gate1, up1)


def down_kernel(
    core_ref, hidden0_ref, hidden1_ref, down0_ref, down1_ref, out_ref, down_ref, result_ref, *, half
):
    chips, rows0, units = hidden0_ref.shape
    width = down0_ref.shape[1]
    for c in range(CORES):

        @pl.when(core_ref[0] == c)
        def _():
            down_ref[:, c * width : (c + 1) * width] = down0_ref[...]
            down_ref[:, (1 - c) * width : (2 - c) * width] = down1_ref[...]

    for at, ref in ((0, hidden0_ref), (rows0, hidden1_ref)):
        rows = ref.shape[1]
        total = jnp.zeros((rows, CORES * width), jnp.float32)
        for j in range(chips):
            total = total + jnp.dot(
                ref[j],
                down_ref[j * units : (j + 1) * units, :],
                preferred_element_type=jnp.float32,
            )
        result_ref[at : at + rows, :] = total.astype(jnp.bfloat16)
    step = GROUP * half
    place = packed_place((GROUP * PAD, step), 0, half)
    for g in range(out_ref.shape[0] // (GROUP * PAD)):
        out_ref[g * GROUP * PAD : (g + 1) * GROUP * PAD, :] = jnp.dot(
            place, result_ref[g * step : (g + 1) * step, :], preferred_element_type=jnp.float32
        ).astype(jnp.bfloat16)


def down_of(core, hidden0, hidden1, down0, down1, half):
    rows = hidden0.shape[1] + hidden1.shape[1]
    full, width = down0.shape

    def body(*refs):
        down_kernel(*refs, half=half)

    return pl.pallas_call(
        body,
        in_specs=[whole(pltpu.SMEM)] + [whole()] * 4,
        out_shape=jax.ShapeDtypeStruct((rows // half * PAD, CORES * width), jnp.bfloat16),
        scratch_shapes=[
            pltpu.VMEM((full, CORES * width), jnp.bfloat16),
            pltpu.VMEM((rows, CORES * width), jnp.bfloat16),
        ],
        compiler_params=params(24),
        name="down",
    )(core, hidden0, hidden1, down0, down1)


def combine_kernel(returned_ref, cols_ref, mixed_ref):
    _, rows, width = mixed_ref.shape
    slots = returned_ref.shape[0]
    cols = cols_ref[...]
    targets = cols[:, 0:2].astype(jnp.int32)
    slot_index = lax.broadcasted_iota(jnp.int32, (rows, slots), 1)
    returned = returned_ref[...]
    mixed = jnp.zeros((rows, CORES * width), jnp.float32)
    for k in range(2):
        chosen = jnp.where(slot_index == targets[:, k : k + 1], 1.0, 0.0).astype(jnp.bfloat16)
        picked = jnp.dot(chosen, returned, preferred_element_type=jnp.float32)
        mixed = mixed + picked * cols[:, 2 + k : 3 + k]
    for c in range(CORES):
        mixed_ref[c] = mixed[:, c * width : (c + 1) * width]


def combine(returned, cols):
    wide = returned.shape[1]
    rows = cols.shape[0]
    return pl.pallas_call(
        combine_kernel,
        out_shape=jax.ShapeDtypeStruct((CORES, rows, wide // CORES), jnp.float32),
        compiler_params=params(8),
        name="combine",
    )(returned, cols)


def sums_kernel(mixed_ref, sums_ref):
    _, rows, _ = mixed_ref.shape
    mixed = mixed_ref[0] + mixed_ref[1]
    sums = jnp.sum(mixed * mixed, axis=1, keepdims=True)
    line = jnp.transpose(jnp.broadcast_to(sums, (rows, 128)))[0:1, :]
    for j in range(sums_ref.shape[0]):
        sums_ref[j] = line


def sums_of(mixed, peers):
    return pl.pallas_call(
        sums_kernel,
        out_shape=jax.ShapeDtypeStruct((peers, 1, mixed.shape[1]), jnp.float32),
        compiler_params=params(4),
        name="sums",
    )(mixed)


def final_kernel(mixed_ref, sums_ref, gain_ref, out_ref):
    rows, width = out_ref.shape
    peers = sums_ref.shape[0]
    total = sums_ref[0]
    for j in range(1, peers):
        total = total + sums_ref[j]
    scale = lax.rsqrt(total / (peers * width) + epsilon)
    column = jnp.transpose(jnp.broadcast_to(scale, (8, rows)))[:, 0:1]
    mixed = mixed_ref[0] + mixed_ref[1]
    out_ref[...] = (mixed * column * gain_ref[...]).astype(jnp.bfloat16)


def final(mixed, sums, gain):
    return pl.pallas_call(
        final_kernel,
        out_shape=jax.ShapeDtypeStruct(mixed.shape[1:], jnp.bfloat16),
        compiler_params=params(4),
        name="final",
    )(mixed, sums, gain)


def exchange(value, axis):
    return lax.all_to_all(value, axis, split_axis=0, concat_axis=0, tiled=True)


def blocks_exchange(value):
    wide = value.shape[1]
    return exchange(value.reshape(-1, PAD, wide), "ep").reshape(-1, wide)


def swap(value):
    return lax.ppermute(value, "c", [(0, 1), (1, 0)])


def on_device(
    tokens, expert_ids, route_weights, pre_gain, post_gain, gate_weight, up_weight, down_weight
):
    tok_rows = tokens.shape[0]
    ep_count = lax.axis_size("ep")
    chips = lax.axis_size("x")
    top_count = expert_ids.shape[1]
    capacity = max(2, tok_rows * top_count * 5 // (4 * ep_count))
    half = capacity // CORES
    core = lax.axis_index("c").astype(jnp.int32).reshape(1)
    gate0, up0 = gate_weight[0], up_weight[0]
    down0 = down_weight[0]
    gate1, up1, down1 = in_hbm(swap(gate0)), in_hbm(swap(up0)), in_hbm(swap(down0))
    both = lax.all_gather(prepare(in_hbm(tokens), in_hbm(pre_gain[None, :])), "c", axis=0)
    outgoing, cols = dispatch(
        core,
        both,
        in_hbm(jnp.transpose(expert_ids)),
        in_hbm(jnp.transpose(route_weights)),
        ep_count,
        capacity,
    )
    arrived = blocks_exchange(outgoing)
    first, second = arrange(arrived, both, chips, half)
    second = exchange(second, "x")
    first = lax.all_gather(first, "x", axis=0)
    hidden0, hidden1 = hidden_of(core, first, second, gate0, up0, gate1, up1)
    hidden1 = exchange(hidden1, "x")
    hidden0 = lax.all_gather(hidden0, "x", axis=0)
    returned = blocks_exchange(down_of(core, hidden0, hidden1, down0, down1, half))
    mixed = exchange(combine(returned, cols), "c")
    sums = exchange(sums_of(mixed, chips * CORES), ("x", "c"))
    return final(mixed, sums, in_hbm(post_gain[None, :]))


def solution(mesh):
    ep_count, tp_count = mesh.devices.shape
    devices = mesh.devices.reshape(ep_count, tp_count // CORES, CORES)
    return jax.shard_map(
        on_device,
        mesh=Mesh(devices, ("ep", "x", "c")),
        in_specs=(
            P("ep", ("x", "c")),
            P("ep", None),
            P("ep", None),
            P(("x", "c")),
            P(("x", "c")),
            P("ep", None, ("x", "c")),
            P("ep", None, ("x", "c")),
            P("ep", None, ("x", "c")),
        ),
        out_specs=P("ep", ("x", "c")),
        check_vma=False,
    )
```

time: 198 us -> 192 us (0.970)
  waiting for transfers between devices: 100 us -> 8.72 us
  blocking collectives: 41.3 us -> 131 us
  between operations: 13.4 us -> 0.1 us
  starting transfers between devices: 24 us -> 35.9 us
  Pallas kernels: 17.1 us -> 13.6 us
    all_gather x2 -> x0, waiting for transfers between devices: 88 us -> none  [the longest x1 48.2 us: on_device(): hidden_whole = lax.all_gather(hidden, 'tp', axis=0, tiled=False)]
    all_gather x0 -> x3, blocking collectives: none -> 87.6 us  [the longest x1 44.6 us: on_device(): hidden0 = lax.all_gather(hidden0, 'x', axis=0)]
    ppermute x0 -> x3, starting transfers between devices: none -> 13.7 us  [swap(): return lax.ppermute(value, 'c', [(0, 1), (1, 0)])]
    pallas_call x5 -> x8, Pallas kernels: 17.1 us -> 13.6 us  [the longest x1 4.61 us: hidden_of(): pl.pallas_call(hidden_kernel, in_specs=[whole(pltpu.SMEM)] + [whole()] *...]
    all_to_all x1 -> x3, waiting for transfers between devices: 12.1 us -> 8.71 us  [exchange(): return lax.all_to_all(value, axis, split_axis=0, concat_axis=0, tiled=True)]
    all_to_all x2 -> x3, blocking collectives: 41.3 us -> 43.7 us  [exchange(): return lax.all_to_all(value, axis, split_axis=0, concat_axis=0, tiled=True)]
    all_to_all x1 -> x3, starting transfers between devices: 23.9 us -> 22.3 us  [exchange(): return lax.all_to_all(value, axis, split_axis=0, concat_axis=0, tiled=True)]
  transfers between devices with their start and end apart: 3 -> 6, of which waited for: 3 -> 1; matrix products, arithmetic and copies ran while one was open for 0% -> 0% of each run, Pallas kernels for 0% -> 0%
where the time goes in v3:
time: 192 us
  blocking collectives  131 us (68%)
  starting transfers between devices  35.9 us (19%)
  Pallas kernels  13.6 us (7%)
  waiting for transfers between devices  8.72 us (5%)
  local copies, waits for them, and re-layouts  1.98 us (1%)
    all_gather x1, blocking collectives, on_device(): hidden0 = lax.all_gather(hidden0, 'x', axis=0)  44.6 us
    all_to_all x3, blocking collectives, exchange(): return lax.all_to_all(value, axis, split_axis=0, concat_axis=0, tiled=True)  43.7 us
    all_gather x1, blocking collectives, on_device(): first = lax.all_gather(first, 'x', axis=0)  27.4 us
    all_to_all x3, starting transfers between devices, exchange(): return lax.all_to_all(value, axis, split_axis=0, concat_axis=0, tiled=True)  22.3 us
    all_gather x1, blocking collectives, on_device(): lax.all_gather(prepare(in_hbm(tokens), in_hbm(pre_gain[None, :])), 'c', a...  15.7 us
    ppermute x3, starting transfers between devices, swap(): return lax.ppermute(value, 'c', [(0, 1), (1, 0)])  13.7 us
    all_to_all x3, waiting for transfers between devices, exchange(): return lax.all_to_all(value, axis, split_axis=0, concat_axis=0, tiled=True)  8.71 us
    pallas_call x1, Pallas kernels, hidden_of(): pl.pallas_call(hidden_kernel, in_specs=[whole(pltpu.SMEM)] + [whole()] *...  4.61 us
  transfers between devices with their start and end apart: 6, of which 1 were waited for; matrix products, arithmetic and copies ran while one was open for 0% of the time, Pallas kernels for 0%

profile of v3, /device:TPU:1, one launch (start us, length us, event | category | flops | bytes accessed | tf_op | source)
XLA Modules:
  0.0 191.6 jit_solution(8791643478307164)
XLA Ops:
  0.0 1.0 prepare.1
  1.0 15.7 %all-gather = bf16[544,128]{1,0:T(8,128)(2,1)S(1)} all-gather(bf16[272,128]{1,0:T(8,128)(2,1)S(1)} %prepare.1), channel_id=2, replica_groups=mesh['ep'=64,'x'=8,'c'=2] {'c'}, dimensions={0}, use_global_device_ids=true | all-gather | bytes 208896 | tf_op jit(solution)/shard_map/all_gather | solution.py:381
  16.7 1.9 dispatch.1
  18.6 0.7 copy-done.2
  19.2 10.5 %all-to-all-start = ((bf16[64,8,256]{2,1,0:T(8,128)(2,1)}), bf16[64,8,256]{2,1,0:T(8,128)(2,1)S(1)}, u32[]{:S(2)}, u32[]{:S(2)}) async-start(bf16[64,8,256]{2,1,0:T(8,128)(2,1)} %bitcast.5), calls=%async_computation | async-start | bytes 524288 | tf_op jit(solution)/shard_map/all_to_all | solution.py:356
  29.7 2.5 %collective-permute-start = (bf16[2048,256]{1,0:T(8,128)(2,1)}, bf16[2048,256]{1,0:T(8,128)(2,1)}, u32[]{:S(2)}, u32[]{:S(2)}) collective-permute-start(bf16[2048,256]{1,0:T(8,128)(2,1)} %bitcast.22), channel_id=1, source_target_pairs={{0,1},{1,0},{2,3},{3,2},{4,5},{5,4},{6,7},{7,6},{8,9},{9,8},{10,11... | collective-permute-start | bytes 3145736 | tf_op jit(solution)/shard_map/ppermute | solution.py:365
  32.3 1.9 %collective-permute-start.1 = (bf16[2048,256]{1,0:T(8,128)(2,1)}, bf16[2048,256]{1,0:T(8,128)(2,1)}, u32[]{:S(2)}, u32[]{:S(2)}) collective-permute-start(bf16[2048,256]{1,0:T(8,128)(2,1)} %bitcast.24), channel_id=1, source_target_pairs={{0,1},{1,0},{2,3},{3,2},{4,5},{5,4},{6,7},{7,6},{8,9},{9,8},{10,11... | collective-permute-start | bytes 3145736 | tf_op jit(solution)/shard_map/ppermute | solution.py:365
  34.2 8.7 %all-to-all-done = bf16[64,8,256]{2,1,0:T(8,128)(2,1)S(1)} async-done(((bf16[64,8,256]{2,1,0:T(8,128)(2,1)}), bf16[64,8,256]{2,1,0:T(8,128)(2,1)S(1)}, u32[]{:S(2)}, u32[]{:S(2)}) %all-to-all-start) | async-done | bytes 262176 | tf_op jit(solution)/shard_map/all_to_all | solution.py:356
  42.9 1.0 arrange.1
  43.9 0.6 copy-done.6
  44.5 6.5 %all-to-all-start.1 = ((bf16[8,96,256]{2,1,0:T(8,128)(2,1)}), bf16[8,96,256]{2,1,0:T(8,128)(2,1)S(1)}, u32[]{:S(2)}, u32[]{:S(2)}) async-start(bf16[8,96,256]{2,1,0:T(8,128)(2,1)} %get-tuple-element.13), calls=%async_computation.1 | async-start | bytes 786432 | tf_op jit(solution)/shard_map/all_to_all | solution.py:356
  51.0 27.4 %all-gather.1 = bf16[1920,256]{1,0:T(8,128)(2,1)S(1)} all-gather(bf16[240,256]{1,0:T(8,128)(2,1)} %copy-done.6), channel_id=3, replica_groups=mesh['ep'=64,'x'=8,'c'=2] {'x'}, dimensions={0}, use_global_device_ids=true | all-gather | bytes 1105920 | tf_op jit(solution)/shard_map/all_gather | solution.py:393
  78.4 0.0 collective-permute-done.gate1_ref
  78.4 0.0 collective-permute-done.1.up1_ref
  78.4 0.0 all-to-all-done.1.second_ref
  78.4 0.0 copy-done
  78.4 0.0 copy-done.1
  78.4 4.6 %hidden.1 = (bf16[120,512]{1,0:T(8,128)(2,1)S(1)}, bf16[8,200,512]{2,1,0:T(8,128)(2,1)}) custom-call(s32[1]{0:T(128)} %bitcast.refs_0_.core_ref, bf16[8,240,256]{2,1,0:T(8,128)(2,1)S(1)} %bitcast.16, bf16[8,96,256]{2,1,0:T(8,128)(2,1)S(1)} %all-to-all-done.1.second_ref, bf16[2048,256]{1,0:T(8,128)(2,1)S(1)} %bitcast.23, bf16[2048,256]{1,0:T(8,128)(2,1)S(1)} %bitcast.25, ...), custom_call_target="tpu_custom_call" | custom-call | tf_op jit(solution)/shard_map/hidden/pallas_call | solution.py:223
  83.0 0.7 copy-done.4
  83.7 5.3 %all-to-all-start.2 = ((bf16[8,200,512]{2,1,0:T(8,128)(2,1)}), bf16[8,200,512]{2,1,0:T(8,128)(2,1)S(1)}, u32[]{:S(2)}, u32[]{:S(2)}) async-start(bf16[8,200,512]{2,1,0:T(8,128)(2,1)} %get-tuple-element.15), calls=%async_computation.2 | async-start | bytes 3276800 | tf_op jit(solution)/shard_map/all_to_all | solution.py:356
  88.9 9.2 %collective-permute-start.2 = (bf16[4096,128]{1,0:T(8,128)(2,1)}, bf16[4096,128]{1,0:T(8,128)(2,1)}, u32[]{:S(2)}, u32[]{:S(2)}) collective-permute-start(bf16[4096,128]{1,0:T(8,128)(2,1)} %bitcast.11.refs_3_), channel_id=1, source_target_pairs={{0,1},{1,0},{2,3},{3,2},{4,5},{5,4},{6,7},{7,6},{8,9},{9,8},{10,11... | collective-permute-start | bytes 3145736 | tf_op jit(solution)/shard_map/ppermute | solution.py:365
  98.2 44.6 %all-gather.2 = bf16[960,512]{1,0:T(8,128)(2,1)S(1)} all-gather(bf16[120,512]{1,0:T(8,128)(2,1)S(1)} %copy-done.5), channel_id=4, replica_groups=mesh['ep'=64,'x'=8,'c'=2] {'x'}, dimensions={0}, use_global_device_ids=true | all-gather | bytes 1105920 | tf_op jit(solution)/shard_map/all_gather | solution.py:396
  142.8 0.0 collective-permute-done.2.refs_4_
  142.8 0.0 all-to-all-done.2.refs_2_
  142.8 3.1 %down.1 = bf16[512,256]{1,0:T(8,128)(2,1)S(1)} custom-call(s32[1]{0:T(128)} %bitcast.refs_0_.core_ref, bf16[8,120,512]{2,1,0:T(8,128)(2,1)S(1)} %bitcast.15, bf16[8,200,512]{2,1,0:T(8,128)(2,1)S(1)} %all-to-all-done.2.refs_2_, bf16[4096,128]{1,0:T(8,128)(2,1)} %bitcast.11.refs_3_, bf16[4096,128]{1,0:T(8,128)(2,1)} %collective-permute-done.2.refs_4_), custom_call_target="tpu_custom_call" | custom-call | tf_op jit(solution)/shard_map/down/pallas_call | solution.py:276
  145.9 17.7 %all_to_all.30 = bf16[64,8,256]{2,1,0:T(8,128)(2,1)S(1)} all-to-all(bf16[64,8,256]{2,1,0:T(8,128)(2,1)S(1)} %bitcast.19), channel_id=1, replica_groups=mesh['ep'=64,'x'=8,'c'=2] {'ep'}, dimensions={0} | all-to-all | bytes 524288 | tf_op jit(solution)/shard_map/all_to_all | solution.py:356
  163.6 0.0 copy-done.3
  163.6 0.4 combine.1
  164.0 13.2 %all_to_all.31.mixed_ref = f32[2,256,128]{2,1,0:T(8,128)S(1)} all-to-all(f32[2,256,128]{2,1,0:T(8,128)S(1)} %combine.1), channel_id=1, replica_groups=mesh['ep'=64,'x'=8,'c'=2] {'c'}, dimensions={0} | all-to-all | bytes 524288 | tf_op jit(solution)/shard_map/all_to_all | solution.py:356
  177.2 0.1 sums.1
  177.3 12.8 %all_to_all.32.sums_ref = f32[16,1,256]{2,1,0:T(1,128)S(1)} all-to-all(f32[16,1,256]{2,1,0:T(1,128)S(1)} %sums.1), channel_id=1, replica_groups=mesh['ep'=64,'x'=8,'c'=2] {'x','c'}, dimensions={0} | all-to-all | bytes 32768 | tf_op jit(solution)/shard_map/all_to_all | solution.py:356
  190.1 1.6 final.1
  (8 shorter events, 0.0 us)
Async XLA Ops:
  0.0 78.4 %copy-start = (bf16[1,2048,256]{2,1,0:T(8,128)(2,1)S(1)}, bf16[1,2048,256]{2,1,0:T(8,128)(2,1)}, u32[]{:S(2)}) copy-start(bf16[1,2048,256]{2,1,0:T(8,128)(2,1)} %param.13) | copy-start | bytes 3145732
  0.0 78.4 %copy-start.1 = (bf16[1,2048,256]{2,1,0:T(8,128)(2,1)S(1)}, bf16[1,2048,256]{2,1,0:T(8,128)(2,1)}, u32[]{:S(2)}) copy-start(bf16[1,2048,256]{2,1,0:T(8,128)(2,1)} %param.14) | copy-start | bytes 3145732
  18.6 0.7 copy-start.2
  19.2 23.7 %all-to-all-start = ((bf16[64,8,256]{2,1,0:T(8,128)(2,1)}), bf16[64,8,256]{2,1,0:T(8,128)(2,1)S(1)}, u32[]{:S(2)}, u32[]{:S(2)}) async-start(bf16[64,8,256]{2,1,0:T(8,128)(2,1)} %bitcast.5), calls=%async_computation | async-start | bytes 524288 | tf_op jit(solution)/shard_map/all_to_all | solution.py:356
  29.7 48.6 %collective-permute-start = (bf16[2048,256]{1,0:T(8,128)(2,1)}, bf16[2048,256]{1,0:T(8,128)(2,1)}, u32[]{:S(2)}, u32[]{:S(2)}) collective-permute-start(bf16[2048,256]{1,0:T(8,128)(2,1)} %bitcast.22), channel_id=1, source_target_pairs={{0,1},{1,0},{2,3},{3,2},{4,5},{5,4},{6,7},{7,6},{8,9},{9,8},{10,11... | collective-permute-start | bytes 3145736 | tf_op jit(solution)/shard_map/ppermute | solution.py:365
  32.3 46.1 %collective-permute-start.1 = (bf16[2048,256]{1,0:T(8,128)(2,1)}, bf16[2048,256]{1,0:T(8,128)(2,1)}, u32[]{:S(2)}, u32[]{:S(2)}) collective-permute-start(bf16[2048,256]{1,0:T(8,128)(2,1)} %bitcast.24), channel_id=1, source_target_pairs={{0,1},{1,0},{2,3},{3,2},{4,5},{5,4},{6,7},{7,6},{8,9},{9,8},{10,11... | collective-permute-start | bytes 3145736 | tf_op jit(solution)/shard_map/ppermute | solution.py:365
  43.9 0.6 copy-start.6
  44.5 33.8 %all-to-all-start.1 = ((bf16[8,96,256]{2,1,0:T(8,128)(2,1)}), bf16[8,96,256]{2,1,0:T(8,128)(2,1)S(1)}, u32[]{:S(2)}, u32[]{:S(2)}) async-start(bf16[8,96,256]{2,1,0:T(8,128)(2,1)} %get-tuple-element.13), calls=%async_computation.1 | async-start | bytes 786432 | tf_op jit(solution)/shard_map/all_to_all | solution.py:356
  83.0 0.7 copy-start.4
  83.7 14.5 %copy-start.5 = (bf16[120,512]{1,0:T(8,128)(2,1)S(1)}, bf16[120,512]{1,0:T(8,128)(2,1)}, u32[]{:S(2)}) copy-start(bf16[120,512]{1,0:T(8,128)(2,1)} %copy-done.4) | copy-start | bytes 368644
  83.7 59.1 %all-to-all-start.2 = ((bf16[8,200,512]{2,1,0:T(8,128)(2,1)}), bf16[8,200,512]{2,1,0:T(8,128)(2,1)S(1)}, u32[]{:S(2)}, u32[]{:S(2)}) async-start(bf16[8,200,512]{2,1,0:T(8,128)(2,1)} %get-tuple-element.15), calls=%async_computation.2 | async-start | bytes 3276800 | tf_op jit(solution)/shard_map/all_to_all | solution.py:356
  88.9 53.9 %collective-permute-start.2 = (bf16[4096,128]{1,0:T(8,128)(2,1)}, bf16[4096,128]{1,0:T(8,128)(2,1)}, u32[]{:S(2)}, u32[]{:S(2)}) collective-permute-start(bf16[4096,128]{1,0:T(8,128)(2,1)} %bitcast.11.refs_3_), channel_id=1, source_target_pairs={{0,1},{1,0},{2,3},{3,2},{4,5},{5,4},{6,7},{7,6},{8,9},{9,8},{10,11... | collective-permute-start | bytes 3145736 | tf_op jit(solution)/shard_map/ppermute | solution.py:365
  142.8 20.8 %copy-start.3 = (f32[256,8]{1,0:T(8,128)S(1)}, f32[256,8]{1,0:T(8,128)}, u32[]{:S(2)}) copy-start(f32[256,8]{1,0:T(8,128)} %copy-done.2) | copy-start | bytes 24580

commit v4 on v3

--- a/solution.py
+++ b/solution.py
@@ -26,26 +26,8 @@
     return pl.BlockSpec(memory_space=memory_space)
 
 
-def prepare_kernel(tok_ref, gain_ref, out_ref):
-    rows = tok_ref.shape[0]
-    out_ref[0:rows, :] = tok_ref[...]
-    gain = gain_ref[...]
-    piece0 = gain.astype(jnp.bfloat16).astype(jnp.float32)
-    piece1 = (gain - piece0).astype(jnp.bfloat16).astype(jnp.float32)
-    piece2 = gain - piece0 - piece1
-    empty = jnp.zeros((EXTRA - 3, gain.shape[1]), jnp.float32)
-    lines = jnp.concatenate([piece0, piece1, piece2, empty], axis=0)
-    out_ref[rows : rows + EXTRA, :] = lines.astype(jnp.bfloat16)
-
-
-def prepare(tokens, gain):
-    rows, width = tokens.shape
-    return pl.pallas_call(
-        prepare_kernel,
-        out_shape=jax.ShapeDtypeStruct((rows + EXTRA, width), jnp.bfloat16),
-        compiler_params=params(4),
-        name="prepare",
-    )(tokens, gain)
+def blocked(shape):
+    return pl.BlockSpec(shape, lambda: (0,) * len(shape))
 
 
 def dispatch_kernel(core_ref, tok_ref, ids_ref, weights_ref, out_ref, cols_ref, *, capacity):
@@ -74,7 +56,7 @@
     width = tok_ref.shape[2]
     for c in range(CORES):
         out_ref[:, c * width : (c + 1) * width] = jnp.dot(
-            chosen, tok_ref[c, 0:rows, :], preferred_element_type=jnp.float32
+            chosen, tok_ref[c], preferred_element_type=jnp.float32
         ).astype(jnp.bfloat16)
     lines = jnp.concatenate(
         [
@@ -98,9 +80,10 @@
     return pl.pallas_call(
         body,
         in_specs=[whole(pltpu.SMEM), whole(), whole(), whole()],
+        out_specs=(blocked((experts * PAD, CORES * width)), blocked((rows, 8))),
         out_shape=(
-            jax.ShapeDtypeStruct((experts * PAD, CORES * width), jnp.bfloat16),
-            jax.ShapeDtypeStruct((rows, 8), jnp.float32),
+            pltpu.HBM((experts * PAD, CORES * width), jnp.bfloat16),
+            pltpu.HBM((rows, 8), jnp.float32),
         ),
         compiler_params=params(8),
         name="dispatch",
@@ -116,10 +99,17 @@
     return jnp.where(same, 1.0, 0.0).astype(jnp.bfloat16)
 
 
-def arrange_kernel(arrived_ref, tok_ref, first_ref, second_ref, *, half):
+def pieces_of(gain):
+    piece0 = gain.astype(jnp.bfloat16).astype(jnp.float32)
+    piece1 = (gain - piece0).astype(jnp.bfloat16).astype(jnp.float32)
+    piece2 = gain - piece0 - piece1
+    empty = jnp.zeros((EXTRA - 3, gain.shape[1]), jnp.float32)
+    return jnp.concatenate([piece0, piece1, piece2, empty], axis=0).astype(jnp.bfloat16)
+
+
+def arrange_kernel(core_ref, arrived_ref, gain0_ref, gain1_ref, first_ref, second_ref, *, half):
     step = GROUP * half
-    width = tok_ref.shape[2]
-    first = tok_ref.shape[1] - EXTRA
+    width = gain0_ref.shape[1]
     place = packed_place((step, GROUP * PAD), 1, half)
     groups = arrived_ref.shape[0] // (GROUP * PAD)
     for g in range(groups):
@@ -135,32 +125,35 @@
             for j in range(second_ref.shape[0]):
                 second_ref[j, begin : begin + step, :] = rows
     last = (groups - GATHERED) * step
-    for j in range(second_ref.shape[0]):
-        for c in range(CORES):
-            second_ref[j, last : last + EXTRA, c * width : (c + 1) * width] = tok_ref[
-                c, first : first + EXTRA, :
-            ]
-
-
-def arrange(arrived, tokens, chips, half):
+    own = pieces_of(gain0_ref[...])
+    other = pieces_of(gain1_ref[...])
+    for c in range(CORES):
+
+        @pl.when(core_ref[0] == c)
+        def _():
+            for j in range(second_ref.shape[0]):
+                second_ref[j, last : last + EXTRA, c * width : (c + 1) * width] = own
+                second_ref[j, last : last + EXTRA, (1 - c) * width : (2 - c) * width] = other
+
+
+def arrange(core, arrived, gain0, gain1, chips, half):
     groups = arrived.shape[0] // (GROUP * PAD)
     width = arrived.shape[1]
     step = GROUP * half
+    first = (GATHERED * step, width)
+    second = (chips, (groups - GATHERED) * step + EXTRA, width)
 
     def body(*refs):
         arrange_kernel(*refs, half=half)
 
     return pl.pallas_call(
         body,
-        out_shape=(
-            jax.ShapeDtypeStruct((GATHERED * step, width), jnp.bfloat16),
-            jax.ShapeDtypeStruct(
-                (chips, (groups - GATHERED) * step + EXTRA, width), jnp.bfloat16
-            ),
-        ),
+        in_specs=[whole(pltpu.SMEM), whole(), whole(), whole()],
+        out_specs=(blocked(first), blocked(second)),
+        out_shape=(pltpu.HBM(first, jnp.bfloat16), pltpu.HBM(second, jnp.bfloat16)),
         compiler_params=params(8),
         name="arrange",
-    )(arrived, tokens)
+    )(core, arrived, gain0, gain1)
 
 
 def hidden_kernel(
@@ -173,6 +166,7 @@
     up1_ref,
     out0_ref,
     out1_ref,
+    out2_ref,
     normed_ref,
     hidden_ref,
 ):
@@ -212,20 +206,25 @@
 
     rows0 = out0_ref.shape[0]
     out0_ref[...] = hidden_ref[0:rows0, :]
+    out1_ref[...] = hidden_ref[rows0 : 2 * rows0, :]
     for j in range(chips):
-        out1_ref[j] = hidden_ref[rows0:, :]
+        out2_ref[j] = hidden_ref[2 * rows0 :, :]
 
 
 def hidden_of(core, first, second, gate0, up0, gate1, up1):
     chips, _, wide = first.shape
     rows = first.shape[1] + second.shape[1] - EXTRA
     units = gate0.shape[1]
+    taken = (TAKEN, CORES * units)
+    sent = (chips, rows - 2 * TAKEN, CORES * units)
     return pl.pallas_call(
         hidden_kernel,
         in_specs=[whole(pltpu.SMEM)] + [whole()] * 6,
+        out_specs=(blocked(taken), blocked(taken), blocked(sent)),
         out_shape=(
-            jax.ShapeDtypeStruct((TAKEN, CORES * units), jnp.bfloat16),
-            jax.ShapeDtypeStruct((chips, rows - TAKEN, CORES * units), jnp.bfloat16),
+            pltpu.HBM(taken, jnp.bfloat16),
+            pltpu.HBM(taken, jnp.bfloat16),
+            pltpu.HBM(sent, jnp.bfloat16),
         ),
         scratch_shapes=[
             pltpu.VMEM((rows, chips * wide), jnp.bfloat16),
@@ -237,7 +236,17 @@
 
 
 def down_kernel(
-    core_ref, hidden0_ref, hidden1_ref, down0_ref, down1_ref, out_ref, down_ref, result_ref, *, half
+    core_ref,
+    hidden0_ref,
+    hidden1_ref,
+    hidden2_ref,
+    down0_ref,
+    down1_ref,
+    out_ref,
+    down_ref,
+    result_ref,
+    *,
+    half,
 ):
     chips, rows0, units = hidden0_ref.shape
     width = down0_ref.shape[1]
@@ -248,7 +257,7 @@
             down_ref[:, c * width : (c + 1) * width] = down0_ref[...]
             down_ref[:, (1 - c) * width : (2 - c) * width] = down1_ref[...]
 
-    for at, ref in ((0, hidden0_ref), (rows0, hidden1_ref)):
+    for at, ref in ((0, hidden0_ref), (rows0, hidden1_ref), (2 * rows0, hidden2_ref)):
         rows = ref.shape[1]
         total = jnp.zeros((rows, CORES * width), jnp.float32)
         for j in range(chips):
@@ -266,8 +275,8 @@
         ).astype(jnp.bfloat16)
 
 
-def down_of(core, hidden0, hidden1, down0, down1, half):
-    rows = hidden0.shape[1] + hidden1.shape[1]
+def down_of(core, hidden0, hidden1, hidden2, down0, down1, half):
+    rows = hidden0.shape[1] + hidden1.shape[1] + hidden2.shape[1]
     full, width = down0.shape
 
     def body(*refs):
@@ -275,7 +284,7 @@
 
     return pl.pallas_call(
         body,
-        in_specs=[whole(pltpu.SMEM)] + [whole()] * 4,
+        in_specs=[whole(pltpu.SMEM)] + [whole()] * 5,
         out_shape=jax.ShapeDtypeStruct((rows // half * PAD, CORES * width), jnp.bfloat16),
         scratch_shapes=[
             pltpu.VMEM((full, CORES * width), jnp.bfloat16),
@@ -283,70 +292,78 @@
         ],
         compiler_params=params(24),
         name="down",
-    )(core, hidden0, hidden1, down0, down1)
+    )(core, hidden0, hidden1, hidden2, down0, down1)
 
 
 def combine_kernel(returned_ref, cols_ref, mixed_ref):
-    _, rows, width = mixed_ref.shape
+    rows, wide = mixed_ref.shape
     slots = returned_ref.shape[0]
     cols = cols_ref[...]
     targets = cols[:, 0:2].astype(jnp.int32)
     slot_index = lax.broadcasted_iota(jnp.int32, (rows, slots), 1)
     returned = returned_ref[...]
-    mixed = jnp.zeros((rows, CORES * width), jnp.float32)
+    mixed = jnp.zeros((rows, wide), jnp.float32)
     for k in range(2):
         chosen = jnp.where(slot_index == targets[:, k : k + 1], 1.0, 0.0).astype(jnp.bfloat16)
         picked = jnp.dot(chosen, returned, preferred_element_type=jnp.float32)
         mixed = mixed + picked * cols[:, 2 + k : 3 + k]
-    for c in range(CORES):
-        mixed_ref[c] = mixed[:, c * width : (c + 1) * width]
+    mixed_ref[...] = mixed
 
 
 def combine(returned, cols):
-    wide = returned.shape[1]
-    rows = cols.shape[0]
     return pl.pallas_call(
         combine_kernel,
-        out_shape=jax.ShapeDtypeStruct((CORES, rows, wide // CORES), jnp.float32),
+        out_shape=jax.ShapeDtypeStruct((cols.shape[0], returned.shape[1]), jnp.float32),
         compiler_params=params(8),
         name="combine",
     )(returned, cols)
 
 
-def sums_kernel(mixed_ref, sums_ref):
-    _, rows, _ = mixed_ref.shape
-    mixed = mixed_ref[0] + mixed_ref[1]
+def sums_kernel(core_ref, parts_ref, mixed_ref, sums_ref):
+    rows, width = mixed_ref.shape
+    for c in range(CORES):
+
+        @pl.when(core_ref[0] == c)
+        def _():
+            own = slice(c * width, (c + 1) * width)
+            mixed_ref[...] = parts_ref[0, :, own] + parts_ref[1, :, own]
+
+    mixed = mixed_ref[...]
     sums = jnp.sum(mixed * mixed, axis=1, keepdims=True)
     line = jnp.transpose(jnp.broadcast_to(sums, (rows, 128)))[0:1, :]
     for j in range(sums_ref.shape[0]):
         sums_ref[j] = line
 
 
-def sums_of(mixed, peers):
+def sums_of(core, parts, peers):
+    _, rows, wide = parts.shape
     return pl.pallas_call(
         sums_kernel,
-        out_shape=jax.ShapeDtypeStruct((peers, 1, mixed.shape[1]), jnp.float32),
+        in_specs=[whole(pltpu.SMEM), whole()],
+        out_shape=(
+            jax.ShapeDtypeStruct((rows, wide // CORES), jnp.float32),
+            jax.ShapeDtypeStruct((peers, 1, rows), jnp.float32),
+        ),
         compiler_params=params(4),
         name="sums",
-    )(mixed)
+    )(core, parts)
 
 
 def final_kernel(mixed_ref, sums_ref, gain_ref, out_ref):
-    rows, width = out_ref.shape
+    rows, width = mixed_ref.shape
     peers = sums_ref.shape[0]
     total = sums_ref[0]
     for j in range(1, peers):
         total = total + sums_ref[j]
     scale = lax.rsqrt(total / (peers * width) + epsilon)
     column = jnp.transpose(jnp.broadcast_to(scale, (8, rows)))[:, 0:1]
-    mixed = mixed_ref[0] + mixed_ref[1]
-    out_ref[...] = (mixed * column * gain_ref[...]).astype(jnp.bfloat16)
+    out_ref[...] = (mixed_ref[...] * column * gain_ref[...]).astype(jnp.bfloat16)
 
 
 def final(mixed, sums, gain):
     return pl.pallas_call(
         final_kernel,
-        out_shape=jax.ShapeDtypeStruct(mixed.shape[1:], jnp.bfloat16),
+        out_shape=jax.ShapeDtypeStruct(mixed.shape, jnp.bfloat16),
         compiler_params=params(4),
         name="final",
     )(mixed, sums, gain)
@@ -377,26 +394,29 @@
     core = lax.axis_index("c").astype(jnp.int32).reshape(1)
     gate0, up0 = gate_weight[0], up_weight[0]
     down0 = down_weight[0]
-    gate1, up1, down1 = in_hbm(swap(gate0)), in_hbm(swap(up0)), in_hbm(swap(down0))
-    both = lax.all_gather(prepare(in_hbm(tokens), in_hbm(pre_gain[None, :])), "c", axis=0)
+    gain0 = pre_gain[None, :]
+    gate1, up1, down1 = in_hbm(swap(gate0)), in_hbm(swap(up0)), swap(down0)
+    gain1 = in_hbm(swap(gain0))
     outgoing, cols = dispatch(
         core,
-        both,
+        lax.all_gather(tokens, "c", axis=0),
         in_hbm(jnp.transpose(expert_ids)),
         in_hbm(jnp.transpose(route_weights)),
         ep_count,
         capacity,
     )
-    arrived = blocks_exchange(outgoing)
-    first, second = arrange(arrived, both, chips, half)
+    arrived, down1 = lax.optimization_barrier((blocks_exchange(outgoing), down1))
+    first, second = arrange(core, arrived, in_hbm(gain0), gain1, chips, half)
     second = exchange(second, "x")
     first = lax.all_gather(first, "x", axis=0)
-    hidden0, hidden1 = hidden_of(core, first, second, gate0, up0, gate1, up1)
-    hidden1 = exchange(hidden1, "x")
+    hidden0, hidden1, hidden2 = hidden_of(core, first, second, gate0, up0, gate1, up1)
+    hidden2 = exchange(hidden2, "x")
     hidden0 = lax.all_gather(hidden0, "x", axis=0)
-    returned = blocks_exchange(down_of(core, hidden0, hidden1, down0, down1, half))
-    mixed = exchange(combine(returned, cols), "c")
-    sums = exchange(sums_of(mixed, chips * CORES), ("x", "c"))
+    hidden1 = lax.all_gather(hidden1, "x", axis=0)
+    result = down_of(core, hidden0, hidden1, hidden2, down0, in_hbm(down1), half)
+    mixed = lax.all_gather(combine(blocks_exchange(result), cols), "c", axis=0)
+    mixed, sums = sums_of(core, mixed, chips * CORES)
+    sums = exchange(sums, ("x", "c"))
     return final(mixed, sums, in_hbm(post_gain[None, :]))
 
 

time: 192 us -> 201 us (1.047)
  starting transfers between devices: 35.9 us -> 45.3 us
  waiting for transfers between devices: 8.72 us -> 6.17 us
    all_gather x1 -> x3, blocking collectives: 15.7 us -> 43.4 us  [the longest x1 21.6 us: on_device(): hidden1 = lax.all_gather(hidden1, 'x', axis=0)]
    all_gather x1, blocking collectives: 44.6 us -> 29.8 us  [on_device(): hidden0 = lax.all_gather(hidden0, 'x', axis=0)]
    all_to_all x3 -> x2, blocking collectives: 43.7 us -> 33 us  [exchange(): return lax.all_to_all(value, axis, split_axis=0, concat_axis=0, tiled=True)]
    ppermute x3 -> x4, starting transfers between devices: 13.7 us -> 22.9 us  [swap(): return lax.ppermute(value, 'c', [(0, 1), (1, 0)])]
    all_to_all x3, waiting for transfers between devices: 8.71 us -> 6.16 us  [exchange(): return lax.all_to_all(value, axis, split_axis=0, concat_axis=0, tiled=True)]
    pallas_call x6 -> x5, Pallas kernels: 7.08 us -> 6.97 us  [the longest x1 2.78 us: down_of(): pl.pallas_call(body, in_specs=[whole(pltpu.SMEM)] + [whole()] * 5, out_sh...]
  transfers between devices with their start and end apart: 6 -> 7, of which waited for: 1 -> 1; matrix products, arithmetic and copies ran while one was open for 0% -> 0% of each run, Pallas kernels for 0% -> 2%
where the time goes in v4:
time: 201 us; the launch traced here: 200 us
  blocking collectives  133 us (66%)
  starting transfers between devices  45.3 us (23%)
  Pallas kernels  13.1 us (7%)
  waiting for transfers between devices  6.17 us (3%)
    all_to_all x2, blocking collectives, exchange(): return lax.all_to_all(value, axis, split_axis=0, concat_axis=0, tiled=True)  33 us
    all_gather x1, blocking collectives, on_device(): hidden0 = lax.all_gather(hidden0, 'x', axis=0)  29.8 us
    all_gather x1, blocking collectives, on_device(): first = lax.all_gather(first, 'x', axis=0)  27.2 us
    ppermute x4, starting transfers between devices, swap(): return lax.ppermute(value, 'c', [(0, 1), (1, 0)])  22.9 us
    all_to_all x3, starting transfers between devices, exchange(): return lax.all_to_all(value, axis, split_axis=0, concat_axis=0, tiled=True)  22.3 us
    all_gather x1, blocking collectives, on_device(): hidden1 = lax.all_gather(hidden1, 'x', axis=0)  21.6 us
    all_gather x1, blocking collectives, on_device(): mixed = lax.all_gather(combine(blocks_exchange(result), cols), 'c', axis=0)  19.2 us
    all_to_all x3, waiting for transfers between devices, exchange(): return lax.all_to_all(value, axis, split_axis=0, concat_axis=0, tiled=True)  6.16 us
  transfers between devices with their start and end apart: 7, of which 1 were waited for; matrix products, arithmetic and copies ran while one was open for 0% of the time, Pallas kernels for 2%

profile of v4, /device:TPU:1, one launch (start us, length us, event | category | flops | bytes accessed | tf_op | source)
XLA Modules:
  0.0 199.9 jit_solution(56384275670105839)
XLA Ops:
  0.0 16.0 %collective-permute-start = (bf16[4096,128]{1,0:T(8,128)(2,1)}, bf16[4096,128]{1,0:T(8,128)(2,1)S(1)}, u32[]{:S(2)}, u32[]{:S(2)}) collective-permute-start(bf16[4096,128]{1,0:T(8,128)(2,1)} %bitcast.21), channel_id=1, source_target_pairs={{0,1},{1,0},{2,3},{3,2},{4,5},{5,4},{6,7},{7,6},{8,9},{9,8},{10,11... | collective-permute-start | bytes 3145736 | tf_op jit(solution)/shard_map/ppermute | solution.py:382
  16.0 2.6 %all-gather = bf16[512,128]{1,0:T(8,128)(2,1)S(1)} all-gather(bf16[256,128]{1,0:T(8,128)(2,1)} %param.8), channel_id=2, replica_groups=mesh['ep'=64,'x'=8,'c'=2] {'c'}, dimensions={0}, use_global_device_ids=true | all-gather | bytes 196608 | tf_op jit(solution)/shard_map/all_gather | solution.py:402
  18.6 1.9 dispatch.1
  20.5 10.5 %all-to-all-start = ((bf16[64,8,256]{2,1,0:T(8,128)(2,1)}), bf16[64,8,256]{2,1,0:T(8,128)(2,1)S(1)}, u32[]{:S(2)}, u32[]{:S(2)}) async-start(bf16[64,8,256]{2,1,0:T(8,128)(2,1)} %bitcast.31), calls=%async_computation | async-start | bytes 524288 | tf_op jit(solution)/shard_map/all_to_all | solution.py:373
  31.0 2.6 %collective-permute-start.2 = (bf16[2048,256]{1,0:T(8,128)(2,1)}, bf16[2048,256]{1,0:T(8,128)(2,1)}, u32[]{:S(2)}, u32[]{:S(2)}) collective-permute-start(bf16[2048,256]{1,0:T(8,128)(2,1)} %bitcast.26), channel_id=1, source_target_pairs={{0,1},{1,0},{2,3},{3,2},{4,5},{5,4},{6,7},{7,6},{8,9},{9,8},{10,11... | collective-permute-start | bytes 3145736 | tf_op jit(solution)/shard_map/ppermute | solution.py:382
  33.6 0.0 copy-start.7
  33.6 1.9 collective-permute-start.3
  35.5 0.0 copy-done.7
  35.5 2.4 %collective-permute-start.1 = (f32[1,128]{1,0:T(1,128)S(1)}, f32[1,128]{1,0:T(1,128)S(1)}, u32[]{:S(2)}, u32[]{:S(2)}) collective-permute-start(f32[1,128]{1,0:T(1,128)S(1)} %bitcast.35), channel_id=1, source_target_pairs={{0,1},{1,0},{2,3},{3,2},{4,5},{5,4},{6,7},{7,6},{8,9},{9,8},{10,11... | collective-permute-start | bytes 1544 | tf_op jit(solution)/shard_map/ppermute | solution.py:382
  37.9 6.2 %all-to-all-done = bf16[64,8,256]{2,1,0:T(8,128)(2,1)S(1)} async-done(((bf16[64,8,256]{2,1,0:T(8,128)(2,1)}), bf16[64,8,256]{2,1,0:T(8,128)(2,1)S(1)}, u32[]{:S(2)}, u32[]{:S(2)}) %all-to-all-start) | async-done | bytes 262176 | tf_op jit(solution)/shard_map/all_to_all | solution.py:373
  44.1 0.0 collective-permute-done.refs_5_
  44.1 0.0 collective-permute-done.1.refs_3_
  44.1 0.6 copy-done.8
  44.7 2.1 %arrange.1 = (bf16[240,256]{1,0:T(8,128)(2,1)}, bf16[8,96,256]{2,1,0:T(8,128)(2,1)}) custom-call(s32[1]{0:T(128)} %bitcast.refs_0_.core_ref, bf16[512,256]{1,0:T(8,128)(2,1)S(1)} %bitcast.24, f32[1,128]{1,0:T(1,128)} %bitcast.34, f32[1,128]{1,0:T(1,128)} %copy-done.8), custom_call_target="tpu_custom_call" | custom-call | tf_op jit(solution)/shard_map/arrange/pallas_call | solution.py:149
  46.8 6.5 %all-to-all-start.1 = ((bf16[8,96,256]{2,1,0:T(8,128)(2,1)}), bf16[8,96,256]{2,1,0:T(8,128)(2,1)S(1)}, u32[]{:S(2)}, u32[]{:S(2)}) async-start(bf16[8,96,256]{2,1,0:T(8,128)(2,1)} %get-tuple-element.19), calls=%async_computation.1 | async-start | bytes 786432 | tf_op jit(solution)/shard_map/all_to_all | solution.py:373
  53.3 27.2 %all-gather.1 = bf16[1920,256]{1,0:T(8,128)(2,1)S(1)} all-gather(bf16[240,256]{1,0:T(8,128)(2,1)} %get-tuple-element.18), channel_id=3, replica_groups=mesh['ep'=64,'x'=8,'c'=2] {'x'}, dimensions={0}, use_global_device_ids=true | all-gather | bytes 1105920 | tf_op jit(solution)/shard_map/all_gather | solution.py:411
  80.5 0.0 collective-permute-done.2.gate1_ref
  80.5 0.0 collective-permute-done.3.up1_ref
  80.5 0.0 all-to-all-done.1.second_ref
  80.5 4.3 %hidden.1 = (bf16[120,512]{1,0:T(8,128)(2,1)}, bf16[120,512]{1,0:T(8,128)(2,1)}, bf16[8,80,512]{2,1,0:T(8,128)(2,1)}) custom-call(s32[1]{0:T(128)} %bitcast.refs_0_.core_ref, bf16[8,240,256]{2,1,0:T(8,128)(2,1)S(1)} %bitcast.19, bf16[8,96,256]{2,1,0:T(8,128)(2,1)S(1)} %all-to-all-done.1.second_ref, bf16[2048,256]{1,0:T(8,128)(2,1)S(1)} %bitcast.27, ...), custom_call_target="tpu_custom_call" | custom-call | tf_op jit(solution)/shard_map/hidden/pallas_call | solution.py:220
  84.8 5.4 %all-to-all-start.2 = ((bf16[8,80,512]{2,1,0:T(8,128)(2,1)}), bf16[8,80,512]{2,1,0:T(8,128)(2,1)S(1)}, u32[]{:S(2)}, u32[]{:S(2)}) async-start(bf16[8,80,512]{2,1,0:T(8,128)(2,1)} %get-tuple-element.22), calls=%async_computation.2 | async-start | bytes 1310720 | tf_op jit(solution)/shard_map/all_to_all | solution.py:373
  90.1 29.8 %all-gather.2 = bf16[960,512]{1,0:T(8,128)(2,1)S(1)} all-gather(bf16[120,512]{1,0:T(8,128)(2,1)S(1)} %copy-done.6), channel_id=4, replica_groups=mesh['ep'=64,'x'=8,'c'=2] {'x'}, dimensions={0}, use_global_device_ids=true | all-gather | bytes 1105920 | tf_op jit(solution)/shard_map/all_gather | solution.py:414
  120.0 21.6 %all-gather.3 = bf16[960,512]{1,0:T(8,128)(2,1)S(1)} all-gather(bf16[120,512]{1,0:T(8,128)(2,1)S(1)} %copy-done.5), channel_id=5, replica_groups=mesh['ep'=64,'x'=8,'c'=2] {'x'}, dimensions={0}, use_global_device_ids=true | all-gather | bytes 1105920 | tf_op jit(solution)/shard_map/all_gather | solution.py:415
  141.6 0.0 all-to-all-done.2.refs_3_
  141.6 1.2 copy-done
  142.8 2.8 %down.1 = bf16[512,256]{1,0:T(8,128)(2,1)S(1)} custom-call(s32[1]{0:T(128)} %bitcast.refs_0_.core_ref, bf16[8,120,512]{2,1,0:T(8,128)(2,1)S(1)} %bitcast.17, bf16[8,120,512]{2,1,0:T(8,128)(2,1)S(1)} %bitcast.18, bf16[8,80,512]{2,1,0:T(8,128)(2,1)S(1)} %all-to-all-done.2.refs_3_, bf16[4096,128]{1,0:T(8,128)(2,1)S(1)} %bitcast.22, bf16[4096,128]{1,0:T(8,128)(2,1)} %copy-done.4), custom_call_target="tpu_custom_call" | custom-call | tf_op jit(solution)/shard_map/down/pallas_call | solution.py:285
  145.6 19.6 %all_to_all.25 = bf16[64,8,256]{2,1,0:T(8,128)(2,1)S(1)} all-to-all(bf16[64,8,256]{2,1,0:T(8,128)(2,1)S(1)} %bitcast.23), channel_id=1, replica_groups=mesh['ep'=64,'x'=8,'c'=2] {'ep'}, dimensions={0} | all-to-all | bytes 524288 | tf_op jit(solution)/shard_map/all_to_all | solution.py:373
  165.2 0.4 combine.1
  165.5 19.2 %all-gather.4 = f32[512,256]{1,0:T(8,128)S(1)} all-gather(f32[256,256]{1,0:T(8,128)S(1)} %combine.1), channel_id=6, replica_groups=mesh['ep'=64,'x'=8,'c'=2] {'c'}, dimensions={0}, use_global_device_ids=true | all-gather | bytes 786432 | tf_op jit(solution)/shard_map/all_gather | solution.py:417
  184.8 0.2 sums.1
  184.9 13.4 %all_to_all.26.sums_ref = f32[16,1,256]{2,1,0:T(1,128)S(1)} all-to-all(f32[16,1,256]{2,1,0:T(1,128)S(1)} %get-tuple-element.26), channel_id=1, replica_groups=mesh['ep'=64,'x'=8,'c'=2] {'x','c'}, dimensions={0} | all-to-all | bytes 32768 | tf_op jit(solution)/shard_map/all_to_all | solution.py:373
  198.3 1.6 final.1
  (14 shorter events, 0.0 us)
Async XLA Ops:
  0.0 44.1 %collective-permute-start = (bf16[4096,128]{1,0:T(8,128)(2,1)}, bf16[4096,128]{1,0:T(8,128)(2,1)S(1)}, u32[]{:S(2)}, u32[]{:S(2)}) collective-permute-start(bf16[4096,128]{1,0:T(8,128)(2,1)} %bitcast.21), channel_id=1, source_target_pairs={{0,1},{1,0},{2,3},{3,2},{4,5},{5,4},{6,7},{7,6},{8,9},{9,8},{10,11... | collective-permute-start | bytes 3145736 | tf_op jit(solution)/shard_map/ppermute | solution.py:382
  20.5 23.6 %all-to-all-start = ((bf16[64,8,256]{2,1,0:T(8,128)(2,1)}), bf16[64,8,256]{2,1,0:T(8,128)(2,1)S(1)}, u32[]{:S(2)}, u32[]{:S(2)}) async-start(bf16[64,8,256]{2,1,0:T(8,128)(2,1)} %bitcast.31), calls=%async_computation | async-start | bytes 524288 | tf_op jit(solution)/shard_map/all_to_all | solution.py:373
  31.0 49.5 %collective-permute-start.2 = (bf16[2048,256]{1,0:T(8,128)(2,1)}, bf16[2048,256]{1,0:T(8,128)(2,1)}, u32[]{:S(2)}, u32[]{:S(2)}) collective-permute-start(bf16[2048,256]{1,0:T(8,128)(2,1)} %bitcast.26), channel_id=1, source_target_pairs={{0,1},{1,0},{2,3},{3,2},{4,5},{5,4},{6,7},{7,6},{8,9},{9,8},{10,11... | collective-permute-start | bytes 3145736 | tf_op jit(solution)/shard_map/ppermute | solution.py:382
  33.6 1.9 copy-start.7
  33.6 46.9 %collective-permute-start.3 = (bf16[2048,256]{1,0:T(8,128)(2,1)}, bf16[2048,256]{1,0:T(8,128)(2,1)}, u32[]{:S(2)}, u32[]{:S(2)}) collective-permute-start(bf16[2048,256]{1,0:T(8,128)(2,1)} %bitcast.28), channel_id=1, source_target_pairs={{0,1},{1,0},{2,3},{3,2},{4,5},{5,4},{6,7},{7,6},{8,9},{9,8},{10,11... | collective-permute-start | bytes 3145736 | tf_op jit(solution)/shard_map/ppermute | solution.py:382
  35.5 8.6 %collective-permute-start.1 = (f32[1,128]{1,0:T(1,128)S(1)}, f32[1,128]{1,0:T(1,128)S(1)}, u32[]{:S(2)}, u32[]{:S(2)}) collective-permute-start(f32[1,128]{1,0:T(1,128)S(1)} %bitcast.35), channel_id=1, source_target_pairs={{0,1},{1,0},{2,3},{3,2},{4,5},{5,4},{6,7},{7,6},{8,9},{9,8},{10,11... | collective-permute-start | bytes 1544 | tf_op jit(solution)/shard_map/ppermute | solution.py:382
  44.1 2.7 %copy-start.4 = (bf16[4096,128]{1,0:T(8,128)(2,1)}, bf16[4096,128]{1,0:T(8,128)(2,1)S(1)}, u32[]{:S(2)}) copy-start(bf16[4096,128]{1,0:T(8,128)(2,1)S(1)} %collective-permute-done.refs_5_) | copy-start | bytes 3145732
  44.1 36.4 %copy-start.1 = (bf16[1,2048,256]{2,1,0:T(8,128)(2,1)S(1)}, bf16[1,2048,256]{2,1,0:T(8,128)(2,1)}, u32[]{:S(2)}) copy-start(bf16[1,2048,256]{2,1,0:T(8,128)(2,1)} %param.13) | copy-start | bytes 3145732
  44.1 36.4 %copy-start.2 = (bf16[1,2048,256]{2,1,0:T(8,128)(2,1)S(1)}, bf16[1,2048,256]{2,1,0:T(8,128)(2,1)}, u32[]{:S(2)}) copy-start(bf16[1,2048,256]{2,1,0:T(8,128)(2,1)} %param.14) | copy-start | bytes 3145732
  44.1 0.6 copy-start.8
  46.8 33.7 %all-to-all-start.1 = ((bf16[8,96,256]{2,1,0:T(8,128)(2,1)}), bf16[8,96,256]{2,1,0:T(8,128)(2,1)S(1)}, u32[]{:S(2)}, u32[]{:S(2)}) async-start(bf16[8,96,256]{2,1,0:T(8,128)(2,1)} %get-tuple-element.19), calls=%async_computation.1 | async-start | bytes 786432 | tf_op jit(solution)/shard_map/all_to_all | solution.py:373
  84.8 5.4 %copy-start.6 = (bf16[120,512]{1,0:T(8,128)(2,1)S(1)}, bf16[120,512]{1,0:T(8,128)(2,1)}, u32[]{:S(2)}) copy-start(bf16[120,512]{1,0:T(8,128)(2,1)} %get-tuple-element.20) | copy-start | bytes 368644
  84.8 56.8 %all-to-all-start.2 = ((bf16[8,80,512]{2,1,0:T(8,128)(2,1)}), bf16[8,80,512]{2,1,0:T(8,128)(2,1)S(1)}, u32[]{:S(2)}, u32[]{:S(2)}) async-start(bf16[8,80,512]{2,1,0:T(8,128)(2,1)} %get-tuple-element.22), calls=%async_computation.2 | async-start | bytes 1310720 | tf_op jit(solution)/shard_map/all_to_all | solution.py:373
  90.1 29.8 %copy-start.5 = (bf16[120,512]{1,0:T(8,128)(2,1)S(1)}, bf16[120,512]{1,0:T(8,128)(2,1)}, u32[]{:S(2)}) copy-start(bf16[120,512]{1,0:T(8,128)(2,1)} %get-tuple-element.21) | copy-start | bytes 368644
  141.6 1.2 copy-start
  145.6 19.6 %copy-start.3 = (f32[256,8]{1,0:T(8,128)S(1)}, f32[256,8]{1,0:T(8,128)}, u32[]{:S(2)}) copy-start(f32[256,8]{1,0:T(8,128)} %get-tuple-element.24.cols_ref) | copy-start | bytes 24580

commit v5 on v3

v5 whole, which is shorter than its diff:
```python
import jax
import jax.numpy as jnp
from jax import lax
from jax.experimental import pallas as pl
from jax.experimental.pallas import tpu as pltpu
from jax.sharding import Mesh, PartitionSpec as P

epsilon = 1e-06
CORES = 2
PAD = 8
EXTRA = 16
GROUP = 16


def params(mebibytes):
    return pltpu.CompilerParams(vmem_limit_bytes=mebibytes << 20)


def in_hbm(value):
    return pltpu.with_memory_space_constraint(value, pltpu.HBM)


def whole(memory_space=pltpu.VMEM):
    return pl.BlockSpec(memory_space=memory_space)


def prepare_kernel(tok_ref, gain_ref, out_ref):
    rows = tok_ref.shape[0]
    out_ref[0:rows, :] = tok_ref[...]
    gain = gain_ref[...]
    piece0 = gain.astype(jnp.bfloat16).astype(jnp.float32)
    piece1 = (gain - piece0).astype(jnp.bfloat16).astype(jnp.float32)
    piece2 = gain - piece0 - piece1
    empty = jnp.zeros((EXTRA - 3, gain.shape[1]), jnp.float32)
    lines = jnp.concatenate([piece0, piece1, piece2, empty], axis=0)
    out_ref[rows : rows + EXTRA, :] = lines.astype(jnp.bfloat16)


def prepare(tokens, gain):
    rows, width = tokens.shape
    return pl.pallas_call(
        prepare_kernel,
        out_shape=jax.ShapeDtypeStruct((rows + EXTRA, width), jnp.bfloat16),
        compiler_params=params(4),
        name="prepare",
    )(tokens, gain)


def dispatch_kernel(place_ref, tok_ref, ids_ref, weights_ref, out_ref, cols_ref, *, capacity):
    rows = ids_ref.shape[1]
    slots = out_ref.shape[0]
    experts = slots // PAD
    ids = ids_ref[...]
    expert_index = lax.broadcasted_iota(jnp.int32, (experts, rows), 0)
    hot0 = jnp.where(expert_index == ids[0:1, :], 1.0, 0.0)
    hot1 = jnp.where(expert_index == ids[1:2, :], 1.0, 0.0)
    earlier = lax.broadcasted_iota(jnp.int32, (rows, rows), 0) < lax.broadcasted_iota(
        jnp.int32, (rows, rows), 1
    )
    earlier = jnp.where(earlier, 1.0, 0.0).astype(jnp.bfloat16)
    counts = jnp.dot((hot0 + hot1).astype(jnp.bfloat16), earlier, preferred_element_type=jnp.float32)
    half = capacity // CORES
    targets = []
    for k, hot in enumerate((hot0, hot1)):
        slot = jnp.sum(hot * counts, axis=0, keepdims=True).astype(jnp.int32)
        slot = slot - place_ref[1] * half
        mine = jnp.logical_and(slot >= 0, slot < half)
        targets.append(jnp.where(mine, ids[k : k + 1, :] * PAD + slot, -1))
    slot_index = lax.broadcasted_iota(jnp.int32, (slots, rows), 0)
    chosen = jnp.logical_or(slot_index == targets[0], slot_index == targets[1])
    chosen = jnp.where(chosen, 1.0, 0.0).astype(jnp.bfloat16)
    width = tok_ref.shape[2]
    for c in range(CORES):
        out_ref[:, c * width : (c + 1) * width] = jnp.dot(
            chosen, tok_ref[c, 0:rows, :], preferred_element_type=jnp.float32
        ).astype(jnp.bfloat16)
    lines = jnp.concatenate(
        [
            targets[0].astype(jnp.float32),
            targets[1].astype(jnp.float32),
            weights_ref[...],
            jnp.zeros((4, rows), jnp.float32),
        ],
        axis=0,
    )
    cols_ref[...] = jnp.transpose(lines)


def dispatch(place, tokens, ids, weights, experts, capacity):
    rows = ids.shape[1]
    width = tokens.shape[2]

    def body(*refs):
        dispatch_kernel(*refs, capacity=capacity)

    return pl.pallas_call(
        body,
        in_specs=[whole(pltpu.SMEM), whole(), whole(), whole()],
        out_shape=(
            jax.ShapeDtypeStruct((experts * PAD, CORES * width), jnp.bfloat16),
            pltpu.HBM((rows, 8), jnp.float32),
        ),
        compiler_params=params(8),
        name="dispatch",
    )(place, tokens, ids, weights)


def packed_place(shape, slot_axis, capacity):
    padded = lax.broadcasted_iota(jnp.int32, shape, slot_axis)
    packed = lax.broadcasted_iota(jnp.int32, shape, 1 - slot_axis)
    block = padded // PAD
    slot = padded - block * PAD
    same = jnp.logical_and(slot < capacity, packed == block * capacity + slot)
    return jnp.where(same, 1.0, 0.0).astype(jnp.bfloat16)


def arrange_kernel(arrived_ref, tok_ref, out_ref, *, half):
    step = GROUP * half
    width = tok_ref.shape[2]
    first = tok_ref.shape[1] - EXTRA
    chips, rows, _ = out_ref.shape
    place = packed_place((step, GROUP * PAD), 1, half)
    for g in range(arrived_ref.shape[0] // (GROUP * PAD)):
        packed = jnp.dot(
            place,
            arrived_ref[g * GROUP * PAD : (g + 1) * GROUP * PAD, :],
            preferred_element_type=jnp.float32,
        ).astype(jnp.bfloat16)
        for j in range(chips):
            out_ref[j, g * step : (g + 1) * step, :] = packed
    for j in range(chips):
        for c in range(CORES):
            out_ref[j, rows - EXTRA :, c * width : (c + 1) * width] = tok_ref[
                c, first : first + EXTRA, :
            ]


def arrange(arrived, tokens, chips, half):
    blocks = arrived.shape[0] // PAD
    width = arrived.shape[1]

    def body(*refs):
        arrange_kernel(*refs, half=half)

    return pl.pallas_call(
        body,
        out_shape=jax.ShapeDtypeStruct((chips, blocks * half + EXTRA, width), jnp.bfloat16),
        compiler_params=params(8),
        name="arrange",
    )(arrived, tokens)


def hidden_kernel(
    place_ref, feat_ref, gate0_ref, up0_ref, gate1_ref, up1_ref, out_ref, normed_ref
):
    chips, rows, wide = feat_ref.shape
    rows = rows - EXTRA
    full = chips * wide
    units = gate0_ref.shape[1]
    total = jnp.zeros((rows, wide), jnp.float32)
    for j in range(chips):
        part = feat_ref[j, 0:rows, :].astype(jnp.float32)
        total = total + part * part
    scale = lax.rsqrt(jnp.sum(total, axis=1, keepdims=True) / full + epsilon)
    for j in range(chips):
        pieces = feat_ref[j, rows : rows + EXTRA, :].astype(jnp.float32)
        gain = pieces[0:1, :] + pieces[1:2, :] + pieces[2:3, :]
        part = feat_ref[j, 0:rows, :].astype(jnp.float32)
        normed_ref[:, j * wide : (j + 1) * wide] = (part * scale * gain).astype(jnp.bfloat16)

    def hidden_of(gate_ref, up_ref):
        normed = normed_ref[...]
        gate = jnp.dot(normed, gate_ref[...], preferred_element_type=jnp.float32)
        upper = jnp.dot(normed, up_ref[...], preferred_element_type=jnp.float32)
        return (gate / (1.0 + jnp.exp(-gate)) * upper).astype(jnp.bfloat16)

    own = hidden_of(gate0_ref, up0_ref)
    other = hidden_of(gate1_ref, up1_ref)
    for c in range(CORES):

        @pl.when(place_ref[1] == c)
        def _():
            out_ref[:, c * units : (c + 1) * units] = own
            out_ref[:, (1 - c) * units : (2 - c) * units] = other


def hidden_of(place, features, gate0, up0, gate1, up1):
    chips, rows, wide = features.shape
    units = gate0.shape[1]
    return pl.pallas_call(
        hidden_kernel,
        in_specs=[whole(pltpu.SMEM)] + [whole()] * 5,
        out_shape=jax.ShapeDtypeStruct((rows - EXTRA, CORES * units), jnp.bfloat16),
        scratch_shapes=[pltpu.VMEM((rows - EXTRA, chips * wide), jnp.bfloat16)],
        compiler_params=params(24),
        name="hidden",
    )(place, features, gate0, up0, gate1, up1)


def down_kernel(*refs, offsets, half):
    place_ref, *hidden_refs, down0_ref, down1_ref, out_ref, down_ref, result_ref = refs
    rows, units = hidden_refs[0].shape
    width = down0_ref.shape[1]
    for c in range(CORES):

        @pl.when(place_ref[1] == c)
        def _():
            down_ref[:, c * width : (c + 1) * width] = down0_ref[...]
            down_ref[:, (1 - c) * width : (2 - c) * width] = down1_ref[...]

    chips = len(offsets)
    total = jnp.zeros((rows, CORES * width), jnp.float32)
    for offset, ref in zip(offsets, hidden_refs):
        chip = lax.rem(place_ref[0] + (offset + chips), chips)
        begin = pl.multiple_of(chip * units, units)
        total = total + jnp.dot(
            ref[...], down_ref[pl.ds(begin, units), :], preferred_element_type=jnp.float32
        )
    result_ref[...] = total.astype(jnp.bfloat16)
    step = GROUP * half
    place = packed_place((GROUP * PAD, step), 0, half)
    for g in range(out_ref.shape[0] // (GROUP * PAD)):
        out_ref[g * GROUP * PAD : (g + 1) * GROUP * PAD, :] = jnp.dot(
            place, result_ref[g * step : (g + 1) * step, :], preferred_element_type=jnp.float32
        ).astype(jnp.bfloat16)


def down_of(place, hiddens, down0, down1, half):
    offsets = [offset for offset, _ in hiddens]
    arrays = [array for _, array in hiddens]
    rows = arrays[0].shape[0]
    full, width = down0.shape

    def body(*refs):
        down_kernel(*refs, offsets=offsets, half=half)

    return pl.pallas_call(
        body,
        in_specs=[whole(pltpu.SMEM)] + [whole()] * (len(arrays) + 2),
        out_shape=jax.ShapeDtypeStruct((rows // half * PAD, CORES * width), jnp.bfloat16),
        scratch_shapes=[
            pltpu.VMEM((full, CORES * width), jnp.bfloat16),
            pltpu.VMEM((rows, CORES * width), jnp.bfloat16),
        ],
        compiler_params=params(24),
        name="down",
    )(place, *arrays, down0, down1)


def combine_kernel(returned_ref, cols_ref, mixed_ref):
    rows, wide = mixed_ref.shape
    slots = returned_ref.shape[0]
    cols = cols_ref[...]
    targets = cols[:, 0:2].astype(jnp.int32)
    slot_index = lax.broadcasted_iota(jnp.int32, (rows, slots), 1)
    returned = returned_ref[...]
    mixed = jnp.zeros((rows, wide), jnp.float32)
    for k in range(2):
        chosen = jnp.where(slot_index == targets[:, k : k + 1], 1.0, 0.0).astype(jnp.bfloat16)
        picked = jnp.dot(chosen, returned, preferred_element_type=jnp.float32)
        mixed = mixed + picked * cols[:, 2 + k : 3 + k]
    mixed_ref[...] = mixed


def combine(returned, cols):
    return pl.pallas_call(
        combine_kernel,
        out_shape=jax.ShapeDtypeStruct((cols.shape[0], returned.shape[1]), jnp.float32),
        compiler_params=params(8),
        name="combine",
    )(returned, cols)


def sums_kernel(place_ref, parts_ref, mixed_ref, sums_ref):
    rows, width = mixed_ref.shape
    for c in range(CORES):

        @pl.when(place_ref[1] == c)
        def _():
            own = slice(c * width, (c + 1) * width)
            mixed_ref[...] = parts_ref[0, :, own] + parts_ref[1, :, own]

    mixed = mixed_ref[...]
    sums = jnp.sum(mixed * mixed, axis=1, keepdims=True)
    line = jnp.transpose(jnp.broadcast_to(sums, (rows, 128)))[0:1, :]
    for j in range(sums_ref.shape[0]):
        sums_ref[j] = line


def sums_of(place, parts, peers):
    _, rows, wide = parts.shape
    return pl.pallas_call(
        sums_kernel,
        in_specs=[whole(pltpu.SMEM), whole()],
        out_shape=(
            jax.ShapeDtypeStruct((rows, wide // CORES), jnp.float32),
            jax.ShapeDtypeStruct((peers, 1, rows), jnp.float32),
        ),
        compiler_params=params(4),
        name="sums",
    )(place, parts)


def final_kernel(mixed_ref, sums_ref, gain_ref, out_ref):
    rows, width = mixed_ref.shape
    peers = sums_ref.shape[0]
    total = sums_ref[0]
    for j in range(1, peers):
        total = total + sums_ref[j]
    scale = lax.rsqrt(total / (peers * width) + epsilon)
    column = jnp.transpose(jnp.broadcast_to(scale, (8, rows)))[:, 0:1]
    out_ref[...] = (mixed_ref[...] * column * gain_ref[...]).astype(jnp.bfloat16)


def final(mixed, sums, gain):
    return pl.pallas_call(
        final_kernel,
        out_shape=jax.ShapeDtypeStruct(mixed.shape, jnp.bfloat16),
        compiler_params=params(4),
        name="final",
    )(mixed, sums, gain)


def exchange(value, axis):
    return lax.all_to_all(value, axis, split_axis=0, concat_axis=0, tiled=True)


def blocks_exchange(value):
    wide = value.shape[1]
    return exchange(value.reshape(-1, PAD, wide), "ep").reshape(-1, wide)


def swap(value):
    return lax.ppermute(value, "c", [(0, 1), (1, 0)])


def ring(value):
    chips = lax.axis_size("x")
    onward = [(i, (i + 1) % chips) for i in range(chips)]
    backward = [(i, (i - 1) % chips) for i in range(chips)]
    arrays = [(0, value)]
    before, after = value, value
    for step in range(1, chips // 2 + 1):
        before = lax.ppermute(before, "x", onward)
        arrays.append((-step, before))
        if step < chips - step:
            after = lax.ppermute(after, "x", backward)
            arrays.append((step, after))
    return arrays


def on_device(
    tokens, expert_ids, route_weights, pre_gain, post_gain, gate_weight, up_weight, down_weight
):
    tok_rows = tokens.shape[0]
    ep_count = lax.axis_size("ep")
    chips = lax.axis_size("x")
    top_count = expert_ids.shape[1]
    capacity = max(2, tok_rows * top_count * 5 // (4 * ep_count))
    half = capacity // CORES
    place = jnp.stack([lax.axis_index("x"), lax.axis_index("c")]).astype(jnp.int32)
    gate0, up0, down0 = gate_weight[0], up_weight[0], down_weight[0]
    gate1, up1 = in_hbm(swap(gate0)), in_hbm(swap(up0))
    both = lax.all_gather(prepare(in_hbm(tokens), in_hbm(pre_gain[None, :])), "c", axis=0)
    outgoing, cols = dispatch(
        place,
        both,
        in_hbm(jnp.transpose(expert_ids)),
        in_hbm(jnp.transpose(route_weights)),
        ep_count,
        capacity,
    )
    outgoing, later = lax.optimization_barrier((outgoing, down0))
    arrived, down1 = lax.optimization_barrier((blocks_exchange(outgoing), swap(later)))
    features = exchange(arrange(arrived, both, chips, half), "x")
    hidden = hidden_of(place, features, gate0, up0, gate1, up1)
    result = down_of(place, ring(hidden), in_hbm(down0), in_hbm(down1), half)
    mixed = lax.all_gather(combine(blocks_exchange(result), cols), "c", axis=0)
    mixed, sums = sums_of(place, mixed, chips * CORES)
    sums = exchange(sums, ("x", "c"))
    return final(mixed, sums, in_hbm(post_gain[None, :]))


def solution(mesh):
    ep_count, tp_count = mesh.devices.shape
    devices = mesh.devices.reshape(ep_count, tp_count // CORES, CORES)
    return jax.shard_map(
        on_device,
        mesh=Mesh(devices, ("ep", "x", "c")),
        in_specs=(
            P("ep", ("x", "c")),
            P("ep", None),
            P("ep", None),
            P(("x", "c")),
            P(("x", "c")),
            P("ep", None, ("x", "c")),
            P("ep", None, ("x", "c")),
            P("ep", None, ("x", "c")),
        ),
        out_specs=P("ep", ("x", "c")),
        check_vma=False,
    )
```

time: 192 us -> 175 us (0.911)
  blocking collectives: 131 us -> 74.4 us
  waiting for transfers between devices: 8.72 us -> 49.2 us
    all_gather x2 -> x1, blocking collectives: 72 us -> 7.44 us  [on_device(): mixed = lax.all_gather(combine(blocks_exchange(result), cols), 'c', axis=0)]
    ppermute x0 -> x7, starting transfers between devices: none -> 21.5 us  [the longest x3 13.7 us: ring(): after = lax.ppermute(after, 'x', backward)]
    ppermute x0 -> x7, waiting for transfers between devices: none -> 20.6 us  [the longest x4 20.6 us: ring(): before = lax.ppermute(before, 'x', onward)]
    all_to_all x3 -> x1, waiting for transfers between devices: 8.71 us -> 26.9 us  [exchange(): return lax.all_to_all(value, axis, split_axis=0, concat_axis=0, tiled=True)]
    all_to_all x3 -> x1, starting transfers between devices: 22.3 us -> 6.61 us  [exchange(): return lax.all_to_all(value, axis, split_axis=0, concat_axis=0, tiled=True)]
    all_to_all x3, blocking collectives: 43.7 us -> 51.2 us  [exchange(): return lax.all_to_all(value, axis, split_axis=0, concat_axis=0, tiled=True)]
    ppermute x3, starting transfers between devices: 13.7 us -> 8.83 us  [swap(): return lax.ppermute(value, 'c', [(0, 1), (1, 0)])]
  transfers between devices with their start and end apart: 6 -> 11, of which waited for: 1 -> 7; matrix products, arithmetic and copies ran while one was open for 0% -> 0% of each run, Pallas kernels for 0% -> 0%
where the time goes in v5:
time: 175 us
  blocking collectives  74.4 us (43%)
  waiting for transfers between devices  49.2 us (28%)
  starting transfers between devices  36.9 us (21%)
  Pallas kernels  13 us (7%)
    all_to_all x3, blocking collectives, exchange(): return lax.all_to_all(value, axis, split_axis=0, concat_axis=0, tiled=True)  51.2 us
    all_to_all x1, waiting for transfers between devices, exchange(): return lax.all_to_all(value, axis, split_axis=0, concat_axis=0, tiled=True)  26.9 us
    ppermute x4, waiting for transfers between devices, ring(): before = lax.ppermute(before, 'x', onward)  20.6 us
    all_gather x1, blocking collectives, on_device(): lax.all_gather(prepare(in_hbm(tokens), in_hbm(pre_gain[None, :])), 'c', a...  15.7 us
    ppermute x3, starting transfers between devices, ring(): after = lax.ppermute(after, 'x', backward)  13.7 us
    ppermute x3, starting transfers between devices, swap(): return lax.ppermute(value, 'c', [(0, 1), (1, 0)])  8.83 us
    ppermute x4, starting transfers between devices, ring(): before = lax.ppermute(before, 'x', onward)  7.78 us
    all_gather x1, blocking collectives, on_device(): mixed = lax.all_gather(combine(blocks_exchange(result), cols), 'c', axis=0)  7.44 us
  transfers between devices with their start and end apart: 11, of which 7 were waited for; matrix products, arithmetic and copies ran while one was open for 0% of the time, Pallas kernels for 0%

profile of v5, /device:TPU:1, one launch (start us, length us, event | category | flops | bytes accessed | tf_op | source)
XLA Modules:
  0.0 174.8 jit_solution(16165700980269127384)
XLA Ops:
  0.0 0.9 prepare.1
  0.9 15.7 %all-gather = bf16[544,128]{1,0:T(8,128)(2,1)S(1)} all-gather(bf16[272,128]{1,0:T(8,128)(2,1)S(1)} %prepare.1), channel_id=2, replica_groups=mesh['ep'=64,'x'=8,'c'=2] {'c'}, dimensions={0}, use_global_device_ids=true | all-gather | bytes 208896 | tf_op jit(solution)/shard_map/all_gather | solution.py:364
  16.6 1.8 %dispatch.1 = (bf16[512,256]{1,0:T(8,128)(2,1)S(1)}, f32[256,8]{1,0:T(8,128)}) custom-call(s32[2]{0:T(128)S(1)} %pad_add_fusion.refs_0_.place_ref, bf16[2,272,128]{2,1,0:T(8,128)(2,1)S(1)} %bitcast.16, s32[2,256]{1,0:T(2,128)} %bitcast.28, f32[2,256]{1,0:T(2,128)} %bitcast.29), custom_call_target="tpu_custom_call" | custom-call | tf_op jit(solution)/shard_map/dispatch/pallas_call | solution.py:96
  18.4 2.3 %collective-permute-start = (bf16[4096,128]{1,0:T(8,128)(2,1)}, bf16[4096,128]{1,0:T(8,128)(2,1)}, u32[]{:S(2)}, u32[]{:S(2)}) collective-permute-start(bf16[4096,128]{1,0:T(8,128)(2,1)} %bitcast.26), channel_id=1, source_target_pairs={{0,1},{1,0},{2,3},{3,2},{4,5},{5,4},{6,7},{7,6},{8,9},{9,8},{10,11... | collective-permute-start | bytes 3145736 | tf_op jit(solution)/shard_map/ppermute | solution.py:334
  20.7 23.7 %all_to_all.20 = bf16[64,8,256]{2,1,0:T(8,128)(2,1)S(1)} all-to-all(bf16[64,8,256]{2,1,0:T(8,128)(2,1)S(1)} %bitcast.25), channel_id=1, replica_groups=mesh['ep'=64,'x'=8,'c'=2] {'ep'}, dimensions={0} | all-to-all | bytes 524288 | tf_op jit(solution)/shard_map/all_to_all | solution.py:325
  44.4 1.3 arrange.1
  45.7 6.6 %all-to-all-start.1 = ((bf16[8,336,256]{2,1,0:T(8,128)(2,1)}), bf16[8,336,256]{2,1,0:T(8,128)(2,1)S(1)}, u32[]{:S(2)}, u32[]{:S(2)}) async-start(bf16[8,336,256]{2,1,0:T(8,128)(2,1)} %arrange.1), calls=%async_computation.1 | async-start | bytes 2752512 | tf_op jit(solution)/shard_map/all_to_all | solution.py:325
  52.4 4.7 %collective-permute-start.1 = (bf16[2048,256]{1,0:T(8,128)(2,1)S(1)}, bf16[2048,256]{1,0:T(8,128)(2,1)S(1)}, u32[]{:S(2)}, u32[]{:S(2)}) collective-permute-start(bf16[2048,256]{1,0:T(8,128)(2,1)S(1)} %bitcast.21), channel_id=1, source_target_pairs={{0,1},{1,0},{2,3},{3,2},{4,5},{5,4},{6,7},{7,6},{8,9},{9,8},{10,11... | collective-permute-start | bytes 3145736 | tf_op jit(solution)/shard_map/ppermute | solution.py:334
  57.0 1.9 %collective-permute-start.2 = (bf16[2048,256]{1,0:T(8,128)(2,1)S(1)}, bf16[2048,256]{1,0:T(8,128)(2,1)}, u32[]{:S(2)}, u32[]{:S(2)}) collective-permute-start(bf16[2048,256]{1,0:T(8,128)(2,1)S(1)} %bitcast.23), channel_id=1, source_target_pairs={{0,1},{1,0},{2,3},{3,2},{4,5},{5,4},{6,7},{7,6},{8,9},{9,8},{10,11... | collective-permute-start | bytes 3145736 | tf_op jit(solution)/shard_map/ppermute | solution.py:334
  59.0 0.3 collective-permute-done.1.gate1_ref
  59.3 1.0 copy-done.3
  60.3 1.4 collective-permute-done.2.up1_ref
  61.7 26.9 %all-to-all-done.1.feat_ref = bf16[8,336,256]{2,1,0:T(8,128)(2,1)S(1)} async-done(((bf16[8,336,256]{2,1,0:T(8,128)(2,1)}), bf16[8,336,256]{2,1,0:T(8,128)(2,1)S(1)}, u32[]{:S(2)}, u32[]{:S(2)}) %all-to-all-start.1) | async-done | bytes 1376288 | tf_op jit(solution)/shard_map/all_to_all | solution.py:325
  88.6 3.3 %hidden.1.refs_1_ = bf16[320,512]{1,0:T(8,128)(2,1)S(1)} custom-call(s32[2]{0:T(128)S(1)} %pad_add_fusion.refs_0_.place_ref, bf16[8,336,256]{2,1,0:T(8,128)(2,1)S(1)} %all-to-all-done.1.feat_ref, bf16[2048,256]{1,0:T(8,128)(2,1)S(1)} %bitcast.22, bf16[2048,256]{1,0:T(8,128)(2,1)S(1)} %bitcast.24, bf16[2048,256]{1,0:T(8,128)(2,1)} %copy-done.3, ...), custom_call_target="tpu_custom_call" | custom-call | tf_op jit(solution)/shard_map/hidden/pallas_call | solution.py:190
  91.9 2.1 %collective-permute-start.3 = (bf16[320,512]{1,0:T(8,128)(2,1)S(1)}, bf16[320,512]{1,0:T(8,128)(2,1)S(1)}, u32[]{:S(2)}, u32[]{:S(2)}) collective-permute-start(bf16[320,512]{1,0:T(8,128)(2,1)S(1)} %hidden.1.refs_1_), channel_id=1, source_target_pairs={{0,2},{2,4},{4,6},{6,8},{8,10},{10,12},{12,14},{14,0},{1,3},{3,5},... | collective-permute-start | bytes 983048 | tf_op jit(solution)/shard_map/ppermute | solution.py:344
  94.0 4.6 %collective-permute-start.4 = (bf16[320,512]{1,0:T(8,128)(2,1)S(1)}, bf16[320,512]{1,0:T(8,128)(2,1)S(1)}, u32[]{:S(2)}, u32[]{:S(2)}) collective-permute-start(bf16[320,512]{1,0:T(8,128)(2,1)S(1)} %hidden.1.refs_1_), channel_id=1, source_target_pairs={{0,14},{2,0},{4,2},{6,4},{8,6},{10,8},{12,10},{14,12},{1,15},{3,1}... | collective-permute-start | bytes 983048 | tf_op jit(solution)/shard_map/ppermute | solution.py:347
  98.6 5.4 %collective-permute-done.3.refs_2_ = bf16[320,512]{1,0:T(8,128)(2,1)S(1)} collective-permute-done((bf16[320,512]{1,0:T(8,128)(2,1)S(1)}, bf16[320,512]{1,0:T(8,128)(2,1)S(1)}, u32[]{:S(2)}, u32[]{:S(2)}) %collective-permute-start.3) | collective-permute-done | bytes 327712 | tf_op jit(solution)/shard_map/ppermute | solution.py:344
  103.9 1.9 %collective-permute-start.5 = (bf16[320,512]{1,0:T(8,128)(2,1)S(1)}, bf16[320,512]{1,0:T(8,128)(2,1)S(1)}, u32[]{:S(2)}, u32[]{:S(2)}) collective-permute-start(bf16[320,512]{1,0:T(8,128)(2,1)S(1)} %collective-permute-done.3.refs_2_), channel_id=1, source_target_pairs={{0,2},{2,4},{4,6},{6,8},{8,10},{10,12},{12,14},{14,0},{1,3},{3,5},... | collective-permute-start | bytes 983048 | tf_op jit(solution)/shard_map/ppermute | solution.py:344
  105.9 4.6 %collective-permute-start.6 = (bf16[320,512]{1,0:T(8,128)(2,1)S(1)}, bf16[320,512]{1,0:T(8,128)(2,1)S(1)}, u32[]{:S(2)}, u32[]{:S(2)}) collective-permute-start(bf16[320,512]{1,0:T(8,128)(2,1)S(1)} %collective-permute-done.4.refs_3_), channel_id=1, source_target_pairs={{0,14},{2,0},{4,2},{6,4},{8,6},{10,8},{12,10},{14,12},{1,15},{3,1}... | collective-permute-start | bytes 983048 | tf_op jit(solution)/shard_map/ppermute | solution.py:347
  110.4 4.5 %collective-permute-done.5.refs_4_ = bf16[320,512]{1,0:T(8,128)(2,1)S(1)} collective-permute-done((bf16[320,512]{1,0:T(8,128)(2,1)S(1)}, bf16[320,512]{1,0:T(8,128)(2,1)S(1)}, u32[]{:S(2)}, u32[]{:S(2)}) %collective-permute-start.5) | collective-permute-done | bytes 327712 | tf_op jit(solution)/shard_map/ppermute | solution.py:344
  114.9 1.9 %collective-permute-start.7 = (bf16[320,512]{1,0:T(8,128)(2,1)S(1)}, bf16[320,512]{1,0:T(8,128)(2,1)S(1)}, u32[]{:S(2)}, u32[]{:S(2)}) collective-permute-start(bf16[320,512]{1,0:T(8,128)(2,1)S(1)} %collective-permute-done.5.refs_4_), channel_id=1, source_target_pairs={{0,2},{2,4},{4,6},{6,8},{8,10},{10,12},{12,14},{14,0},{1,3},{3,5},... | collective-permute-start | bytes 983048 | tf_op jit(solution)/shard_map/ppermute | solution.py:344
  116.9 4.6 %collective-permute-start.8 = (bf16[320,512]{1,0:T(8,128)(2,1)S(1)}, bf16[320,512]{1,0:T(8,128)(2,1)S(1)}, u32[]{:S(2)}, u32[]{:S(2)}) collective-permute-start(bf16[320,512]{1,0:T(8,128)(2,1)S(1)} %collective-permute-done.6.refs_5_), channel_id=1, source_target_pairs={{0,14},{2,0},{4,2},{6,4},{8,6},{10,8},{12,10},{14,12},{1,15},{3,1}... | collective-permute-start | bytes 983048 | tf_op jit(solution)/shard_map/ppermute | solution.py:347
  121.5 3.6 %collective-permute-done.7.refs_6_ = bf16[320,512]{1,0:T(8,128)(2,1)S(1)} collective-permute-done((bf16[320,512]{1,0:T(8,128)(2,1)S(1)}, bf16[320,512]{1,0:T(8,128)(2,1)S(1)}, u32[]{:S(2)}, u32[]{:S(2)}) %collective-permute-start.7) | collective-permute-done | bytes 327712 | tf_op jit(solution)/shard_map/ppermute | solution.py:344
  125.1 1.9 %collective-permute-start.9 = (bf16[320,512]{1,0:T(8,128)(2,1)S(1)}, bf16[320,512]{1,0:T(8,128)(2,1)S(1)}, u32[]{:S(2)}, u32[]{:S(2)}) collective-permute-start(bf16[320,512]{1,0:T(8,128)(2,1)S(1)} %collective-permute-done.7.refs_6_), channel_id=1, source_target_pairs={{0,2},{2,4},{4,6},{6,8},{8,10},{10,12},{12,14},{14,0},{1,3},{3,5},... | collective-permute-start | bytes 983048 | tf_op jit(solution)/shard_map/ppermute | solution.py:344
  127.0 7.1 %collective-permute-done.9.refs_8_ = bf16[320,512]{1,0:T(8,128)(2,1)S(1)} collective-permute-done((bf16[320,512]{1,0:T(8,128)(2,1)S(1)}, bf16[320,512]{1,0:T(8,128)(2,1)S(1)}, u32[]{:S(2)}, u32[]{:S(2)}) %collective-permute-start.9) | collective-permute-done | bytes 327712 | tf_op jit(solution)/shard_map/ppermute | solution.py:344
  134.1 3.0 %down.1 = bf16[512,256]{1,0:T(8,128)(2,1)S(1)} custom-call(s32[2]{0:T(128)S(1)} %pad_add_fusion.refs_0_.place_ref, bf16[320,512]{1,0:T(8,128)(2,1)S(1)} %hidden.1.refs_1_, bf16[320,512]{1,0:T(8,128)(2,1)S(1)} %collective-permute-done.3.refs_2_, bf16[320,512]{1,0:T(8,128)(2,1)S(1)} %collective-permute-done.4.refs_3_, ...), custom_call_target="tpu_custom_call" | custom-call | tf_op jit(solution)/shard_map/down/pallas_call | solution.py:237
  137.2 17.4 %all_to_all.21 = bf16[64,8,256]{2,1,0:T(8,128)(2,1)S(1)} all-to-all(bf16[64,8,256]{2,1,0:T(8,128)(2,1)S(1)} %bitcast.18), channel_id=1, replica_groups=mesh['ep'=64,'x'=8,'c'=2] {'ep'}, dimensions={0} | all-to-all | bytes 524288 | tf_op jit(solution)/shard_map/all_to_all | solution.py:325
  154.5 0.4 combine.1
  154.9 7.4 %all-gather.1 = f32[512,256]{1,0:T(8,128)S(1)} all-gather(f32[256,256]{1,0:T(8,128)S(1)} %combine.1), channel_id=3, replica_groups=mesh['ep'=64,'x'=8,'c'=2] {'c'}, dimensions={0}, use_global_device_ids=true | all-gather | bytes 786432 | tf_op jit(solution)/shard_map/all_gather | solution.py:378
  162.4 0.7 sums.1
  163.1 10.1 %all_to_all.22.sums_ref = f32[16,1,256]{2,1,0:T(1,128)S(1)} all-to-all(f32[16,1,256]{2,1,0:T(1,128)S(1)} %get-tuple-element.20), channel_id=1, replica_groups=mesh['ep'=64,'x'=8,'c'=2] {'x','c'}, dimensions={0} | all-to-all | bytes 32768 | tf_op jit(solution)/shard_map/all_to_all | solution.py:325
  173.2 1.6 final.1
  (12 shorter events, 0.1 us)
Async XLA Ops:
  18.4 26.0 %collective-permute-start = (bf16[4096,128]{1,0:T(8,128)(2,1)}, bf16[4096,128]{1,0:T(8,128)(2,1)}, u32[]{:S(2)}, u32[]{:S(2)}) collective-permute-start(bf16[4096,128]{1,0:T(8,128)(2,1)} %bitcast.26), channel_id=1, source_target_pairs={{0,1},{1,0},{2,3},{3,2},{4,5},{5,4},{6,7},{7,6},{8,9},{9,8},{10,11... | collective-permute-start | bytes 3145736 | tf_op jit(solution)/shard_map/ppermute | solution.py:334
  45.7 6.6 %copy-start = (bf16[1,2048,256]{2,1,0:T(8,128)(2,1)S(1)}, bf16[1,2048,256]{2,1,0:T(8,128)(2,1)}, u32[]{:S(2)}) copy-start(bf16[1,2048,256]{2,1,0:T(8,128)(2,1)} %param.13) | copy-start | bytes 3145732
  45.7 11.3 %copy-start.1 = (bf16[1,2048,256]{2,1,0:T(8,128)(2,1)S(1)}, bf16[1,2048,256]{2,1,0:T(8,128)(2,1)}, u32[]{:S(2)}) copy-start(bf16[1,2048,256]{2,1,0:T(8,128)(2,1)} %param.14) | copy-start | bytes 3145732
  45.7 42.8 %all-to-all-start.1 = ((bf16[8,336,256]{2,1,0:T(8,128)(2,1)}), bf16[8,336,256]{2,1,0:T(8,128)(2,1)S(1)}, u32[]{:S(2)}, u32[]{:S(2)}) async-start(bf16[8,336,256]{2,1,0:T(8,128)(2,1)} %arrange.1), calls=%async_computation.1 | async-start | bytes 2752512 | tf_op jit(solution)/shard_map/all_to_all | solution.py:325
  52.4 6.9 %collective-permute-start.1 = (bf16[2048,256]{1,0:T(8,128)(2,1)S(1)}, bf16[2048,256]{1,0:T(8,128)(2,1)S(1)}, u32[]{:S(2)}, u32[]{:S(2)}) collective-permute-start(bf16[2048,256]{1,0:T(8,128)(2,1)S(1)} %bitcast.21), channel_id=1, source_target_pairs={{0,1},{1,0},{2,3},{3,2},{4,5},{5,4},{6,7},{7,6},{8,9},{9,8},{10,11... | collective-permute-start | bytes 3145736 | tf_op jit(solution)/shard_map/ppermute | solution.py:334
  57.0 4.7 %collective-permute-start.2 = (bf16[2048,256]{1,0:T(8,128)(2,1)S(1)}, bf16[2048,256]{1,0:T(8,128)(2,1)}, u32[]{:S(2)}, u32[]{:S(2)}) collective-permute-start(bf16[2048,256]{1,0:T(8,128)(2,1)S(1)} %bitcast.23), channel_id=1, source_target_pairs={{0,1},{1,0},{2,3},{3,2},{4,5},{5,4},{6,7},{7,6},{8,9},{9,8},{10,11... | collective-permute-start | bytes 3145736 | tf_op jit(solution)/shard_map/ppermute | solution.py:334
  59.3 1.0 copy-start.3
  91.9 62.6 %copy-start.2 = (f32[256,8]{1,0:T(8,128)S(1)}, f32[256,8]{1,0:T(8,128)}, u32[]{:S(2)}) copy-start(f32[256,8]{1,0:T(8,128)} %get-tuple-element.18.cols_ref) | copy-start | bytes 24580
  91.9 12.0 %collective-permute-start.3 = (bf16[320,512]{1,0:T(8,128)(2,1)S(1)}, bf16[320,512]{1,0:T(8,128)(2,1)S(1)}, u32[]{:S(2)}, u32[]{:S(2)}) collective-permute-start(bf16[320,512]{1,0:T(8,128)(2,1)S(1)} %hidden.1.refs_1_), channel_id=1, source_target_pairs={{0,2},{2,4},{4,6},{6,8},{8,10},{10,12},{12,14},{14,0},{1,3},{3,5},... | collective-permute-start | bytes 983048 | tf_op jit(solution)/shard_map/ppermute | solution.py:344
  94.0 11.9 %collective-permute-start.4 = (bf16[320,512]{1,0:T(8,128)(2,1)S(1)}, bf16[320,512]{1,0:T(8,128)(2,1)S(1)}, u32[]{:S(2)}, u32[]{:S(2)}) collective-permute-start(bf16[320,512]{1,0:T(8,128)(2,1)S(1)} %hidden.1.refs_1_), channel_id=1, source_target_pairs={{0,14},{2,0},{4,2},{6,4},{8,6},{10,8},{12,10},{14,12},{1,15},{3,1}... | collective-permute-start | bytes 983048 | tf_op jit(solution)/shard_map/ppermute | solution.py:347
  103.9 11.0 %collective-permute-start.5 = (bf16[320,512]{1,0:T(8,128)(2,1)S(1)}, bf16[320,512]{1,0:T(8,128)(2,1)S(1)}, u32[]{:S(2)}, u32[]{:S(2)}) collective-permute-start(bf16[320,512]{1,0:T(8,128)(2,1)S(1)} %collective-permute-done.3.refs_2_), channel_id=1, source_target_pairs={{0,2},{2,4},{4,6},{6,8},{8,10},{10,12},{12,14},{14,0},{1,3},{3,5},... | collective-permute-start | bytes 983048 | tf_op jit(solution)/shard_map/ppermute | solution.py:344
  105.9 11.0 %collective-permute-start.6 = (bf16[320,512]{1,0:T(8,128)(2,1)S(1)}, bf16[320,512]{1,0:T(8,128)(2,1)S(1)}, u32[]{:S(2)}, u32[]{:S(2)}) collective-permute-start(bf16[320,512]{1,0:T(8,128)(2,1)S(1)} %collective-permute-done.4.refs_3_), channel_id=1, source_target_pairs={{0,14},{2,0},{4,2},{6,4},{8,6},{10,8},{12,10},{14,12},{1,15},{3,1}... | collective-permute-start | bytes 983048 | tf_op jit(solution)/shard_map/ppermute | solution.py:347
  114.9 10.2 %collective-permute-start.7 = (bf16[320,512]{1,0:T(8,128)(2,1)S(1)}, bf16[320,512]{1,0:T(8,128)(2,1)S(1)}, u32[]{:S(2)}, u32[]{:S(2)}) collective-permute-start(bf16[320,512]{1,0:T(8,128)(2,1)S(1)} %collective-permute-done.5.refs_4_), channel_id=1, source_target_pairs={{0,2},{2,4},{4,6},{6,8},{8,10},{10,12},{12,14},{14,0},{1,3},{3,5},... | collective-permute-start | bytes 983048 | tf_op jit(solution)/shard_map/ppermute | solution.py:344
  116.9 10.2 %collective-permute-start.8 = (bf16[320,512]{1,0:T(8,128)(2,1)S(1)}, bf16[320,512]{1,0:T(8,128)(2,1)S(1)}, u32[]{:S(2)}, u32[]{:S(2)}) collective-permute-start(bf16[320,512]{1,0:T(8,128)(2,1)S(1)} %collective-permute-done.6.refs_5_), channel_id=1, source_target_pairs={{0,14},{2,0},{4,2},{6,4},{8,6},{10,8},{12,10},{14,12},{1,15},{3,1}... | collective-permute-start | bytes 983048 | tf_op jit(solution)/shard_map/ppermute | solution.py:347
  125.1 9.0 %collective-permute-start.9 = (bf16[320,512]{1,0:T(8,128)(2,1)S(1)}, bf16[320,512]{1,0:T(8,128)(2,1)S(1)}, u32[]{:S(2)}, u32[]{:S(2)}) collective-permute-start(bf16[320,512]{1,0:T(8,128)(2,1)S(1)} %collective-permute-done.7.refs_6_), channel_id=1, source_target_pairs={{0,2},{2,4},{4,6},{6,8},{8,10},{10,12},{12,14},{14,0},{1,3},{3,5},... | collective-permute-start | bytes 983048 | tf_op jit(solution)/shard_map/ppermute | solution.py:344

commit v6 on v5

--- a/solution.py
+++ b/solution.py
@@ -4,6 +4,7 @@
 from jax.experimental import pallas as pl
 from jax.experimental.pallas import tpu as pltpu
 from jax.sharding import Mesh, PartitionSpec as P
+
 
 epsilon = 1e-06
 CORES = 2
@@ -197,9 +198,7 @@
     )(place, features, gate0, up0, gate1, up1)
 
 
-def down_kernel(*refs, offsets, half):
-    place_ref, *hidden_refs, down0_ref, down1_ref, out_ref, down_ref, result_ref = refs
-    rows, units = hidden_refs[0].shape
+def both_columns(place_ref, down0_ref, down1_ref, down_ref):
     width = down0_ref.shape[1]
     for c in range(CORES):
 
@@ -208,14 +207,47 @@
             down_ref[:, c * width : (c + 1) * width] = down0_ref[...]
             down_ref[:, (1 - c) * width : (2 - c) * width] = down1_ref[...]
 
-    chips = len(offsets)
-    total = jnp.zeros((rows, CORES * width), jnp.float32)
+
+def down_early_kernel(*refs, offsets, chips):
+    place_ref, *hidden_refs, down0_ref, down1_ref, out_ref, down_ref = refs
+    _, units = hidden_refs[0].shape
+    both_columns(place_ref, down0_ref, down1_ref, down_ref)
+    total = jnp.zeros(out_ref.shape, jnp.float32)
     for offset, ref in zip(offsets, hidden_refs):
         chip = lax.rem(place_ref[0] + (offset + chips), chips)
         begin = pl.multiple_of(chip * units, units)
         total = total + jnp.dot(
             ref[...], down_ref[pl.ds(begin, units), :], preferred_element_type=jnp.float32
         )
+    out_ref[...] = total
+
+
+def down_early(place, hiddens, down0, down1, chips):
+    offsets = [offset for offset, _ in hiddens]
+    arrays = [array for _, array in hiddens]
+    rows = arrays[0].shape[0]
+    full, width = down0.shape
+
+    def body(*refs):
+        down_early_kernel(*refs, offsets=offsets, chips=chips)
+
+    return pl.pallas_call(
+        body,
+        in_specs=[whole(pltpu.SMEM)] + [whole()] * (len(arrays) + 2),
+        out_shape=jax.ShapeDtypeStruct((rows, CORES * width), jnp.float32),
+        scratch_shapes=[pltpu.VMEM((full, CORES * width), jnp.bfloat16)],
+        compiler_params=params(16),
+        name="down_early",
+    )(place, *arrays, down0, down1)
+
+
+def down_last_kernel(
+    place_ref, total_ref, hidden_ref, down0_ref, down1_ref, out_ref, down_ref, result_ref, *, half
+):
+    both_columns(place_ref, down0_ref, down1_ref, down_ref)
+    total = total_ref[...] + jnp.dot(
+        hidden_ref[...], down_ref[...], preferred_element_type=jnp.float32
+    )
     result_ref[...] = total.astype(jnp.bfloat16)
     step = GROUP * half
     place = packed_place((GROUP * PAD, step), 0, half)
@@ -225,26 +257,38 @@
         ).astype(jnp.bfloat16)
 
 
-def down_of(place, hiddens, down0, down1, half):
-    offsets = [offset for offset, _ in hiddens]
-    arrays = [array for _, array in hiddens]
-    rows = arrays[0].shape[0]
-    full, width = down0.shape
+def down_last(place, total, last, down0, down1, chips, half):
+    offset, hidden = last
+    rows, units = hidden.shape
+    _, width = down0.shape
 
     def body(*refs):
-        down_kernel(*refs, offsets=offsets, half=half)
+        down_last_kernel(*refs, half=half)
+
+    def chip_rows(place_ref):
+        return lax.rem(place_ref[0] + (offset + chips), chips)
 
     return pl.pallas_call(
         body,
-        in_specs=[whole(pltpu.SMEM)] + [whole()] * (len(arrays) + 2),
+        grid_spec=pltpu.PrefetchScalarGridSpec(
+            num_scalar_prefetch=1,
+            grid=(1,),
+            in_specs=[
+                pl.BlockSpec((rows, CORES * width), lambda i, p: (0, 0)),
+                pl.BlockSpec((rows, units), lambda i, p: (0, 0)),
+                pl.BlockSpec((units, width), lambda i, p: (chip_rows(p), 0)),
+                pl.BlockSpec((units, width), lambda i, p: (chip_rows(p), 0)),
+            ],
+            out_specs=pl.BlockSpec((rows // half * PAD, CORES * width), lambda i, p: (0, 0)),
+            scratch_shapes=[
+                pltpu.VMEM((units, CORES * width), jnp.bfloat16),
+                pltpu.VMEM((rows, CORES * width), jnp.bfloat16),
+            ],
+        ),
         out_shape=jax.ShapeDtypeStruct((rows // half * PAD, CORES * width), jnp.bfloat16),
-        scratch_shapes=[
-            pltpu.VMEM((full, CORES * width), jnp.bfloat16),
-            pltpu.VMEM((rows, CORES * width), jnp.bfloat16),
-        ],
-        compiler_params=params(24),
-        name="down",
-    )(place, *arrays, down0, down1)
+        compiler_params=params(8),
+        name="down_last",
+    )(place, total, hidden, down0, down1)
 
 
 def combine_kernel(returned_ref, cols_ref, mixed_ref):
@@ -273,28 +317,27 @@
 
 def sums_kernel(place_ref, parts_ref, mixed_ref, sums_ref):
     rows, width = mixed_ref.shape
+    both = parts_ref[0] + parts_ref[1]
     for c in range(CORES):
 
         @pl.when(place_ref[1] == c)
         def _():
-            own = slice(c * width, (c + 1) * width)
-            mixed_ref[...] = parts_ref[0, :, own] + parts_ref[1, :, own]
-
-    mixed = mixed_ref[...]
-    sums = jnp.sum(mixed * mixed, axis=1, keepdims=True)
+            mixed_ref[...] = both[:, c * width : (c + 1) * width]
+
+    sums = jnp.sum(both * both, axis=1, keepdims=True)
     line = jnp.transpose(jnp.broadcast_to(sums, (rows, 128)))[0:1, :]
     for j in range(sums_ref.shape[0]):
         sums_ref[j] = line
 
 
-def sums_of(place, parts, peers):
+def sums_of(place, parts, chips):
     _, rows, wide = parts.shape
     return pl.pallas_call(
         sums_kernel,
         in_specs=[whole(pltpu.SMEM), whole()],
         out_shape=(
             jax.ShapeDtypeStruct((rows, wide // CORES), jnp.float32),
-            jax.ShapeDtypeStruct((peers, 1, rows), jnp.float32),
+            jax.ShapeDtypeStruct((chips, 1, rows), jnp.float32),
         ),
         compiler_params=params(4),
         name="sums",
@@ -303,11 +346,11 @@
 
 def final_kernel(mixed_ref, sums_ref, gain_ref, out_ref):
     rows, width = mixed_ref.shape
-    peers = sums_ref.shape[0]
+    chips = sums_ref.shape[0]
     total = sums_ref[0]
-    for j in range(1, peers):
+    for j in range(1, chips):
         total = total + sums_ref[j]
-    scale = lax.rsqrt(total / (peers * width) + epsilon)
+    scale = lax.rsqrt(total / (chips * CORES * width) + epsilon)
     column = jnp.transpose(jnp.broadcast_to(scale, (8, rows)))[:, 0:1]
     out_ref[...] = (mixed_ref[...] * column * gain_ref[...]).astype(jnp.bfloat16)
 
@@ -349,7 +392,7 @@
     return arrays
 
 
-def on_device(
+def layer(
     tokens, expert_ids, route_weights, pre_gain, post_gain, gate_weight, up_weight, down_weight
 ):
     tok_rows = tokens.shape[0]
@@ -360,7 +403,6 @@
     half = capacity // CORES
     place = jnp.stack([lax.axis_index("x"), lax.axis_index("c")]).astype(jnp.int32)
     gate0, up0, down0 = gate_weight[0], up_weight[0], down_weight[0]
-    gate1, up1 = in_hbm(swap(gate0)), in_hbm(swap(up0))
     both = lax.all_gather(prepare(in_hbm(tokens), in_hbm(pre_gain[None, :])), "c", axis=0)
     outgoing, cols = dispatch(
         place,
@@ -370,14 +412,19 @@
         ep_count,
         capacity,
     )
-    outgoing, later = lax.optimization_barrier((outgoing, down0))
-    arrived, down1 = lax.optimization_barrier((blocks_exchange(outgoing), swap(later)))
+    arrived = blocks_exchange(outgoing)
+    swapped = []
+    for weight in (gate0, up0, down0):
+        swapped.append(swap(weight))
+    arrived, gate1, up1, down1 = lax.optimization_barrier((arrived, *swapped))
     features = exchange(arrange(arrived, both, chips, half), "x")
-    hidden = hidden_of(place, features, gate0, up0, gate1, up1)
-    result = down_of(place, ring(hidden), in_hbm(down0), in_hbm(down1), half)
+    hidden = hidden_of(place, features, gate0, up0, in_hbm(gate1), in_hbm(up1))
+    *early, last = ring(hidden)
+    total = down_early(place, early, in_hbm(down0), in_hbm(down1), chips)
+    result = down_last(place, total, last, in_hbm(down0), in_hbm(down1), chips, half)
     mixed = lax.all_gather(combine(blocks_exchange(result), cols), "c", axis=0)
-    mixed, sums = sums_of(place, mixed, chips * CORES)
-    sums = exchange(sums, ("x", "c"))
+    mixed, sums = sums_of(place, mixed, chips)
+    sums = exchange(sums, "x")
     return final(mixed, sums, in_hbm(post_gain[None, :]))
 
 
@@ -385,7 +432,7 @@
     ep_count, tp_count = mesh.devices.shape
     devices = mesh.devices.reshape(ep_count, tp_count // CORES, CORES)
     return jax.shard_map(
-        on_device,
+        layer,
         mesh=Mesh(devices, ("ep", "x", "c")),
         in_specs=(
             P("ep", ("x", "c")),

time: 175 us -> 173 us (0.989)
  waiting for transfers between devices: 49.2 us -> 13.5 us
  blocking collectives: 74.4 us -> 103 us
  starting transfers between devices: 36.9 us -> 41.7 us
    all_to_all x3 -> x4, blocking collectives: 51.2 us -> 90.6 us  [exchange(): return lax.all_to_all(value, axis, split_axis=0, concat_axis=0, tiled=True)]
    all_to_all x1 -> x0, waiting for transfers between devices: 26.9 us -> none  [exchange(): return lax.all_to_all(value, axis, split_axis=0, concat_axis=0, tiled=True)]
    ppermute x3, starting transfers between devices: 8.83 us -> 20.3 us  [swap(): return lax.ppermute(value, 'c', [(0, 1), (1, 0)])]
    all_gather x2, blocking collectives: 23.1 us -> 12.1 us  [the longest x1 10.1 us: layer(): mixed = lax.all_gather(combine(blocks_exchange(result), cols), 'c', axis=0)]
    ppermute x4, waiting for transfers between devices: 20.6 us -> 13.5 us  [ring(): before = lax.ppermute(before, 'x', onward)]
    all_to_all x1 -> x0, starting transfers between devices: 6.61 us -> none  [exchange(): return lax.all_to_all(value, axis, split_axis=0, concat_axis=0, tiled=True)]
    ppermute x3, waiting for transfers between devices: 1.76 us -> 0.01 us  [swap(): return lax.ppermute(value, 'c', [(0, 1), (1, 0)])]
    pallas_call x1 -> x2, Pallas kernels: 3.02 us -> 4.74 us  [the longest x1 2.69 us: down_early(): pl.pallas_call(body, in_specs=[whole(pltpu.SMEM)] + [whole()] * (len(arra...]
  transfers between devices with their start and end apart: 11 -> 10, of which waited for: 7 -> 4; matrix products, arithmetic and copies ran while one was open for 0% -> 0% of each run, Pallas kernels for 0% -> 3%
where the time goes in v6:
time: 173 us; the launch traced here: 172 us
  blocking collectives  103 us (60%)
  starting transfers between devices  41.7 us (24%)
  Pallas kernels  13.6 us (8%)
  waiting for transfers between devices  13.5 us (8%)
    all_to_all x4, blocking collectives, exchange(): return lax.all_to_all(value, axis, split_axis=0, concat_axis=0, tiled=True)  90.6 us
    ppermute x3, starting transfers between devices, swap(): return lax.ppermute(value, 'c', [(0, 1), (1, 0)])  20.3 us
    ppermute x3, starting transfers between devices, ring(): after = lax.ppermute(after, 'x', backward)  13.7 us
    ppermute x4, waiting for transfers between devices, ring(): before = lax.ppermute(before, 'x', onward)  13.5 us
    all_gather x1, blocking collectives, layer(): mixed = lax.all_gather(combine(blocks_exchange(result), cols), 'c', axis=0)  10.1 us
    ppermute x4, starting transfers between devices, ring(): before = lax.ppermute(before, 'x', onward)  7.65 us
  transfers between devices with their start and end apart: 10, of which 4 were waited for; matrix products, arithmetic and copies ran while one was open for 0% of the time, Pallas kernels for 3%

profile of v6, /device:TPU:1, one launch (start us, length us, event | category | flops | bytes accessed | tf_op | source)
XLA Modules:
  0.0 171.9 jit_solution(13609674254125604341)
XLA Ops:
  0.0 16.0 %collective-permute-start = (bf16[2048,256]{1,0:T(8,128)(2,1)}, bf16[2048,256]{1,0:T(8,128)(2,1)S(1)}, u32[]{:S(2)}, u32[]{:S(2)}) collective-permute-start(bf16[2048,256]{1,0:T(8,128)(2,1)} %bitcast.21), channel_id=1, source_target_pairs={{0,1},{1,0},{2,3},{3,2},{4,5},{5,4},{6,7},{7,6},{8,9},{9,8},{10,11... | collective-permute-start | bytes 3145736 | tf_op jit(solution)/shard_map/ppermute | solution.py:377
  16.0 1.9 %collective-permute-start.1 = (bf16[2048,256]{1,0:T(8,128)(2,1)}, bf16[2048,256]{1,0:T(8,128)(2,1)S(1)}, u32[]{:S(2)}, u32[]{:S(2)}) collective-permute-start(bf16[2048,256]{1,0:T(8,128)(2,1)} %bitcast.23), channel_id=1, source_target_pairs={{0,1},{1,0},{2,3},{3,2},{4,5},{5,4},{6,7},{7,6},{8,9},{9,8},{10,11... | collective-permute-start | bytes 3145736 | tf_op jit(solution)/shard_map/ppermute | solution.py:377
  18.0 2.4 %collective-permute-start.2 = (bf16[4096,128]{1,0:T(8,128)(2,1)}, bf16[4096,128]{1,0:T(8,128)(2,1)S(1)}, u32[]{:S(2)}, u32[]{:S(2)}) collective-permute-start(bf16[4096,128]{1,0:T(8,128)(2,1)} %bitcast.26), channel_id=1, source_target_pairs={{0,1},{1,0},{2,3},{3,2},{4,5},{5,4},{6,7},{7,6},{8,9},{9,8},{10,11... | collective-permute-start | bytes 3145736 | tf_op jit(solution)/shard_map/ppermute | solution.py:377
  20.4 0.9 prepare.1
  21.2 1.9 %all-gather = bf16[544,128]{1,0:T(8,128)(2,1)S(1)} all-gather(bf16[272,128]{1,0:T(8,128)(2,1)S(1)} %prepare.1), channel_id=2, replica_groups=mesh['ep'=64,'x'=8,'c'=2] {'c'}, dimensions={0}, use_global_device_ids=true | all-gather | bytes 208896 | tf_op jit(solution)/shard_map/all_gather | solution.py:406
  23.1 0.1 pad_add_fusion.refs_0_.place_ref
  23.2 1.8 %dispatch.1 = (bf16[512,256]{1,0:T(8,128)(2,1)S(1)}, f32[256,8]{1,0:T(8,128)}) custom-call(s32[2]{0:T(128)S(1)} %pad_add_fusion.refs_0_.place_ref, bf16[2,272,128]{2,1,0:T(8,128)(2,1)S(1)} %bitcast.16, s32[2,256]{1,0:T(2,128)} %bitcast.29, f32[2,256]{1,0:T(2,128)} %bitcast.30), custom_call_target="tpu_custom_call" | custom-call | tf_op jit(solution)/shard_map/dispatch/pallas_call | solution.py:97
  25.0 23.7 %all_to_all.20 = bf16[64,8,256]{2,1,0:T(8,128)(2,1)S(1)} all-to-all(bf16[64,8,256]{2,1,0:T(8,128)(2,1)S(1)} %bitcast.25), channel_id=1, replica_groups=mesh['ep'=64,'x'=8,'c'=2] {'ep'}, dimensions={0} | all-to-all | bytes 524288 | tf_op jit(solution)/shard_map/all_to_all | solution.py:368
  48.8 0.2 arrange.1
  49.0 0.0 copy-start
  49.0 0.0 copy-start.1
  49.1 39.1 %all_to_all.21.feat_ref = bf16[8,336,256]{2,1,0:T(8,128)(2,1)S(1)} all-to-all(bf16[8,336,256]{2,1,0:T(8,128)(2,1)S(1)} %arrange.1), channel_id=1, replica_groups=mesh['ep'=64,'x'=8,'c'=2] {'x'}, dimensions={0} | all-to-all | bytes 2752512 | tf_op jit(solution)/shard_map/all_to_all | solution.py:368
  88.2 3.3 %hidden.1.refs_1_ = bf16[320,512]{1,0:T(8,128)(2,1)S(1)} custom-call(s32[2]{0:T(128)S(1)} %pad_add_fusion.refs_0_.place_ref, bf16[8,336,256]{2,1,0:T(8,128)(2,1)S(1)} %all_to_all.21.feat_ref, bf16[2048,256]{1,0:T(8,128)(2,1)S(1)} %bitcast.22, bf16[2048,256]{1,0:T(8,128)(2,1)S(1)} %bitcast.24, bf16[2048,256]{1,0:T(8,128)(2,1)} %copy-done.4, ...), custom_call_target="tpu_custom_call" | custom-call | tf_op jit(solution)/shard_map/hidden/pallas_call | solution.py:191
  91.6 1.9 %collective-permute-start.3 = (bf16[320,512]{1,0:T(8,128)(2,1)S(1)}, bf16[320,512]{1,0:T(8,128)(2,1)S(1)}, u32[]{:S(2)}, u32[]{:S(2)}) collective-permute-start(bf16[320,512]{1,0:T(8,128)(2,1)S(1)} %hidden.1.refs_1_), channel_id=1, source_target_pairs={{0,2},{2,4},{4,6},{6,8},{8,10},{10,12},{12,14},{14,0},{1,3},{3,5},... | collective-permute-start | bytes 983048 | tf_op jit(solution)/shard_map/ppermute | solution.py:387
  93.5 4.6 %collective-permute-start.4 = (bf16[320,512]{1,0:T(8,128)(2,1)S(1)}, bf16[320,512]{1,0:T(8,128)(2,1)S(1)}, u32[]{:S(2)}, u32[]{:S(2)}) collective-permute-start(bf16[320,512]{1,0:T(8,128)(2,1)S(1)} %hidden.1.refs_1_), channel_id=1, source_target_pairs={{0,14},{2,0},{4,2},{6,4},{8,6},{10,8},{12,10},{14,12},{1,15},{3,1}... | collective-permute-start | bytes 983048 | tf_op jit(solution)/shard_map/ppermute | solution.py:390
  98.1 2.5 %collective-permute-done.3.refs_2_ = bf16[320,512]{1,0:T(8,128)(2,1)S(1)} collective-permute-done((bf16[320,512]{1,0:T(8,128)(2,1)S(1)}, bf16[320,512]{1,0:T(8,128)(2,1)S(1)}, u32[]{:S(2)}, u32[]{:S(2)}) %collective-permute-start.3) | collective-permute-done | bytes 327712 | tf_op jit(solution)/shard_map/ppermute | solution.py:387
  100.6 1.9 %collective-permute-start.5 = (bf16[320,512]{1,0:T(8,128)(2,1)S(1)}, bf16[320,512]{1,0:T(8,128)(2,1)S(1)}, u32[]{:S(2)}, u32[]{:S(2)}) collective-permute-start(bf16[320,512]{1,0:T(8,128)(2,1)S(1)} %collective-permute-done.3.refs_2_), channel_id=1, source_target_pairs={{0,2},{2,4},{4,6},{6,8},{8,10},{10,12},{12,14},{14,0},{1,3},{3,5},... | collective-permute-start | bytes 983048 | tf_op jit(solution)/shard_map/ppermute | solution.py:387
  102.5 4.6 %collective-permute-start.6 = (bf16[320,512]{1,0:T(8,128)(2,1)S(1)}, bf16[320,512]{1,0:T(8,128)(2,1)S(1)}, u32[]{:S(2)}, u32[]{:S(2)}) collective-permute-start(bf16[320,512]{1,0:T(8,128)(2,1)S(1)} %collective-permute-done.4.refs_3_), channel_id=1, source_target_pairs={{0,14},{2,0},{4,2},{6,4},{8,6},{10,8},{12,10},{14,12},{1,15},{3,1}... | collective-permute-start | bytes 983048 | tf_op jit(solution)/shard_map/ppermute | solution.py:390
  107.1 2.5 %collective-permute-done.5.refs_4_ = bf16[320,512]{1,0:T(8,128)(2,1)S(1)} collective-permute-done((bf16[320,512]{1,0:T(8,128)(2,1)S(1)}, bf16[320,512]{1,0:T(8,128)(2,1)S(1)}, u32[]{:S(2)}, u32[]{:S(2)}) %collective-permute-start.5) | collective-permute-done | bytes 327712 | tf_op jit(solution)/shard_map/ppermute | solution.py:387
  109.6 1.9 %collective-permute-start.7 = (bf16[320,512]{1,0:T(8,128)(2,1)S(1)}, bf16[320,512]{1,0:T(8,128)(2,1)S(1)}, u32[]{:S(2)}, u32[]{:S(2)}) collective-permute-start(bf16[320,512]{1,0:T(8,128)(2,1)S(1)} %collective-permute-done.5.refs_4_), channel_id=1, source_target_pairs={{0,2},{2,4},{4,6},{6,8},{8,10},{10,12},{12,14},{14,0},{1,3},{3,5},... | collective-permute-start | bytes 983048 | tf_op jit(solution)/shard_map/ppermute | solution.py:387
  111.6 4.6 %collective-permute-start.8 = (bf16[320,512]{1,0:T(8,128)(2,1)S(1)}, bf16[320,512]{1,0:T(8,128)(2,1)S(1)}, u32[]{:S(2)}, u32[]{:S(2)}) collective-permute-start(bf16[320,512]{1,0:T(8,128)(2,1)S(1)} %collective-permute-done.6.refs_5_), channel_id=1, source_target_pairs={{0,14},{2,0},{4,2},{6,4},{8,6},{10,8},{12,10},{14,12},{1,15},{3,1}... | collective-permute-start | bytes 983048 | tf_op jit(solution)/shard_map/ppermute | solution.py:390
  116.1 2.7 %collective-permute-done.7.refs_6_ = bf16[320,512]{1,0:T(8,128)(2,1)S(1)} collective-permute-done((bf16[320,512]{1,0:T(8,128)(2,1)S(1)}, bf16[320,512]{1,0:T(8,128)(2,1)S(1)}, u32[]{:S(2)}, u32[]{:S(2)}) %collective-permute-start.7) | collective-permute-done | bytes 327712 | tf_op jit(solution)/shard_map/ppermute | solution.py:387
  118.9 1.9 %collective-permute-start.9 = (bf16[320,512]{1,0:T(8,128)(2,1)S(1)}, bf16[320,512]{1,0:T(8,128)(2,1)S(1)}, u32[]{:S(2)}, u32[]{:S(2)}) collective-permute-start(bf16[320,512]{1,0:T(8,128)(2,1)S(1)} %collective-permute-done.7.refs_6_), channel_id=1, source_target_pairs={{0,2},{2,4},{4,6},{6,8},{8,10},{10,12},{12,14},{14,0},{1,3},{3,5},... | collective-permute-start | bytes 983048 | tf_op jit(solution)/shard_map/ppermute | solution.py:387
  120.8 2.7 %down_early.1.refs_1_ = f32[320,256]{1,0:T(8,128)S(1)} custom-call(s32[2]{0:T(128)S(1)} %pad_add_fusion.refs_0_.place_ref, bf16[320,512]{1,0:T(8,128)(2,1)S(1)} %hidden.1.refs_1_, bf16[320,512]{1,0:T(8,128)(2,1)S(1)} %collective-permute-done.3.refs_2_, bf16[320,512]{1,0:T(8,128)(2,1)S(1)} %collective-permute-done.4.refs_3_, ...), custom_call_target="tpu_custom_call" | custom-call | tf_op jit(solution)/shard_map/down_early/pallas_call | solution.py:234
  123.5 5.8 %collective-permute-done.9.refs_2_ = bf16[320,512]{1,0:T(8,128)(2,1)S(1)} collective-permute-done((bf16[320,512]{1,0:T(8,128)(2,1)S(1)}, bf16[320,512]{1,0:T(8,128)(2,1)S(1)}, u32[]{:S(2)}, u32[]{:S(2)}) %collective-permute-start.9) | collective-permute-done | bytes 327712 | tf_op jit(solution)/shard_map/ppermute | solution.py:387
  129.2 2.0 %down_last.1 = bf16[512,256]{1,0:T(8,128)(2,1)S(1)} custom-call(s32[2]{0:T(128)S(1)} %pad_add_fusion.refs_0_.place_ref, f32[320,256]{1,0:T(8,128)S(1)} %down_early.1.refs_1_, bf16[320,512]{1,0:T(8,128)(2,1)S(1)} %collective-permute-done.9.refs_2_, bf16[4096,128]{1,0:T(8,128)(2,1)} %bitcast.28, bf16[4096,128]{1,0:T(8,128)(2,1)} %copy-done.3), custom_call_target="tpu_custom_call" | custom-call | tf_op jit(solution)/shard_map/down_last/pallas_call | solution.py:271
  131.3 18.3 %all_to_all.22 = bf16[64,8,256]{2,1,0:T(8,128)(2,1)S(1)} all-to-all(bf16[64,8,256]{2,1,0:T(8,128)(2,1)S(1)} %bitcast.19), channel_id=1, replica_groups=mesh['ep'=64,'x'=8,'c'=2] {'ep'}, dimensions={0} | all-to-all | bytes 524288 | tf_op jit(solution)/shard_map/all_to_all | solution.py:368
  149.6 0.4 combine.1
  150.0 10.1 %all-gather.1 = f32[512,256]{1,0:T(8,128)S(1)} all-gather(f32[256,256]{1,0:T(8,128)S(1)} %combine.1), channel_id=3, replica_groups=mesh['ep'=64,'x'=8,'c'=2] {'c'}, dimensions={0}, use_global_device_ids=true | all-gather | bytes 786432 | tf_op jit(solution)/shard_map/all_gather | solution.py:425
  160.1 0.7 sums.1
  160.8 9.5 %all_to_all.23.sums_ref = f32[8,1,256]{2,1,0:T(1,128)S(1)} all-to-all(f32[8,1,256]{2,1,0:T(1,128)S(1)} %get-tuple-element.20), channel_id=1, replica_groups=mesh['ep'=64,'x'=8,'c'=2] {'x'}, dimensions={0} | all-to-all | bytes 16384 | tf_op jit(solution)/shard_map/all_to_all | solution.py:368
  170.3 1.6 final.1
  (16 shorter events, 0.0 us)
Async XLA Ops:
  0.0 48.8 %collective-permute-start = (bf16[2048,256]{1,0:T(8,128)(2,1)}, bf16[2048,256]{1,0:T(8,128)(2,1)S(1)}, u32[]{:S(2)}, u32[]{:S(2)}) collective-permute-start(bf16[2048,256]{1,0:T(8,128)(2,1)} %bitcast.21), channel_id=1, source_target_pairs={{0,1},{1,0},{2,3},{3,2},{4,5},{5,4},{6,7},{7,6},{8,9},{9,8},{10,11... | collective-permute-start | bytes 3145736 | tf_op jit(solution)/shard_map/ppermute | solution.py:377
  16.0 32.7 %collective-permute-start.1 = (bf16[2048,256]{1,0:T(8,128)(2,1)}, bf16[2048,256]{1,0:T(8,128)(2,1)S(1)}, u32[]{:S(2)}, u32[]{:S(2)}) collective-permute-start(bf16[2048,256]{1,0:T(8,128)(2,1)} %bitcast.23), channel_id=1, source_target_pairs={{0,1},{1,0},{2,3},{3,2},{4,5},{5,4},{6,7},{7,6},{8,9},{9,8},{10,11... | collective-permute-start | bytes 3145736 | tf_op jit(solution)/shard_map/ppermute | solution.py:377
  18.0 30.8 %collective-permute-start.2 = (bf16[4096,128]{1,0:T(8,128)(2,1)}, bf16[4096,128]{1,0:T(8,128)(2,1)S(1)}, u32[]{:S(2)}, u32[]{:S(2)}) collective-permute-start(bf16[4096,128]{1,0:T(8,128)(2,1)} %bitcast.26), channel_id=1, source_target_pairs={{0,1},{1,0},{2,3},{3,2},{4,5},{5,4},{6,7},{7,6},{8,9},{9,8},{10,11... | collective-permute-start | bytes 3145736 | tf_op jit(solution)/shard_map/ppermute | solution.py:377
  48.8 39.4 %copy-start.4 = (bf16[2048,256]{1,0:T(8,128)(2,1)}, bf16[2048,256]{1,0:T(8,128)(2,1)S(1)}, u32[]{:S(2)}) copy-start(bf16[2048,256]{1,0:T(8,128)(2,1)S(1)} %collective-permute-done.gate1_ref) | copy-start | bytes 3145732
  48.8 39.4 %copy-start.5 = (bf16[2048,256]{1,0:T(8,128)(2,1)}, bf16[2048,256]{1,0:T(8,128)(2,1)S(1)}, u32[]{:S(2)}) copy-start(bf16[2048,256]{1,0:T(8,128)(2,1)S(1)} %collective-permute-done.1.up1_ref) | copy-start | bytes 3145732
  48.8 39.4 %copy-start.3 = (bf16[4096,128]{1,0:T(8,128)(2,1)}, bf16[4096,128]{1,0:T(8,128)(2,1)S(1)}, u32[]{:S(2)}) copy-start(bf16[4096,128]{1,0:T(8,128)(2,1)S(1)} %collective-permute-done.2.refs_9_.refs_4_) | copy-start | bytes 3145732
  49.0 39.2 %copy-start = (bf16[1,2048,256]{2,1,0:T(8,128)(2,1)S(1)}, bf16[1,2048,256]{2,1,0:T(8,128)(2,1)}, u32[]{:S(2)}) copy-start(bf16[1,2048,256]{2,1,0:T(8,128)(2,1)} %param.13) | copy-start | bytes 3145732
  49.0 39.2 %copy-start.1 = (bf16[1,2048,256]{2,1,0:T(8,128)(2,1)S(1)}, bf16[1,2048,256]{2,1,0:T(8,128)(2,1)}, u32[]{:S(2)}) copy-start(bf16[1,2048,256]{2,1,0:T(8,128)(2,1)} %param.14) | copy-start | bytes 3145732
  91.6 9.0 %collective-permute-start.3 = (bf16[320,512]{1,0:T(8,128)(2,1)S(1)}, bf16[320,512]{1,0:T(8,128)(2,1)S(1)}, u32[]{:S(2)}, u32[]{:S(2)}) collective-permute-start(bf16[320,512]{1,0:T(8,128)(2,1)S(1)} %hidden.1.refs_1_), channel_id=1, source_target_pairs={{0,2},{2,4},{4,6},{6,8},{8,10},{10,12},{12,14},{14,0},{1,3},{3,5},... | collective-permute-start | bytes 983048 | tf_op jit(solution)/shard_map/ppermute | solution.py:387
  93.5 9.0 %collective-permute-start.4 = (bf16[320,512]{1,0:T(8,128)(2,1)S(1)}, bf16[320,512]{1,0:T(8,128)(2,1)S(1)}, u32[]{:S(2)}, u32[]{:S(2)}) collective-permute-start(bf16[320,512]{1,0:T(8,128)(2,1)S(1)} %hidden.1.refs_1_), channel_id=1, source_target_pairs={{0,14},{2,0},{4,2},{6,4},{8,6},{10,8},{12,10},{14,12},{1,15},{3,1}... | collective-permute-start | bytes 983048 | tf_op jit(solution)/shard_map/ppermute | solution.py:390
  100.6 9.0 %collective-permute-start.5 = (bf16[320,512]{1,0:T(8,128)(2,1)S(1)}, bf16[320,512]{1,0:T(8,128)(2,1)S(1)}, u32[]{:S(2)}, u32[]{:S(2)}) collective-permute-start(bf16[320,512]{1,0:T(8,128)(2,1)S(1)} %collective-permute-done.3.refs_2_), channel_id=1, source_target_pairs={{0,2},{2,4},{4,6},{6,8},{8,10},{10,12},{12,14},{14,0},{1,3},{3,5},... | collective-permute-start | bytes 983048 | tf_op jit(solution)/shard_map/ppermute | solution.py:387
  102.5 9.0 %collective-permute-start.6 = (bf16[320,512]{1,0:T(8,128)(2,1)S(1)}, bf16[320,512]{1,0:T(8,128)(2,1)S(1)}, u32[]{:S(2)}, u32[]{:S(2)}) collective-permute-start(bf16[320,512]{1,0:T(8,128)(2,1)S(1)} %collective-permute-done.4.refs_3_), channel_id=1, source_target_pairs={{0,14},{2,0},{4,2},{6,4},{8,6},{10,8},{12,10},{14,12},{1,15},{3,1}... | collective-permute-start | bytes 983048 | tf_op jit(solution)/shard_map/ppermute | solution.py:390
  109.6 9.2 %collective-permute-start.7 = (bf16[320,512]{1,0:T(8,128)(2,1)S(1)}, bf16[320,512]{1,0:T(8,128)(2,1)S(1)}, u32[]{:S(2)}, u32[]{:S(2)}) collective-permute-start(bf16[320,512]{1,0:T(8,128)(2,1)S(1)} %collective-permute-done.5.refs_4_), channel_id=1, source_target_pairs={{0,2},{2,4},{4,6},{6,8},{8,10},{10,12},{12,14},{14,0},{1,3},{3,5},... | collective-permute-start | bytes 983048 | tf_op jit(solution)/shard_map/ppermute | solution.py:387
  111.6 9.2 %collective-permute-start.8 = (bf16[320,512]{1,0:T(8,128)(2,1)S(1)}, bf16[320,512]{1,0:T(8,128)(2,1)S(1)}, u32[]{:S(2)}, u32[]{:S(2)}) collective-permute-start(bf16[320,512]{1,0:T(8,128)(2,1)S(1)} %collective-permute-done.6.refs_5_), channel_id=1, source_target_pairs={{0,14},{2,0},{4,2},{6,4},{8,6},{10,8},{12,10},{14,12},{1,15},{3,1}... | collective-permute-start | bytes 983048 | tf_op jit(solution)/shard_map/ppermute | solution.py:390
  118.9 10.4 %collective-permute-start.9 = (bf16[320,512]{1,0:T(8,128)(2,1)S(1)}, bf16[320,512]{1,0:T(8,128)(2,1)S(1)}, u32[]{:S(2)}, u32[]{:S(2)}) collective-permute-start(bf16[320,512]{1,0:T(8,128)(2,1)S(1)} %collective-permute-done.7.refs_6_), channel_id=1, source_target_pairs={{0,2},{2,4},{4,6},{6,8},{8,10},{10,12},{12,14},{14,0},{1,3},{3,5},... | collective-permute-start | bytes 983048 | tf_op jit(solution)/shard_map/ppermute | solution.py:387
  123.5 26.1 %copy-start.2 = (f32[256,8]{1,0:T(8,128)S(1)}, f32[256,8]{1,0:T(8,128)}, u32[]{:S(2)}) copy-start(f32[256,8]{1,0:T(8,128)} %get-tuple-element.18.cols_ref) | copy-start | bytes 24580

commit v7 on v6

--- a/solution.py
+++ b/solution.py
@@ -119,24 +119,21 @@
     step = GROUP * half
     width = tok_ref.shape[2]
     first = tok_ref.shape[1] - EXTRA
-    chips, rows, _ = out_ref.shape
+    rows, _ = out_ref.shape
     place = packed_place((step, GROUP * PAD), 1, half)
     for g in range(arrived_ref.shape[0] // (GROUP * PAD)):
-        packed = jnp.dot(
+        out_ref[g * step : (g + 1) * step, :] = jnp.dot(
             place,
             arrived_ref[g * GROUP * PAD : (g + 1) * GROUP * PAD, :],
             preferred_element_type=jnp.float32,
         ).astype(jnp.bfloat16)
-        for j in range(chips):
-            out_ref[j, g * step : (g + 1) * step, :] = packed
-    for j in range(chips):
-        for c in range(CORES):
-            out_ref[j, rows - EXTRA :, c * width : (c + 1) * width] = tok_ref[
-                c, first : first + EXTRA, :
-            ]
-
-
-def arrange(arrived, tokens, chips, half):
+    for c in range(CORES):
+        out_ref[rows - EXTRA :, c * width : (c + 1) * width] = tok_ref[
+            c, first : first + EXTRA, :
+        ]
+
+
+def arrange(arrived, tokens, half):
     blocks = arrived.shape[0] // PAD
     width = arrived.shape[1]
 
@@ -145,38 +142,89 @@
 
     return pl.pallas_call(
         body,
-        out_shape=jax.ShapeDtypeStruct((chips, blocks * half + EXTRA, width), jnp.bfloat16),
+        out_shape=jax.ShapeDtypeStruct((blocks * half + EXTRA, width), jnp.bfloat16),
         compiler_params=params(8),
         name="arrange",
     )(arrived, tokens)
 
 
-def hidden_kernel(
-    place_ref, feat_ref, gate0_ref, up0_ref, gate1_ref, up1_ref, out_ref, normed_ref
-):
-    chips, rows, wide = feat_ref.shape
+def gained(feat_ref):
+    rows = feat_ref.shape[0] - EXTRA
+    pieces = feat_ref[rows:, :].astype(jnp.float32)
+    gain = pieces[0:1, :] + pieces[1:2, :] + pieces[2:3, :]
+    part = feat_ref[0:rows, :].astype(jnp.float32)
+    return (part * gain).astype(jnp.bfloat16), part * part
+
+
+def chip_at(place_ref, offset, chips):
+    return lax.rem(place_ref[0] + (offset + chips), chips)
+
+
+def gate_early_kernel(*refs, offsets, last, chips):
+    count = len(offsets)
+    place_ref, *rest = refs
+    feat_refs, weight_refs = rest[:count], rest[count : count + 4]
+    total_refs, (squares_ref, rows_ref) = rest[count + 4 : count + 8], rest[count + 8 :]
+    wide = feat_refs[0].shape[1]
+    totals = [jnp.zeros(ref.shape, jnp.float32) for ref in total_refs]
+    squares = jnp.zeros(squares_ref.shape, jnp.float32)
+    for offset, feat_ref in zip(offsets, feat_refs):
+        begin = pl.multiple_of(chip_at(place_ref, offset, chips) * wide, wide)
+        part, square = gained(feat_ref)
+        squares = squares + square
+        for i, weight_ref in enumerate(weight_refs):
+            totals[i] = totals[i] + jnp.dot(
+                part, weight_ref[pl.ds(begin, wide), :], preferred_element_type=jnp.float32
+            )
+    for i, total in enumerate(totals):
+        total_refs[i][...] = total
+    squares_ref[...] = squares
+    begin = pl.multiple_of(chip_at(place_ref, last, chips) * wide, wide)
+    for i, weight_ref in enumerate(weight_refs):
+        rows_ref[i] = weight_ref[pl.ds(begin, wide), :]
+
+
+def gate_early(place, features, last, weights, chips):
+    offsets = [offset for offset, _ in features]
+    arrays = [array for _, array in features]
+    rows, wide = arrays[0].shape
     rows = rows - EXTRA
-    full = chips * wide
-    units = gate0_ref.shape[1]
-    total = jnp.zeros((rows, wide), jnp.float32)
-    for j in range(chips):
-        part = feat_ref[j, 0:rows, :].astype(jnp.float32)
-        total = total + part * part
-    scale = lax.rsqrt(jnp.sum(total, axis=1, keepdims=True) / full + epsilon)
-    for j in range(chips):
-        pieces = feat_ref[j, rows : rows + EXTRA, :].astype(jnp.float32)
-        gain = pieces[0:1, :] + pieces[1:2, :] + pieces[2:3, :]
-        part = feat_ref[j, 0:rows, :].astype(jnp.float32)
-        normed_ref[:, j * wide : (j + 1) * wide] = (part * scale * gain).astype(jnp.bfloat16)
-
-    def hidden_of(gate_ref, up_ref):
-        normed = normed_ref[...]
-        gate = jnp.dot(normed, gate_ref[...], preferred_element_type=jnp.float32)
-        upper = jnp.dot(normed, up_ref[...], preferred_element_type=jnp.float32)
+    units = weights[0].shape[1]
+
+    def body(*refs):
+        gate_early_kernel(*refs, offsets=offsets, last=last, chips=chips)
+
+    total = jax.ShapeDtypeStruct((rows, units), jnp.float32)
+    return pl.pallas_call(
+        body,
+        in_specs=[whole(pltpu.SMEM)] + [whole()] * (len(arrays) + 4),
+        out_shape=(
+            *[total] * 4,
+            jax.ShapeDtypeStruct((rows, wide), jnp.float32),
+            jax.ShapeDtypeStruct((4, wide, units), jnp.bfloat16),
+        ),
+        compiler_params=params(16),
+        name="gate_early",
+    )(place, *arrays, *weights)
+
+
+def gate_last_kernel(place_ref, *refs, chips):
+    total_refs, (squares_ref, rows_ref, feat_ref, out_ref) = refs[:4], refs[4:]
+    units = rows_ref.shape[2]
+    part, square = gained(feat_ref)
+    square = squares_ref[...] + square
+    full = chips * square.shape[1]
+    scale = lax.rsqrt(jnp.sum(square, axis=1, keepdims=True) / full + epsilon)
+    totals = [
+        scale * (ref[...] + jnp.dot(part, rows_ref[i], preferred_element_type=jnp.float32))
+        for i, ref in enumerate(total_refs)
+    ]
+
+    def hidden_of(gate, upper):
         return (gate / (1.0 + jnp.exp(-gate)) * upper).astype(jnp.bfloat16)
 
-    own = hidden_of(gate0_ref, up0_ref)
-    other = hidden_of(gate1_ref, up1_ref)
+    own = hidden_of(totals[0], totals[1])
+    other = hidden_of(totals[2], totals[3])
     for c in range(CORES):
 
         @pl.when(place_ref[1] == c)
@@ -185,17 +233,19 @@
             out_ref[:, (1 - c) * units : (2 - c) * units] = other
 
 
-def hidden_of(place, features, gate0, up0, gate1, up1):
-    chips, rows, wide = features.shape
-    units = gate0.shape[1]
-    return pl.pallas_call(
-        hidden_kernel,
-        in_specs=[whole(pltpu.SMEM)] + [whole()] * 5,
-        out_shape=jax.ShapeDtypeStruct((rows - EXTRA, CORES * units), jnp.bfloat16),
-        scratch_shapes=[pltpu.VMEM((rows - EXTRA, chips * wide), jnp.bfloat16)],
-        compiler_params=params(24),
-        name="hidden",
-    )(place, features, gate0, up0, gate1, up1)
+def gate_last(place, early, feature, chips):
+    rows, units = early[0].shape
+
+    def body(*refs):
+        gate_last_kernel(*refs, chips=chips)
+
+    return pl.pallas_call(
+        body,
+        in_specs=[whole(pltpu.SMEM)] + [whole()] * 7,
+        out_shape=jax.ShapeDtypeStruct((rows, CORES * units), jnp.bfloat16),
+        compiler_params=params(16),
+        name="gate_last",
+    )(place, *early, feature)
 
 
 def both_columns(place_ref, down0_ref, down1_ref, down_ref):
@@ -208,45 +258,46 @@
             down_ref[:, (1 - c) * width : (2 - c) * width] = down1_ref[...]
 
 
-def down_early_kernel(*refs, offsets, chips):
-    place_ref, *hidden_refs, down0_ref, down1_ref, out_ref, down_ref = refs
+def down_early_kernel(*refs, offsets, last, chips):
+    place_ref, *hidden_refs, down0_ref, down1_ref, out_ref, rows_ref, down_ref = refs
     _, units = hidden_refs[0].shape
     both_columns(place_ref, down0_ref, down1_ref, down_ref)
     total = jnp.zeros(out_ref.shape, jnp.float32)
     for offset, ref in zip(offsets, hidden_refs):
-        chip = lax.rem(place_ref[0] + (offset + chips), chips)
-        begin = pl.multiple_of(chip * units, units)
+        begin = pl.multiple_of(chip_at(place_ref, offset, chips) * units, units)
         total = total + jnp.dot(
             ref[...], down_ref[pl.ds(begin, units), :], preferred_element_type=jnp.float32
         )
     out_ref[...] = total
-
-
-def down_early(place, hiddens, down0, down1, chips):
+    begin = pl.multiple_of(chip_at(place_ref, last, chips) * units, units)
+    rows_ref[...] = down_ref[pl.ds(begin, units), :]
+
+
+def down_early(place, hiddens, last, down0, down1, chips):
     offsets = [offset for offset, _ in hiddens]
     arrays = [array for _, array in hiddens]
-    rows = arrays[0].shape[0]
+    rows, units = arrays[0].shape
     full, width = down0.shape
 
     def body(*refs):
-        down_early_kernel(*refs, offsets=offsets, chips=chips)
+        down_early_kernel(*refs, offsets=offsets, last=last, chips=chips)
 
     return pl.pallas_call(
         body,
         in_specs=[whole(pltpu.SMEM)] + [whole()] * (len(arrays) + 2),
-        out_shape=jax.ShapeDtypeStruct((rows, CORES * width), jnp.float32),
+        out_shape=(
+            jax.ShapeDtypeStruct((rows, CORES * width), jnp.float32),
+            jax.ShapeDtypeStruct((units, CORES * width), jnp.bfloat16),
+        ),
         scratch_shapes=[pltpu.VMEM((full, CORES * width), jnp.bfloat16)],
         compiler_params=params(16),
         name="down_early",
     )(place, *arrays, down0, down1)
 
 
-def down_last_kernel(
-    place_ref, total_ref, hidden_ref, down0_ref, down1_ref, out_ref, down_ref, result_ref, *, half
-):
-    both_columns(place_ref, down0_ref, down1_ref, down_ref)
+def down_last_kernel(total_ref, rows_ref, hidden_ref, out_ref, result_ref, *, half):
     total = total_ref[...] + jnp.dot(
-        hidden_ref[...], down_ref[...], preferred_element_type=jnp.float32
+        hidden_ref[...], rows_ref[...], preferred_element_type=jnp.float32
     )
     result_ref[...] = total.astype(jnp.bfloat16)
     step = GROUP * half
@@ -257,38 +308,19 @@
         ).astype(jnp.bfloat16)
 
 
-def down_last(place, total, last, down0, down1, chips, half):
-    offset, hidden = last
-    rows, units = hidden.shape
-    _, width = down0.shape
+def down_last(early, hidden, half):
+    rows, wide = early[0].shape
 
     def body(*refs):
         down_last_kernel(*refs, half=half)
 
-    def chip_rows(place_ref):
-        return lax.rem(place_ref[0] + (offset + chips), chips)
-
-    return pl.pallas_call(
-        body,
-        grid_spec=pltpu.PrefetchScalarGridSpec(
-            num_scalar_prefetch=1,
-            grid=(1,),
-            in_specs=[
-                pl.BlockSpec((rows, CORES * width), lambda i, p: (0, 0)),
-                pl.BlockSpec((rows, units), lambda i, p: (0, 0)),
-                pl.BlockSpec((units, width), lambda i, p: (chip_rows(p), 0)),
-                pl.BlockSpec((units, width), lambda i, p: (chip_rows(p), 0)),
-            ],
-            out_specs=pl.BlockSpec((rows // half * PAD, CORES * width), lambda i, p: (0, 0)),
-            scratch_shapes=[
-                pltpu.VMEM((units, CORES * width), jnp.bfloat16),
-                pltpu.VMEM((rows, CORES * width), jnp.bfloat16),
-            ],
-        ),
-        out_shape=jax.ShapeDtypeStruct((rows // half * PAD, CORES * width), jnp.bfloat16),
+    return pl.pallas_call(
+        body,
+        out_shape=jax.ShapeDtypeStruct((rows // half * PAD, wide), jnp.bfloat16),
+        scratch_shapes=[pltpu.VMEM((rows, wide), jnp.bfloat16)],
         compiler_params=params(8),
         name="down_last",
-    )(place, total, hidden, down0, down1)
+    )(*early, hidden)
 
 
 def combine_kernel(returned_ref, cols_ref, mixed_ref):
@@ -417,11 +449,12 @@
     for weight in (gate0, up0, down0):
         swapped.append(swap(weight))
     arrived, gate1, up1, down1 = lax.optimization_barrier((arrived, *swapped))
-    features = exchange(arrange(arrived, both, chips, half), "x")
-    hidden = hidden_of(place, features, gate0, up0, in_hbm(gate1), in_hbm(up1))
-    *early, last = ring(hidden)
-    total = down_early(place, early, in_hbm(down0), in_hbm(down1), chips)
-    result = down_last(place, total, last, in_hbm(down0), in_hbm(down1), chips, half)
+    *early, (last, feature) = ring(arrange(arrived, both, half))
+    weights = (gate0, up0, in_hbm(gate1), in_hbm(up1))
+    projected = gate_early(place, early, last, weights, chips)
+    *early, (last, hidden) = ring(gate_last(place, projected, feature, chips))
+    summed = down_early(place, early, last, in_hbm(down0), in_hbm(down1), chips)
+    result = down_last(summed, hidden, half)
     mixed = lax.all_gather(combine(blocks_exchange(result), cols), "c", axis=0)
     mixed, sums = sums_of(place, mixed, chips)
     sums = exchange(sums, "x")

time: 173 us -> 171 us (0.988)
  blocking collectives: 103 us -> 69.2 us
  starting transfers between devices: 41.7 us -> 63.2 us
  waiting for transfers between devices: 13.5 us -> 23.9 us
    all_to_all x4 -> x3, blocking collectives: 90.6 us -> 53 us  [exchange(): return lax.all_to_all(value, axis, split_axis=0, concat_axis=0, tiled=True)]
    ppermute x3 -> x6, starting transfers between devices: 13.7 us -> 26.2 us  [ring(): after = lax.ppermute(after, 'x', backward)]
    ppermute x4 -> x8, waiting for transfers between devices: 13.5 us -> 23.4 us  [ring(): before = lax.ppermute(before, 'x', onward)]
    ppermute x4 -> x8, starting transfers between devices: 7.65 us -> 16.5 us  [ring(): before = lax.ppermute(before, 'x', onward)]
    all_gather x1, blocking collectives: 10.1 us -> 14.3 us  [layer(): mixed = lax.all_gather(combine(blocks_exchange(result), cols), 'c', axis=0)]
    pallas_call x3 -> x4, Pallas kernels: 5.63 us -> 4.68 us  [the longest x1 2.97 us: gate_early(): pl.pallas_call(body, in_specs=[whole(pltpu.SMEM)] + [whole()] * (len(arra...]
  transfers between devices with their start and end apart: 10 -> 17, of which waited for: 4 -> 10; matrix products, arithmetic and copies ran while one was open for 0% -> 0% of each run, Pallas kernels for 3% -> 5%
where the time goes in v7:
time: 171 us; the launch traced here: 170 us
  blocking collectives  69.2 us (40%)
  starting transfers between devices  63.2 us (37%)
  waiting for transfers between devices  23.9 us (14%)
  Pallas kernels  12.6 us (7%)
    all_to_all x3, blocking collectives, exchange(): return lax.all_to_all(value, axis, split_axis=0, concat_axis=0, tiled=True)  53 us
    ppermute x6, starting transfers between devices, ring(): after = lax.ppermute(after, 'x', backward)  26.2 us
    ppermute x8, waiting for transfers between devices, ring(): before = lax.ppermute(before, 'x', onward)  23.4 us
    ppermute x3, starting transfers between devices, swap(): return lax.ppermute(value, 'c', [(0, 1), (1, 0)])  20.5 us
    ppermute x8, starting transfers between devices, ring(): before = lax.ppermute(before, 'x', onward)  16.5 us
    all_gather x1, blocking collectives, layer(): mixed = lax.all_gather(combine(blocks_exchange(result), cols), 'c', axis=0)  14.3 us
  transfers between devices with their start and end apart: 17, of which 10 were waited for; matrix products, arithmetic and copies ran while one was open for 0% of the time, Pallas kernels for 5%

profile of v7, /device:TPU:1, one launch (start us, length us, event | category | flops | bytes accessed | tf_op | source)
XLA Modules:
  0.0 170.5 jit_solution(2774475406694371807)
XLA Ops:
  0.0 16.1 %collective-permute-start = (bf16[2048,256]{1,0:T(8,128)(2,1)}, bf16[2048,256]{1,0:T(8,128)(2,1)S(1)}, u32[]{:S(2)}, u32[]{:S(2)}) collective-permute-start(bf16[2048,256]{1,0:T(8,128)(2,1)} %bitcast.21), channel_id=1, source_target_pairs={{0,1},{1,0},{2,3},{3,2},{4,5},{5,4},{6,7},{7,6},{8,9},{9,8},{10,11... | collective-permute-start | bytes 3145736 | tf_op jit(solution)/shard_map/ppermute | solution.py:409
  16.2 1.9 %collective-permute-start.1 = (bf16[2048,256]{1,0:T(8,128)(2,1)}, bf16[2048,256]{1,0:T(8,128)(2,1)}, u32[]{:S(2)}, u32[]{:S(2)}) collective-permute-start(bf16[2048,256]{1,0:T(8,128)(2,1)} %bitcast.23), channel_id=1, source_target_pairs={{0,1},{1,0},{2,3},{3,2},{4,5},{5,4},{6,7},{7,6},{8,9},{9,8},{10,11... | collective-permute-start | bytes 3145736 | tf_op jit(solution)/shard_map/ppermute | solution.py:409
  18.1 2.4 %collective-permute-start.2 = (bf16[4096,128]{1,0:T(8,128)(2,1)}, bf16[4096,128]{1,0:T(8,128)(2,1)S(1)}, u32[]{:S(2)}, u32[]{:S(2)}) collective-permute-start(bf16[4096,128]{1,0:T(8,128)(2,1)} %bitcast.26), channel_id=1, source_target_pairs={{0,1},{1,0},{2,3},{3,2},{4,5},{5,4},{6,7},{7,6},{8,9},{9,8},{10,11... | collective-permute-start | bytes 3145736 | tf_op jit(solution)/shard_map/ppermute | solution.py:409
  21.4 1.9 %all-gather = bf16[544,128]{1,0:T(8,128)(2,1)S(1)} all-gather(bf16[272,128]{1,0:T(8,128)(2,1)S(1)} %prepare.1), channel_id=2, replica_groups=mesh['ep'=64,'x'=8,'c'=2] {'c'}, dimensions={0}, use_global_device_ids=true | all-gather | bytes 208896 | tf_op jit(solution)/shard_map/all_gather | solution.py:438
  23.3 1.8 %dispatch.1 = (bf16[512,256]{1,0:T(8,128)(2,1)S(1)}, f32[256,8]{1,0:T(8,128)}) custom-call(s32[2]{0:T(128)S(1)} %pad_add_fusion.refs_0_.place_ref, bf16[2,272,128]{2,1,0:T(8,128)(2,1)S(1)} %bitcast.16, s32[2,256]{1,0:T(2,128)} %bitcast.28, f32[2,256]{1,0:T(2,128)} %bitcast.29), custom_call_target="tpu_custom_call" | custom-call | tf_op jit(solution)/shard_map/dispatch/pallas_call | solution.py:97
  25.1 23.7 %all_to_all.15 = bf16[64,8,256]{2,1,0:T(8,128)(2,1)S(1)} all-to-all(bf16[64,8,256]{2,1,0:T(8,128)(2,1)S(1)} %bitcast.25), channel_id=1, replica_groups=mesh['ep'=64,'x'=8,'c'=2] {'ep'}, dimensions={0} | all-to-all | bytes 524288 | tf_op jit(solution)/shard_map/all_to_all | solution.py:400
  49.1 3.1 %collective-permute-start.3 = (bf16[336,256]{1,0:T(8,128)(2,1)S(1)}, bf16[336,256]{1,0:T(8,128)(2,1)S(1)}, u32[]{:S(2)}, u32[]{:S(2)}) collective-permute-start(bf16[336,256]{1,0:T(8,128)(2,1)S(1)} %arrange.1.refs_1_), channel_id=1, source_target_pairs={{0,2},{2,4},{4,6},{6,8},{8,10},{10,12},{12,14},{14,0},{1,3},{3,5},... | collective-permute-start | bytes 516104 | tf_op jit(solution)/shard_map/ppermute | solution.py:419
  52.2 3.4 %collective-permute-start.4 = (bf16[336,256]{1,0:T(8,128)(2,1)S(1)}, bf16[336,256]{1,0:T(8,128)(2,1)S(1)}, u32[]{:S(2)}, u32[]{:S(2)}) collective-permute-start(bf16[336,256]{1,0:T(8,128)(2,1)S(1)} %arrange.1.refs_1_), channel_id=1, source_target_pairs={{0,14},{2,0},{4,2},{6,4},{8,6},{10,8},{12,10},{14,12},{1,15},{3,1}... | collective-permute-start | bytes 516104 | tf_op jit(solution)/shard_map/ppermute | solution.py:422
  56.4 1.9 %collective-permute-start.5 = (bf16[336,256]{1,0:T(8,128)(2,1)S(1)}, bf16[336,256]{1,0:T(8,128)(2,1)S(1)}, u32[]{:S(2)}, u32[]{:S(2)}) collective-permute-start(bf16[336,256]{1,0:T(8,128)(2,1)S(1)} %collective-permute-done.3.refs_2_), channel_id=1, source_target_pairs={{0,2},{2,4},{4,6},{6,8},{8,10},{10,12},{12,14},{14,0},{1,3},{3,5},... | collective-permute-start | bytes 516104 | tf_op jit(solution)/shard_map/ppermute | solution.py:419
  58.7 4.3 %collective-permute-start.6 = (bf16[336,256]{1,0:T(8,128)(2,1)S(1)}, bf16[336,256]{1,0:T(8,128)(2,1)S(1)}, u32[]{:S(2)}, u32[]{:S(2)}) collective-permute-start(bf16[336,256]{1,0:T(8,128)(2,1)S(1)} %collective-permute-done.4.refs_3_), channel_id=1, source_target_pairs={{0,14},{2,0},{4,2},{6,4},{8,6},{10,8},{12,10},{14,12},{1,15},{3,1}... | collective-permute-start | bytes 516104 | tf_op jit(solution)/shard_map/ppermute | solution.py:422
  63.8 1.9 %collective-permute-start.7 = (bf16[336,256]{1,0:T(8,128)(2,1)S(1)}, bf16[336,256]{1,0:T(8,128)(2,1)S(1)}, u32[]{:S(2)}, u32[]{:S(2)}) collective-permute-start(bf16[336,256]{1,0:T(8,128)(2,1)S(1)} %collective-permute-done.5.refs_4_), channel_id=1, source_target_pairs={{0,2},{2,4},{4,6},{6,8},{8,10},{10,12},{12,14},{14,0},{1,3},{3,5},... | collective-permute-start | bytes 516104 | tf_op jit(solution)/shard_map/ppermute | solution.py:419
  65.7 4.6 %collective-permute-start.8 = (bf16[336,256]{1,0:T(8,128)(2,1)S(1)}, bf16[336,256]{1,0:T(8,128)(2,1)S(1)}, u32[]{:S(2)}, u32[]{:S(2)}) collective-permute-start(bf16[336,256]{1,0:T(8,128)(2,1)S(1)} %collective-permute-done.6.refs_5_), channel_id=1, source_target_pairs={{0,14},{2,0},{4,2},{6,4},{8,6},{10,8},{12,10},{14,12},{1,15},{3,1}... | collective-permute-start | bytes 516104 | tf_op jit(solution)/shard_map/ppermute | solution.py:422
  71.1 1.9 %collective-permute-start.9 = (bf16[336,256]{1,0:T(8,128)(2,1)S(1)}, bf16[336,256]{1,0:T(8,128)(2,1)S(1)}, u32[]{:S(2)}, u32[]{:S(2)}) collective-permute-start(bf16[336,256]{1,0:T(8,128)(2,1)S(1)} %collective-permute-done.7.refs_6_), channel_id=1, source_target_pairs={{0,2},{2,4},{4,6},{6,8},{8,10},{10,12},{12,14},{14,0},{1,3},{3,5},... | collective-permute-start | bytes 516104 | tf_op jit(solution)/shard_map/ppermute | solution.py:419
  73.1 1.2 copy-done.1
  74.3 3.0 %gate_early.1 = (f32[320,256]{1,0:T(8,128)S(1)}, f32[320,256]{1,0:T(8,128)S(1)}, f32[320,256]{1,0:T(8,128)S(1)}, f32[320,256]{1,0:T(8,128)S(1)}, f32[320,256]{1,...) custom-call(s32[2]{0:T(128)S(1)} %pad_add_fusion.refs_0_.place_ref, bf16[336,256]{1,0:T(8,128)(2,1)S(1)} %arrange.1.refs_1_, ...), custom_call_target="tpu_custom_call" | custom-call | tf_op jit(solution)/shard_map/gate_early/pallas_call | solution.py:198
  77.3 1.2 collective-permute-done.9.refs_7_
  79.5 1.9 %collective-permute-start.10 = (bf16[320,512]{1,0:T(8,128)(2,1)S(1)}, bf16[320,512]{1,0:T(8,128)(2,1)S(1)}, u32[]{:S(2)}, u32[]{:S(2)}) collective-permute-start(bf16[320,512]{1,0:T(8,128)(2,1)S(1)} %gate_last.1.refs_1_), channel_id=1, source_target_pairs={{0,2},{2,4},{4,6},{6,8},{8,10},{10,12},{12,14},{14,0},{1,3},{3,5},... | collective-permute-start | bytes 983048 | tf_op jit(solution)/shard_map/ppermute | solution.py:419
  81.5 4.6 %collective-permute-start.11 = (bf16[320,512]{1,0:T(8,128)(2,1)S(1)}, bf16[320,512]{1,0:T(8,128)(2,1)S(1)}, u32[]{:S(2)}, u32[]{:S(2)}) collective-permute-start(bf16[320,512]{1,0:T(8,128)(2,1)S(1)} %gate_last.1.refs_1_), channel_id=1, source_target_pairs={{0,14},{2,0},{4,2},{6,4},{8,6},{10,8},{12,10},{14,12},{1,15},{3,1}... | collective-permute-start | bytes 983048 | tf_op jit(solution)/shard_map/ppermute | solution.py:422
  86.0 2.5 %collective-permute-done.10.refs_2_ = bf16[320,512]{1,0:T(8,128)(2,1)S(1)} collective-permute-done((bf16[320,512]{1,0:T(8,128)(2,1)S(1)}, bf16[320,512]{1,0:T(8,128)(2,1)S(1)}, u32[]{:S(2)}, u32[]{:S(2)}) %collective-permute-start.10) | collective-permute-done | bytes 327712 | tf_op jit(solution)/shard_map/ppermute | solution.py:419
  88.6 1.9 %collective-permute-start.12 = (bf16[320,512]{1,0:T(8,128)(2,1)S(1)}, bf16[320,512]{1,0:T(8,128)(2,1)S(1)}, u32[]{:S(2)}, u32[]{:S(2)}) collective-permute-start(bf16[320,512]{1,0:T(8,128)(2,1)S(1)} %collective-permute-done.10.refs_2_), channel_id=1, source_target_pairs={{0,2},{2,4},{4,6},{6,8},{8,10},{10,12},{12,14},{14,0},{1,3},{3,5},... | collective-permute-start | bytes 983048 | tf_op jit(solution)/shard_map/ppermute | solution.py:419
  90.5 4.6 %collective-permute-start.13 = (bf16[320,512]{1,0:T(8,128)(2,1)S(1)}, bf16[320,512]{1,0:T(8,128)(2,1)S(1)}, u32[]{:S(2)}, u32[]{:S(2)}) collective-permute-start(bf16[320,512]{1,0:T(8,128)(2,1)S(1)} %collective-permute-done.11.refs_3_), channel_id=1, source_target_pairs={{0,14},{2,0},{4,2},{6,4},{8,6},{10,8},{12,10},{14,12},{1,15},{3,1}... | collective-permute-start | bytes 983048 | tf_op jit(solution)/shard_map/ppermute | solution.py:422
  95.1 4.5 %collective-permute-done.12.refs_4_ = bf16[320,512]{1,0:T(8,128)(2,1)S(1)} collective-permute-done((bf16[320,512]{1,0:T(8,128)(2,1)S(1)}, bf16[320,512]{1,0:T(8,128)(2,1)S(1)}, u32[]{:S(2)}, u32[]{:S(2)}) %collective-permute-start.12) | collective-permute-done | bytes 327712 | tf_op jit(solution)/shard_map/ppermute | solution.py:419
  99.6 1.9 %collective-permute-start.14 = (bf16[320,512]{1,0:T(8,128)(2,1)S(1)}, bf16[320,512]{1,0:T(8,128)(2,1)S(1)}, u32[]{:S(2)}, u32[]{:S(2)}) collective-permute-start(bf16[320,512]{1,0:T(8,128)(2,1)S(1)} %collective-permute-done.12.refs_4_), channel_id=1, source_target_pairs={{0,2},{2,4},{4,6},{6,8},{8,10},{10,12},{12,14},{14,0},{1,3},{3,5},... | collective-permute-start | bytes 983048 | tf_op jit(solution)/shard_map/ppermute | solution.py:419
  101.5 4.8 %collective-permute-start.15 = (bf16[320,512]{1,0:T(8,128)(2,1)S(1)}, bf16[320,512]{1,0:T(8,128)(2,1)S(1)}, u32[]{:S(2)}, u32[]{:S(2)}) collective-permute-start(bf16[320,512]{1,0:T(8,128)(2,1)S(1)} %collective-permute-done.13.refs_5_), channel_id=1, source_target_pairs={{0,14},{2,0},{4,2},{6,4},{8,6},{10,8},{12,10},{14,12},{1,15},{3,1}... | collective-permute-start | bytes 983048 | tf_op jit(solution)/shard_map/ppermute | solution.py:422
  106.4 5.4 %collective-permute-done.14.refs_6_ = bf16[320,512]{1,0:T(8,128)(2,1)S(1)} collective-permute-done((bf16[320,512]{1,0:T(8,128)(2,1)S(1)}, bf16[320,512]{1,0:T(8,128)(2,1)S(1)}, u32[]{:S(2)}, u32[]{:S(2)}) %collective-permute-start.14) | collective-permute-done | bytes 327712 | tf_op jit(solution)/shard_map/ppermute | solution.py:419
  111.7 1.9 %collective-permute-start.16 = (bf16[320,512]{1,0:T(8,128)(2,1)S(1)}, bf16[320,512]{1,0:T(8,128)(2,1)S(1)}, u32[]{:S(2)}, u32[]{:S(2)}) collective-permute-start(bf16[320,512]{1,0:T(8,128)(2,1)S(1)} %collective-permute-done.14.refs_6_), channel_id=1, source_target_pairs={{0,2},{2,4},{4,6},{6,8},{8,10},{10,12},{12,14},{14,0},{1,3},{3,5},... | collective-permute-start | bytes 983048 | tf_op jit(solution)/shard_map/ppermute | solution.py:419
  113.9 2.7 %down_early.1 = (f32[320,256]{1,0:T(8,128)S(1)}, bf16[512,256]{1,0:T(8,128)(2,1)S(1)}) custom-call(s32[2]{0:T(128)S(1)} %pad_add_fusion.refs_0_.place_ref, bf16[320,512]{1,0:T(8,128)(2,1)S(1)} %gate_last.1.refs_1_, bf16[320,512]{1,0:T(8,128)(2,1)S(1)} %collective-permute-done.10.refs_2_, bf16[320,512]{1,0:T(8,128)(2,1)S(1)} %collective-permute-done.11.refs_3_, ...), custom_call_target="tpu_custom_call" | custom-call | tf_op jit(solution)/shard_map/down_early/pallas_call | solution.py:285
  116.5 7.2 %collective-permute-done.16.refs_2_ = bf16[320,512]{1,0:T(8,128)(2,1)S(1)} collective-permute-done((bf16[320,512]{1,0:T(8,128)(2,1)S(1)}, bf16[320,512]{1,0:T(8,128)(2,1)S(1)}, u32[]{:S(2)}, u32[]{:S(2)}) %collective-permute-start.16) | collective-permute-done | bytes 327712 | tf_op jit(solution)/shard_map/ppermute | solution.py:419
  124.3 16.4 %all_to_all.16 = bf16[64,8,256]{2,1,0:T(8,128)(2,1)S(1)} all-to-all(bf16[64,8,256]{2,1,0:T(8,128)(2,1)S(1)} %bitcast.20), channel_id=1, replica_groups=mesh['ep'=64,'x'=8,'c'=2] {'ep'}, dimensions={0} | all-to-all | bytes 524288 | tf_op jit(solution)/shard_map/all_to_all | solution.py:400
  141.1 14.3 %all-gather.1 = f32[512,256]{1,0:T(8,128)S(1)} all-gather(f32[256,256]{1,0:T(8,128)S(1)} %combine.1), channel_id=3, replica_groups=mesh['ep'=64,'x'=8,'c'=2] {'c'}, dimensions={0}, use_global_device_ids=true | all-gather | bytes 786432 | tf_op jit(solution)/shard_map/all_gather | solution.py:458
  156.1 12.9 %all_to_all.17.sums_ref = f32[8,1,256]{2,1,0:T(1,128)S(1)} all-to-all(f32[8,1,256]{2,1,0:T(1,128)S(1)} %get-tuple-element.36), channel_id=1, replica_groups=mesh['ep'=64,'x'=8,'c'=2] {'x'}, dimensions={0} | all-to-all | bytes 16384 | tf_op jit(solution)/shard_map/all_to_all | solution.py:400
  168.9 1.6 final.1
  (28 shorter events, 6.8 us)
Async XLA Ops:
  0.0 73.1 %copy-start = (bf16[1,2048,256]{2,1,0:T(8,128)(2,1)S(1)}, bf16[1,2048,256]{2,1,0:T(8,128)(2,1)}, u32[]{:S(2)}) copy-start(bf16[1,2048,256]{2,1,0:T(8,128)(2,1)} %param.13) | copy-start | bytes 3145732
  0.0 48.9 %collective-permute-start = (bf16[2048,256]{1,0:T(8,128)(2,1)}, bf16[2048,256]{1,0:T(8,128)(2,1)S(1)}, u32[]{:S(2)}, u32[]{:S(2)}) collective-permute-start(bf16[2048,256]{1,0:T(8,128)(2,1)} %bitcast.21), channel_id=1, source_target_pairs={{0,1},{1,0},{2,3},{3,2},{4,5},{5,4},{6,7},{7,6},{8,9},{9,8},{10,11... | collective-permute-start | bytes 3145736 | tf_op jit(solution)/shard_map/ppermute | solution.py:409
  16.2 32.7 %collective-permute-start.1 = (bf16[2048,256]{1,0:T(8,128)(2,1)}, bf16[2048,256]{1,0:T(8,128)(2,1)}, u32[]{:S(2)}, u32[]{:S(2)}) collective-permute-start(bf16[2048,256]{1,0:T(8,128)(2,1)} %bitcast.23), channel_id=1, source_target_pairs={{0,1},{1,0},{2,3},{3,2},{4,5},{5,4},{6,7},{7,6},{8,9},{9,8},{10,11... | collective-permute-start | bytes 3145736 | tf_op jit(solution)/shard_map/ppermute | solution.py:409
  18.1 30.8 %collective-permute-start.2 = (bf16[4096,128]{1,0:T(8,128)(2,1)}, bf16[4096,128]{1,0:T(8,128)(2,1)S(1)}, u32[]{:S(2)}, u32[]{:S(2)}) collective-permute-start(bf16[4096,128]{1,0:T(8,128)(2,1)} %bitcast.26), channel_id=1, source_target_pairs={{0,1},{1,0},{2,3},{3,2},{4,5},{5,4},{6,7},{7,6},{8,9},{9,8},{10,11... | collective-permute-start | bytes 3145736 | tf_op jit(solution)/shard_map/ppermute | solution.py:409
  48.9 24.2 %copy-start.4 = (bf16[2048,256]{1,0:T(8,128)(2,1)}, bf16[2048,256]{1,0:T(8,128)(2,1)S(1)}, u32[]{:S(2)}) copy-start(bf16[2048,256]{1,0:T(8,128)(2,1)S(1)} %collective-permute-done.refs_10_) | copy-start | bytes 3145732
  48.9 28.4 %copy-start.3 = (bf16[4096,128]{1,0:T(8,128)(2,1)}, bf16[4096,128]{1,0:T(8,128)(2,1)S(1)}, u32[]{:S(2)}) copy-start(bf16[4096,128]{1,0:T(8,128)(2,1)S(1)} %collective-permute-done.2.refs_9_) | copy-start | bytes 3145732
  49.1 7.4 %collective-permute-start.3 = (bf16[336,256]{1,0:T(8,128)(2,1)S(1)}, bf16[336,256]{1,0:T(8,128)(2,1)S(1)}, u32[]{:S(2)}, u32[]{:S(2)}) collective-permute-start(bf16[336,256]{1,0:T(8,128)(2,1)S(1)} %arrange.1.refs_1_), channel_id=1, source_target_pairs={{0,2},{2,4},{4,6},{6,8},{8,10},{10,12},{12,14},{14,0},{1,3},{3,5},... | collective-permute-start | bytes 516104 | tf_op jit(solution)/shard_map/ppermute | solution.py:419
  52.2 6.4 %collective-permute-start.4 = (bf16[336,256]{1,0:T(8,128)(2,1)S(1)}, bf16[336,256]{1,0:T(8,128)(2,1)S(1)}, u32[]{:S(2)}, u32[]{:S(2)}) collective-permute-start(bf16[336,256]{1,0:T(8,128)(2,1)S(1)} %arrange.1.refs_1_), channel_id=1, source_target_pairs={{0,14},{2,0},{4,2},{6,4},{8,6},{10,8},{12,10},{14,12},{1,15},{3,1}... | collective-permute-start | bytes 516104 | tf_op jit(solution)/shard_map/ppermute | solution.py:422
  56.4 7.3 %collective-permute-start.5 = (bf16[336,256]{1,0:T(8,128)(2,1)S(1)}, bf16[336,256]{1,0:T(8,128)(2,1)S(1)}, u32[]{:S(2)}, u32[]{:S(2)}) collective-permute-start(bf16[336,256]{1,0:T(8,128)(2,1)S(1)} %collective-permute-done.3.refs_2_), channel_id=1, source_target_pairs={{0,2},{2,4},{4,6},{6,8},{8,10},{10,12},{12,14},{14,0},{1,3},{3,5},... | collective-permute-start | bytes 516104 | tf_op jit(solution)/shard_map/ppermute | solution.py:419
  58.7 7.1 %collective-permute-start.6 = (bf16[336,256]{1,0:T(8,128)(2,1)S(1)}, bf16[336,256]{1,0:T(8,128)(2,1)S(1)}, u32[]{:S(2)}, u32[]{:S(2)}) collective-permute-start(bf16[336,256]{1,0:T(8,128)(2,1)S(1)} %collective-permute-done.4.refs_3_), channel_id=1, source_target_pairs={{0,14},{2,0},{4,2},{6,4},{8,6},{10,8},{12,10},{14,12},{1,15},{3,1}... | collective-permute-start | bytes 516104 | tf_op jit(solution)/shard_map/ppermute | solution.py:422
  63.8 7.3 %collective-permute-start.7 = (bf16[336,256]{1,0:T(8,128)(2,1)S(1)}, bf16[336,256]{1,0:T(8,128)(2,1)S(1)}, u32[]{:S(2)}, u32[]{:S(2)}) collective-permute-start(bf16[336,256]{1,0:T(8,128)(2,1)S(1)} %collective-permute-done.5.refs_4_), channel_id=1, source_target_pairs={{0,2},{2,4},{4,6},{6,8},{8,10},{10,12},{12,14},{14,0},{1,3},{3,5},... | collective-permute-start | bytes 516104 | tf_op jit(solution)/shard_map/ppermute | solution.py:419
  65.7 7.3 %collective-permute-start.8 = (bf16[336,256]{1,0:T(8,128)(2,1)S(1)}, bf16[336,256]{1,0:T(8,128)(2,1)S(1)}, u32[]{:S(2)}, u32[]{:S(2)}) collective-permute-start(bf16[336,256]{1,0:T(8,128)(2,1)S(1)} %collective-permute-done.6.refs_5_), channel_id=1, source_target_pairs={{0,14},{2,0},{4,2},{6,4},{8,6},{10,8},{12,10},{14,12},{1,15},{3,1}... | collective-permute-start | bytes 516104 | tf_op jit(solution)/shard_map/ppermute | solution.py:422
  71.1 7.3 %collective-permute-start.9 = (bf16[336,256]{1,0:T(8,128)(2,1)S(1)}, bf16[336,256]{1,0:T(8,128)(2,1)S(1)}, u32[]{:S(2)}, u32[]{:S(2)}) collective-permute-start(bf16[336,256]{1,0:T(8,128)(2,1)S(1)} %collective-permute-done.7.refs_6_), channel_id=1, source_target_pairs={{0,2},{2,4},{4,6},{6,8},{8,10},{10,12},{12,14},{14,0},{1,3},{3,5},... | collective-permute-start | bytes 516104 | tf_op jit(solution)/shard_map/ppermute | solution.py:419
  73.1 1.2 copy-start.1
  79.5 9.0 %collective-permute-start.10 = (bf16[320,512]{1,0:T(8,128)(2,1)S(1)}, bf16[320,512]{1,0:T(8,128)(2,1)S(1)}, u32[]{:S(2)}, u32[]{:S(2)}) collective-permute-start(bf16[320,512]{1,0:T(8,128)(2,1)S(1)} %gate_last.1.refs_1_), channel_id=1, source_target_pairs={{0,2},{2,4},{4,6},{6,8},{8,10},{10,12},{12,14},{14,0},{1,3},{3,5},... | collective-permute-start | bytes 983048 | tf_op jit(solution)/shard_map/ppermute | solution.py:419
  81.5 9.0 %collective-permute-start.11 = (bf16[320,512]{1,0:T(8,128)(2,1)S(1)}, bf16[320,512]{1,0:T(8,128)(2,1)S(1)}, u32[]{:S(2)}, u32[]{:S(2)}) collective-permute-start(bf16[320,512]{1,0:T(8,128)(2,1)S(1)} %gate_last.1.refs_1_), channel_id=1, source_target_pairs={{0,14},{2,0},{4,2},{6,4},{8,6},{10,8},{12,10},{14,12},{1,15},{3,1}... | collective-permute-start | bytes 983048 | tf_op jit(solution)/shard_map/ppermute | solution.py:422
  88.6 11.0 %collective-permute-start.12 = (bf16[320,512]{1,0:T(8,128)(2,1)S(1)}, bf16[320,512]{1,0:T(8,128)(2,1)S(1)}, u32[]{:S(2)}, u32[]{:S(2)}) collective-permute-start(bf16[320,512]{1,0:T(8,128)(2,1)S(1)} %collective-permute-done.10.refs_2_), channel_id=1, source_target_pairs={{0,2},{2,4},{4,6},{6,8},{8,10},{10,12},{12,14},{14,0},{1,3},{3,5},... | collective-permute-start | bytes 983048 | tf_op jit(solution)/shard_map/ppermute | solution.py:419
  90.5 11.0 %collective-permute-start.13 = (bf16[320,512]{1,0:T(8,128)(2,1)S(1)}, bf16[320,512]{1,0:T(8,128)(2,1)S(1)}, u32[]{:S(2)}, u32[]{:S(2)}) collective-permute-start(bf16[320,512]{1,0:T(8,128)(2,1)S(1)} %collective-permute-done.11.refs_3_), channel_id=1, source_target_pairs={{0,14},{2,0},{4,2},{6,4},{8,6},{10,8},{12,10},{14,12},{1,15},{3,1}... | collective-permute-start | bytes 983048 | tf_op jit(solution)/shard_map/ppermute | solution.py:422
  99.6 12.2 %collective-permute-start.14 = (bf16[320,512]{1,0:T(8,128)(2,1)S(1)}, bf16[320,512]{1,0:T(8,128)(2,1)S(1)}, u32[]{:S(2)}, u32[]{:S(2)}) collective-permute-start(bf16[320,512]{1,0:T(8,128)(2,1)S(1)} %collective-permute-done.12.refs_4_), channel_id=1, source_target_pairs={{0,2},{2,4},{4,6},{6,8},{8,10},{10,12},{12,14},{14,0},{1,3},{3,5},... | collective-permute-start | bytes 983048 | tf_op jit(solution)/shard_map/ppermute | solution.py:419
  101.5 12.4 %collective-permute-start.15 = (bf16[320,512]{1,0:T(8,128)(2,1)S(1)}, bf16[320,512]{1,0:T(8,128)(2,1)S(1)}, u32[]{:S(2)}, u32[]{:S(2)}) collective-permute-start(bf16[320,512]{1,0:T(8,128)(2,1)S(1)} %collective-permute-done.13.refs_5_), channel_id=1, source_target_pairs={{0,14},{2,0},{4,2},{6,4},{8,6},{10,8},{12,10},{14,12},{1,15},{3,1}... | collective-permute-start | bytes 983048 | tf_op jit(solution)/shard_map/ppermute | solution.py:422
  111.7 12.0 %collective-permute-start.16 = (bf16[320,512]{1,0:T(8,128)(2,1)S(1)}, bf16[320,512]{1,0:T(8,128)(2,1)S(1)}, u32[]{:S(2)}, u32[]{:S(2)}) collective-permute-start(bf16[320,512]{1,0:T(8,128)(2,1)S(1)} %collective-permute-done.14.refs_6_), channel_id=1, source_target_pairs={{0,2},{2,4},{4,6},{6,8},{8,10},{10,12},{12,14},{14,0},{1,3},{3,5},... | collective-permute-start | bytes 983048 | tf_op jit(solution)/shard_map/ppermute | solution.py:419
  124.3 16.4 %copy-start.2 = (f32[256,8]{1,0:T(8,128)S(1)}, f32[256,8]{1,0:T(8,128)}, u32[]{:S(2)}) copy-start(f32[256,8]{1,0:T(8,128)} %get-tuple-element.34.cols_ref) | copy-start | bytes 24580

commit v8 on v7

--- a/solution.py
+++ b/solution.py
@@ -148,83 +148,54 @@
     )(arrived, tokens)
 
 
-def gained(feat_ref):
-    rows = feat_ref.shape[0] - EXTRA
-    pieces = feat_ref[rows:, :].astype(jnp.float32)
-    gain = pieces[0:1, :] + pieces[1:2, :] + pieces[2:3, :]
-    part = feat_ref[0:rows, :].astype(jnp.float32)
-    return (part * gain).astype(jnp.bfloat16), part * part
-
-
 def chip_at(place_ref, offset, chips):
     return lax.rem(place_ref[0] + (offset + chips), chips)
 
 
-def gate_early_kernel(*refs, offsets, last, chips):
-    count = len(offsets)
-    place_ref, *rest = refs
-    feat_refs, weight_refs = rest[:count], rest[count : count + 4]
-    total_refs, (squares_ref, rows_ref) = rest[count + 4 : count + 8], rest[count + 8 :]
-    wide = feat_refs[0].shape[1]
-    totals = [jnp.zeros(ref.shape, jnp.float32) for ref in total_refs]
-    squares = jnp.zeros(squares_ref.shape, jnp.float32)
-    for offset, feat_ref in zip(offsets, feat_refs):
+def squares_kernel(*refs):
+    *feat_refs, out_ref = refs
+    rows = out_ref.shape[0]
+    total = jnp.zeros(out_ref.shape, jnp.float32)
+    for ref in feat_refs:
+        part = ref[0:rows, :].astype(jnp.float32)
+        total = total + part * part
+    out_ref[...] = total
+
+
+def squares_of(arrays):
+    rows, wide = arrays[0].shape
+    return pl.pallas_call(
+        squares_kernel,
+        out_shape=jax.ShapeDtypeStruct((rows - EXTRA, wide), jnp.float32),
+        compiler_params=params(8),
+        name="squares",
+    )(*arrays)
+
+
+def hidden_kernel(*refs, offsets):
+    chips = len(offsets)
+    place_ref, squares_ref, *rest = refs
+    feat_refs, weight_refs, (out_ref, normed_ref) = rest[:chips], rest[chips:-2], rest[-2:]
+    rows, wide = squares_ref.shape
+    units = weight_refs[0].shape[1]
+    part = feat_refs[-1][0:rows, :].astype(jnp.float32)
+    total = squares_ref[...] + part * part
+    scale = lax.rsqrt(jnp.sum(total, axis=1, keepdims=True) / (chips * wide) + epsilon)
+    for offset, ref in zip(offsets, feat_refs):
         begin = pl.multiple_of(chip_at(place_ref, offset, chips) * wide, wide)
-        part, square = gained(feat_ref)
-        squares = squares + square
-        for i, weight_ref in enumerate(weight_refs):
-            totals[i] = totals[i] + jnp.dot(
-                part, weight_ref[pl.ds(begin, wide), :], preferred_element_type=jnp.float32
-            )
-    for i, total in enumerate(totals):
-        total_refs[i][...] = total
-    squares_ref[...] = squares
-    begin = pl.multiple_of(chip_at(place_ref, last, chips) * wide, wide)
-    for i, weight_ref in enumerate(weight_refs):
-        rows_ref[i] = weight_ref[pl.ds(begin, wide), :]
-
-
-def gate_early(place, features, last, weights, chips):
-    offsets = [offset for offset, _ in features]
-    arrays = [array for _, array in features]
-    rows, wide = arrays[0].shape
-    rows = rows - EXTRA
-    units = weights[0].shape[1]
-
-    def body(*refs):
-        gate_early_kernel(*refs, offsets=offsets, last=last, chips=chips)
-
-    total = jax.ShapeDtypeStruct((rows, units), jnp.float32)
-    return pl.pallas_call(
-        body,
-        in_specs=[whole(pltpu.SMEM)] + [whole()] * (len(arrays) + 4),
-        out_shape=(
-            *[total] * 4,
-            jax.ShapeDtypeStruct((rows, wide), jnp.float32),
-            jax.ShapeDtypeStruct((4, wide, units), jnp.bfloat16),
-        ),
-        compiler_params=params(16),
-        name="gate_early",
-    )(place, *arrays, *weights)
-
-
-def gate_last_kernel(place_ref, *refs, chips):
-    total_refs, (squares_ref, rows_ref, feat_ref, out_ref) = refs[:4], refs[4:]
-    units = rows_ref.shape[2]
-    part, square = gained(feat_ref)
-    square = squares_ref[...] + square
-    full = chips * square.shape[1]
-    scale = lax.rsqrt(jnp.sum(square, axis=1, keepdims=True) / full + epsilon)
-    totals = [
-        scale * (ref[...] + jnp.dot(part, rows_ref[i], preferred_element_type=jnp.float32))
-        for i, ref in enumerate(total_refs)
-    ]
-
-    def hidden_of(gate, upper):
+        pieces = ref[rows:, :].astype(jnp.float32)
+        gain = pieces[0:1, :] + pieces[1:2, :] + pieces[2:3, :]
+        part = ref[0:rows, :].astype(jnp.float32)
+        normed_ref[:, pl.ds(begin, wide)] = (part * scale * gain).astype(jnp.bfloat16)
+
+    def hidden_from(gate_ref, up_ref):
+        normed = normed_ref[...]
+        gate = jnp.dot(normed, gate_ref[...], preferred_element_type=jnp.float32)
+        upper = jnp.dot(normed, up_ref[...], preferred_element_type=jnp.float32)
         return (gate / (1.0 + jnp.exp(-gate)) * upper).astype(jnp.bfloat16)
 
-    own = hidden_of(totals[0], totals[1])
-    other = hidden_of(totals[2], totals[3])
+    own = hidden_from(weight_refs[0], weight_refs[1])
+    other = hidden_from(weight_refs[2], weight_refs[3])
     for c in range(CORES):
 
         @pl.when(place_ref[1] == c)
@@ -233,19 +204,23 @@
             out_ref[:, (1 - c) * units : (2 - c) * units] = other
 
 
-def gate_last(place, early, feature, chips):
-    rows, units = early[0].shape
+def hidden_of(place, squares, features, weights):
+    offsets = [offset for offset, _ in features]
+    arrays = [array for _, array in features]
+    rows, wide = squares.shape
+    units = weights[0].shape[1]
 
     def body(*refs):
-        gate_last_kernel(*refs, chips=chips)
+        hidden_kernel(*refs, offsets=offsets)
 
     return pl.pallas_call(
         body,
-        in_specs=[whole(pltpu.SMEM)] + [whole()] * 7,
+        in_specs=[whole(pltpu.SMEM)] + [whole()] * (1 + len(arrays) + len(weights)),
         out_shape=jax.ShapeDtypeStruct((rows, CORES * units), jnp.bfloat16),
+        scratch_shapes=[pltpu.VMEM((rows, len(arrays) * wide), jnp.bfloat16)],
         compiler_params=params(16),
-        name="gate_last",
-    )(place, *early, feature)
+        name="hidden",
+    )(place, squares, *arrays, *weights)
 
 
 def both_columns(place_ref, down0_ref, down1_ref, down_ref):
@@ -449,11 +424,11 @@
     for weight in (gate0, up0, down0):
         swapped.append(swap(weight))
     arrived, gate1, up1, down1 = lax.optimization_barrier((arrived, *swapped))
-    *early, (last, feature) = ring(arrange(arrived, both, half))
-    weights = (gate0, up0, in_hbm(gate1), in_hbm(up1))
-    projected = gate_early(place, early, last, weights, chips)
-    *early, (last, hidden) = ring(gate_last(place, projected, feature, chips))
-    summed = down_early(place, early, last, in_hbm(down0), in_hbm(down1), chips)
+    features = ring(arrange(arrived, both, half))
+    squares = squares_of([array for _, array in features[:-1]])
+    hidden = hidden_of(place, squares, features, (gate0, up0, gate1, up1))
+    *early, (last, hidden) = ring(hidden)
+    summed = down_early(place, early, last, down0, down1, chips)
     result = down_last(summed, hidden, half)
     mixed = lax.all_gather(combine(blocks_exchange(result), cols), "c", axis=0)
     mixed, sums = sums_of(place, mixed, chips)

time: 171 us -> 173 us (1.012)
  waiting for transfers between devices: 23.9 us -> 28.8 us
  Pallas kernels: 12.6 us -> 10.6 us
    ppermute x8, waiting for transfers between devices: 23.4 us -> 28.3 us  [ring(): before = lax.ppermute(before, 'x', onward)]
  transfers between devices with their start and end apart: 17 -> 17, of which waited for: 10 -> 10; matrix products, arithmetic and copies ran while one was open for 0% -> 0% of each run, Pallas kernels for 5% -> 3%
where the time goes in v8:
time: 173 us; the launch traced here: 172 us
  blocking collectives  69.2 us (40%)
  starting transfers between devices  63.2 us (37%)
  waiting for transfers between devices  28.8 us (17%)
  Pallas kernels  10.6 us (6%)
    all_to_all x3, blocking collectives, exchange(): return lax.all_to_all(value, axis, split_axis=0, concat_axis=0, tiled=True)  53 us
    ppermute x8, waiting for transfers between devices, ring(): before = lax.ppermute(before, 'x', onward)  28.3 us
    ppermute x6, starting transfers between devices, ring(): after = lax.ppermute(after, 'x', backward)  26.2 us
    ppermute x3, starting transfers between devices, swap(): return lax.ppermute(value, 'c', [(0, 1), (1, 0)])  20.3 us
    ppermute x8, starting transfers between devices, ring(): before = lax.ppermute(before, 'x', onward)  16.6 us
    all_gather x1, blocking collectives, layer(): mixed = lax.all_gather(combine(blocks_exchange(result), cols), 'c', axis=0)  14.3 us
  transfers between devices with their start and end apart: 17, of which 10 were waited for; matrix products, arithmetic and copies ran while one was open for 0% of the time, Pallas kernels for 3%

profile of v8, /device:TPU:1, one launch (start us, length us, event | category | flops | bytes accessed | tf_op | source)
XLA Modules:
  0.0 172.2 jit_solution(11938904351113123570)
XLA Ops:
  0.0 16.0 %collective-permute-start = (bf16[2048,256]{1,0:T(8,128)(2,1)}, bf16[2048,256]{1,0:T(8,128)(2,1)S(1)}, u32[]{:S(2)}, u32[]{:S(2)}) collective-permute-start(bf16[2048,256]{1,0:T(8,128)(2,1)} %bitcast.18), channel_id=1, source_target_pairs={{0,1},{1,0},{2,3},{3,2},{4,5},{5,4},{6,7},{7,6},{8,9},{9,8},{10,11... | collective-permute-start | bytes 3145736 | tf_op jit(solution)/shard_map/ppermute | solution.py:384
  16.0 1.9 %collective-permute-start.1 = (bf16[2048,256]{1,0:T(8,128)(2,1)}, bf16[2048,256]{1,0:T(8,128)(2,1)S(1)}, u32[]{:S(2)}, u32[]{:S(2)}) collective-permute-start(bf16[2048,256]{1,0:T(8,128)(2,1)} %bitcast.20), channel_id=1, source_target_pairs={{0,1},{1,0},{2,3},{3,2},{4,5},{5,4},{6,7},{7,6},{8,9},{9,8},{10,11... | collective-permute-start | bytes 3145736 | tf_op jit(solution)/shard_map/ppermute | solution.py:384
  18.0 2.4 %collective-permute-start.2 = (bf16[4096,128]{1,0:T(8,128)(2,1)}, bf16[4096,128]{1,0:T(8,128)(2,1)S(1)}, u32[]{:S(2)}, u32[]{:S(2)}) collective-permute-start(bf16[4096,128]{1,0:T(8,128)(2,1)} %bitcast.22), channel_id=1, source_target_pairs={{0,1},{1,0},{2,3},{3,2},{4,5},{5,4},{6,7},{7,6},{8,9},{9,8},{10,11... | collective-permute-start | bytes 3145736 | tf_op jit(solution)/shard_map/ppermute | solution.py:384
  20.4 0.9 prepare.1
  21.2 1.9 %all-gather = bf16[544,128]{1,0:T(8,128)(2,1)S(1)} all-gather(bf16[272,128]{1,0:T(8,128)(2,1)S(1)} %prepare.1), channel_id=2, replica_groups=mesh['ep'=64,'x'=8,'c'=2] {'c'}, dimensions={0}, use_global_device_ids=true | all-gather | bytes 208896 | tf_op jit(solution)/shard_map/all_gather | solution.py:413
  23.2 1.8 %dispatch.1 = (bf16[512,256]{1,0:T(8,128)(2,1)S(1)}, f32[256,8]{1,0:T(8,128)}) custom-call(s32[2]{0:T(128)S(1)} %pad_add_fusion.refs_0_.place_ref, bf16[2,272,128]{2,1,0:T(8,128)(2,1)S(1)} %bitcast.16, s32[2,256]{1,0:T(2,128)} %bitcast.28, f32[2,256]{1,0:T(2,128)} %bitcast.29), custom_call_target="tpu_custom_call" | custom-call | tf_op jit(solution)/shard_map/dispatch/pallas_call | solution.py:97
  25.0 23.7 %all_to_all.15 = bf16[64,8,256]{2,1,0:T(8,128)(2,1)S(1)} all-to-all(bf16[64,8,256]{2,1,0:T(8,128)(2,1)S(1)} %bitcast.27), channel_id=1, replica_groups=mesh['ep'=64,'x'=8,'c'=2] {'ep'}, dimensions={0} | all-to-all | bytes 524288 | tf_op jit(solution)/shard_map/all_to_all | solution.py:375
  49.0 3.2 %collective-permute-start.3 = (bf16[336,256]{1,0:T(8,128)(2,1)S(1)}, bf16[336,256]{1,0:T(8,128)(2,1)S(1)}, u32[]{:S(2)}, u32[]{:S(2)}) collective-permute-start(bf16[336,256]{1,0:T(8,128)(2,1)S(1)} %arrange.1.refs_0_.refs_2_), channel_id=1, source_target_pairs={{0,2},{2,4},{4,6},{6,8},{8,10},{10,12},{12,14},{14,0},{1,3},{3,5},... | collective-permute-start | bytes 516104 | tf_op jit(solution)/shard_map/ppermute | solution.py:394
  52.2 3.4 %collective-permute-start.4 = (bf16[336,256]{1,0:T(8,128)(2,1)S(1)}, bf16[336,256]{1,0:T(8,128)(2,1)S(1)}, u32[]{:S(2)}, u32[]{:S(2)}) collective-permute-start(bf16[336,256]{1,0:T(8,128)(2,1)S(1)} %arrange.1.refs_0_.refs_2_), channel_id=1, source_target_pairs={{0,14},{2,0},{4,2},{6,4},{8,6},{10,8},{12,10},{14,12},{1,15},{3,1}... | collective-permute-start | bytes 516104 | tf_op jit(solution)/shard_map/ppermute | solution.py:397
  56.5 1.9 %collective-permute-start.5 = (bf16[336,256]{1,0:T(8,128)(2,1)S(1)}, bf16[336,256]{1,0:T(8,128)(2,1)S(1)}, u32[]{:S(2)}, u32[]{:S(2)}) collective-permute-start(bf16[336,256]{1,0:T(8,128)(2,1)S(1)} %collective-permute-done.3.refs_1_.refs_3_), channel_id=1, source_target_pairs={{0,2},{2,4},{4,6},{6,8},{8,10},{10,12},{12,14},{14,0},{1,3},{3,5},... | collective-permute-start | bytes 516104 | tf_op jit(solution)/shard_map/ppermute | solution.py:394
  58.7 4.3 %collective-permute-start.6 = (bf16[336,256]{1,0:T(8,128)(2,1)S(1)}, bf16[336,256]{1,0:T(8,128)(2,1)S(1)}, u32[]{:S(2)}, u32[]{:S(2)}) collective-permute-start(bf16[336,256]{1,0:T(8,128)(2,1)S(1)} %collective-permute-done.4.refs_2_.refs_4_), channel_id=1, source_target_pairs={{0,14},{2,0},{4,2},{6,4},{8,6},{10,8},{12,10},{14,12},{1,15},{3,1}... | collective-permute-start | bytes 516104 | tf_op jit(solution)/shard_map/ppermute | solution.py:397
  63.8 1.9 %collective-permute-start.7 = (bf16[336,256]{1,0:T(8,128)(2,1)S(1)}, bf16[336,256]{1,0:T(8,128)(2,1)S(1)}, u32[]{:S(2)}, u32[]{:S(2)}) collective-permute-start(bf16[336,256]{1,0:T(8,128)(2,1)S(1)} %collective-permute-done.5.refs_3_.refs_5_), channel_id=1, source_target_pairs={{0,2},{2,4},{4,6},{6,8},{8,10},{10,12},{12,14},{14,0},{1,3},{3,5},... | collective-permute-start | bytes 516104 | tf_op jit(solution)/shard_map/ppermute | solution.py:394
  65.7 4.6 %collective-permute-start.8 = (bf16[336,256]{1,0:T(8,128)(2,1)S(1)}, bf16[336,256]{1,0:T(8,128)(2,1)S(1)}, u32[]{:S(2)}, u32[]{:S(2)}) collective-permute-start(bf16[336,256]{1,0:T(8,128)(2,1)S(1)} %collective-permute-done.6.refs_4_.refs_6_), channel_id=1, source_target_pairs={{0,14},{2,0},{4,2},{6,4},{8,6},{10,8},{12,10},{14,12},{1,15},{3,1}... | collective-permute-start | bytes 516104 | tf_op jit(solution)/shard_map/ppermute | solution.py:397
  71.2 1.9 %collective-permute-start.9 = (bf16[336,256]{1,0:T(8,128)(2,1)S(1)}, bf16[336,256]{1,0:T(8,128)(2,1)S(1)}, u32[]{:S(2)}, u32[]{:S(2)}) collective-permute-start(bf16[336,256]{1,0:T(8,128)(2,1)S(1)} %collective-permute-done.7.refs_5_.refs_7_), channel_id=1, source_target_pairs={{0,2},{2,4},{4,6},{6,8},{8,10},{10,12},{12,14},{14,0},{1,3},{3,5},... | collective-permute-start | bytes 516104 | tf_op jit(solution)/shard_map/ppermute | solution.py:394
  73.4 5.1 %collective-permute-done.9.refs_9_ = bf16[336,256]{1,0:T(8,128)(2,1)S(1)} collective-permute-done((bf16[336,256]{1,0:T(8,128)(2,1)S(1)}, bf16[336,256]{1,0:T(8,128)(2,1)S(1)}, u32[]{:S(2)}, u32[]{:S(2)}) %collective-permute-start.9) | collective-permute-done | bytes 172064 | tf_op jit(solution)/shard_map/ppermute | solution.py:394
  78.5 2.7 %hidden.1.refs_1_ = bf16[320,512]{1,0:T(8,128)(2,1)S(1)} custom-call(s32[2]{0:T(128)S(1)} %pad_add_fusion.refs_0_.place_ref, f32[320,256]{1,0:T(8,128)S(1)} %squares.1.refs_1_, bf16[336,256]{1,0:T(8,128)(2,1)S(1)} %arrange.1.refs_0_.refs_2_, bf16[336,256]{1,0:T(8,128)(2,1)S(1)} %collective-permute-done.3.refs_1_.refs_3_, ...), custom_call_target="tpu_custom_call" | custom-call | tf_op jit(solution)/shard_map/hidden/pallas_call | solution.py:216
  81.2 1.9 %collective-permute-start.10 = (bf16[320,512]{1,0:T(8,128)(2,1)S(1)}, bf16[320,512]{1,0:T(8,128)(2,1)S(1)}, u32[]{:S(2)}, u32[]{:S(2)}) collective-permute-start(bf16[320,512]{1,0:T(8,128)(2,1)S(1)} %hidden.1.refs_1_), channel_id=1, source_target_pairs={{0,2},{2,4},{4,6},{6,8},{8,10},{10,12},{12,14},{14,0},{1,3},{3,5},... | collective-permute-start | bytes 983048 | tf_op jit(solution)/shard_map/ppermute | solution.py:394
  83.1 4.6 %collective-permute-start.11 = (bf16[320,512]{1,0:T(8,128)(2,1)S(1)}, bf16[320,512]{1,0:T(8,128)(2,1)S(1)}, u32[]{:S(2)}, u32[]{:S(2)}) collective-permute-start(bf16[320,512]{1,0:T(8,128)(2,1)S(1)} %hidden.1.refs_1_), channel_id=1, source_target_pairs={{0,14},{2,0},{4,2},{6,4},{8,6},{10,8},{12,10},{14,12},{1,15},{3,1}... | collective-permute-start | bytes 983048 | tf_op jit(solution)/shard_map/ppermute | solution.py:397
  87.7 2.5 %collective-permute-done.10.refs_2_ = bf16[320,512]{1,0:T(8,128)(2,1)S(1)} collective-permute-done((bf16[320,512]{1,0:T(8,128)(2,1)S(1)}, bf16[320,512]{1,0:T(8,128)(2,1)S(1)}, u32[]{:S(2)}, u32[]{:S(2)}) %collective-permute-start.10) | collective-permute-done | bytes 327712 | tf_op jit(solution)/shard_map/ppermute | solution.py:394
  90.2 1.9 %collective-permute-start.12 = (bf16[320,512]{1,0:T(8,128)(2,1)S(1)}, bf16[320,512]{1,0:T(8,128)(2,1)S(1)}, u32[]{:S(2)}, u32[]{:S(2)}) collective-permute-start(bf16[320,512]{1,0:T(8,128)(2,1)S(1)} %collective-permute-done.10.refs_2_), channel_id=1, source_target_pairs={{0,2},{2,4},{4,6},{6,8},{8,10},{10,12},{12,14},{14,0},{1,3},{3,5},... | collective-permute-start | bytes 983048 | tf_op jit(solution)/shard_map/ppermute | solution.py:394
  92.2 4.6 %collective-permute-start.13 = (bf16[320,512]{1,0:T(8,128)(2,1)S(1)}, bf16[320,512]{1,0:T(8,128)(2,1)S(1)}, u32[]{:S(2)}, u32[]{:S(2)}) collective-permute-start(bf16[320,512]{1,0:T(8,128)(2,1)S(1)} %collective-permute-done.11.refs_3_), channel_id=1, source_target_pairs={{0,14},{2,0},{4,2},{6,4},{8,6},{10,8},{12,10},{14,12},{1,15},{3,1}... | collective-permute-start | bytes 983048 | tf_op jit(solution)/shard_map/ppermute | solution.py:397
  96.7 4.5 %collective-permute-done.12.refs_4_ = bf16[320,512]{1,0:T(8,128)(2,1)S(1)} collective-permute-done((bf16[320,512]{1,0:T(8,128)(2,1)S(1)}, bf16[320,512]{1,0:T(8,128)(2,1)S(1)}, u32[]{:S(2)}, u32[]{:S(2)}) %collective-permute-start.12) | collective-permute-done | bytes 327712 | tf_op jit(solution)/shard_map/ppermute | solution.py:394
  101.3 1.9 %collective-permute-start.14 = (bf16[320,512]{1,0:T(8,128)(2,1)S(1)}, bf16[320,512]{1,0:T(8,128)(2,1)S(1)}, u32[]{:S(2)}, u32[]{:S(2)}) collective-permute-start(bf16[320,512]{1,0:T(8,128)(2,1)S(1)} %collective-permute-done.12.refs_4_), channel_id=1, source_target_pairs={{0,2},{2,4},{4,6},{6,8},{8,10},{10,12},{12,14},{14,0},{1,3},{3,5},... | collective-permute-start | bytes 983048 | tf_op jit(solution)/shard_map/ppermute | solution.py:394
  103.2 4.8 %collective-permute-start.15 = (bf16[320,512]{1,0:T(8,128)(2,1)S(1)}, bf16[320,512]{1,0:T(8,128)(2,1)S(1)}, u32[]{:S(2)}, u32[]{:S(2)}) collective-permute-start(bf16[320,512]{1,0:T(8,128)(2,1)S(1)} %collective-permute-done.13.refs_5_), channel_id=1, source_target_pairs={{0,14},{2,0},{4,2},{6,4},{8,6},{10,8},{12,10},{14,12},{1,15},{3,1}... | collective-permute-start | bytes 983048 | tf_op jit(solution)/shard_map/ppermute | solution.py:397
  108.0 5.4 %collective-permute-done.14.refs_6_ = bf16[320,512]{1,0:T(8,128)(2,1)S(1)} collective-permute-done((bf16[320,512]{1,0:T(8,128)(2,1)S(1)}, bf16[320,512]{1,0:T(8,128)(2,1)S(1)}, u32[]{:S(2)}, u32[]{:S(2)}) %collective-permute-start.14) | collective-permute-done | bytes 327712 | tf_op jit(solution)/shard_map/ppermute | solution.py:394
  113.4 1.9 %collective-permute-start.16 = (bf16[320,512]{1,0:T(8,128)(2,1)S(1)}, bf16[320,512]{1,0:T(8,128)(2,1)S(1)}, u32[]{:S(2)}, u32[]{:S(2)}) collective-permute-start(bf16[320,512]{1,0:T(8,128)(2,1)S(1)} %collective-permute-done.14.refs_6_), channel_id=1, source_target_pairs={{0,2},{2,4},{4,6},{6,8},{8,10},{10,12},{12,14},{14,0},{1,3},{3,5},... | collective-permute-start | bytes 983048 | tf_op jit(solution)/shard_map/ppermute | solution.py:394
  115.5 1.7 down_early.1
  117.2 8.2 %collective-permute-done.16.refs_2_ = bf16[320,512]{1,0:T(8,128)(2,1)S(1)} collective-permute-done((bf16[320,512]{1,0:T(8,128)(2,1)S(1)}, bf16[320,512]{1,0:T(8,128)(2,1)S(1)}, u32[]{:S(2)}, u32[]{:S(2)}) %collective-permute-start.16) | collective-permute-done | bytes 327712 | tf_op jit(solution)/shard_map/ppermute | solution.py:394
  126.0 16.4 %all_to_all.16 = bf16[64,8,256]{2,1,0:T(8,128)(2,1)S(1)} all-to-all(bf16[64,8,256]{2,1,0:T(8,128)(2,1)S(1)} %bitcast.26), channel_id=1, replica_groups=mesh['ep'=64,'x'=8,'c'=2] {'ep'}, dimensions={0} | all-to-all | bytes 524288 | tf_op jit(solution)/shard_map/all_to_all | solution.py:375
  142.7 14.3 %all-gather.1 = f32[512,256]{1,0:T(8,128)S(1)} all-gather(f32[256,256]{1,0:T(8,128)S(1)} %combine.1), channel_id=3, replica_groups=mesh['ep'=64,'x'=8,'c'=2] {'c'}, dimensions={0}, use_global_device_ids=true | all-gather | bytes 786432 | tf_op jit(solution)/shard_map/all_gather | solution.py:433
  157.8 12.9 %all_to_all.17.sums_ref = f32[8,1,256]{2,1,0:T(1,128)S(1)} all-to-all(f32[8,1,256]{2,1,0:T(1,128)S(1)} %get-tuple-element.24), channel_id=1, replica_groups=mesh['ep'=64,'x'=8,'c'=2] {'x'}, dimensions={0} | all-to-all | bytes 16384 | tf_op jit(solution)/shard_map/all_to_all | solution.py:375
  170.6 1.6 final.1
  (26 shorter events, 5.2 us)
Async XLA Ops:
  0.0 48.7 %collective-permute-start = (bf16[2048,256]{1,0:T(8,128)(2,1)}, bf16[2048,256]{1,0:T(8,128)(2,1)S(1)}, u32[]{:S(2)}, u32[]{:S(2)}) collective-permute-start(bf16[2048,256]{1,0:T(8,128)(2,1)} %bitcast.18), channel_id=1, source_target_pairs={{0,1},{1,0},{2,3},{3,2},{4,5},{5,4},{6,7},{7,6},{8,9},{9,8},{10,11... | collective-permute-start | bytes 3145736 | tf_op jit(solution)/shard_map/ppermute | solution.py:384
  16.0 32.7 %collective-permute-start.1 = (bf16[2048,256]{1,0:T(8,128)(2,1)}, bf16[2048,256]{1,0:T(8,128)(2,1)S(1)}, u32[]{:S(2)}, u32[]{:S(2)}) collective-permute-start(bf16[2048,256]{1,0:T(8,128)(2,1)} %bitcast.20), channel_id=1, source_target_pairs={{0,1},{1,0},{2,3},{3,2},{4,5},{5,4},{6,7},{7,6},{8,9},{9,8},{10,11... | collective-permute-start | bytes 3145736 | tf_op jit(solution)/shard_map/ppermute | solution.py:384
  18.0 30.8 %collective-permute-start.2 = (bf16[4096,128]{1,0:T(8,128)(2,1)}, bf16[4096,128]{1,0:T(8,128)(2,1)S(1)}, u32[]{:S(2)}, u32[]{:S(2)}) collective-permute-start(bf16[4096,128]{1,0:T(8,128)(2,1)} %bitcast.22), channel_id=1, source_target_pairs={{0,1},{1,0},{2,3},{3,2},{4,5},{5,4},{6,7},{7,6},{8,9},{9,8},{10,11... | collective-permute-start | bytes 3145736 | tf_op jit(solution)/shard_map/ppermute | solution.py:384
  48.8 29.8 %copy-start = (bf16[1,2048,256]{2,1,0:T(8,128)(2,1)S(1)}, bf16[1,2048,256]{2,1,0:T(8,128)(2,1)}, u32[]{:S(2)}) copy-start(bf16[1,2048,256]{2,1,0:T(8,128)(2,1)} %param.13) | copy-start | bytes 3145732
  48.8 29.8 %copy-start.1 = (bf16[1,2048,256]{2,1,0:T(8,128)(2,1)S(1)}, bf16[1,2048,256]{2,1,0:T(8,128)(2,1)}, u32[]{:S(2)}) copy-start(bf16[1,2048,256]{2,1,0:T(8,128)(2,1)} %param.14) | copy-start | bytes 3145732
  49.0 7.5 %collective-permute-start.3 = (bf16[336,256]{1,0:T(8,128)(2,1)S(1)}, bf16[336,256]{1,0:T(8,128)(2,1)S(1)}, u32[]{:S(2)}, u32[]{:S(2)}) collective-permute-start(bf16[336,256]{1,0:T(8,128)(2,1)S(1)} %arrange.1.refs_0_.refs_2_), channel_id=1, source_target_pairs={{0,2},{2,4},{4,6},{6,8},{8,10},{10,12},{12,14},{14,0},{1,3},{3,5},... | collective-permute-start | bytes 516104 | tf_op jit(solution)/shard_map/ppermute | solution.py:394
  52.2 6.4 %collective-permute-start.4 = (bf16[336,256]{1,0:T(8,128)(2,1)S(1)}, bf16[336,256]{1,0:T(8,128)(2,1)S(1)}, u32[]{:S(2)}, u32[]{:S(2)}) collective-permute-start(bf16[336,256]{1,0:T(8,128)(2,1)S(1)} %arrange.1.refs_0_.refs_2_), channel_id=1, source_target_pairs={{0,14},{2,0},{4,2},{6,4},{8,6},{10,8},{12,10},{14,12},{1,15},{3,1}... | collective-permute-start | bytes 516104 | tf_op jit(solution)/shard_map/ppermute | solution.py:397
  56.5 7.3 %collective-permute-start.5 = (bf16[336,256]{1,0:T(8,128)(2,1)S(1)}, bf16[336,256]{1,0:T(8,128)(2,1)S(1)}, u32[]{:S(2)}, u32[]{:S(2)}) collective-permute-start(bf16[336,256]{1,0:T(8,128)(2,1)S(1)} %collective-permute-done.3.refs_1_.refs_3_), channel_id=1, source_target_pairs={{0,2},{2,4},{4,6},{6,8},{8,10},{10,12},{12,14},{14,0},{1,3},{3,5},... | collective-permute-start | bytes 516104 | tf_op jit(solution)/shard_map/ppermute | solution.py:394
  58.7 7.1 %collective-permute-start.6 = (bf16[336,256]{1,0:T(8,128)(2,1)S(1)}, bf16[336,256]{1,0:T(8,128)(2,1)S(1)}, u32[]{:S(2)}, u32[]{:S(2)}) collective-permute-start(bf16[336,256]{1,0:T(8,128)(2,1)S(1)} %collective-permute-done.4.refs_2_.refs_4_), channel_id=1, source_target_pairs={{0,14},{2,0},{4,2},{6,4},{8,6},{10,8},{12,10},{14,12},{1,15},{3,1}... | collective-permute-start | bytes 516104 | tf_op jit(solution)/shard_map/ppermute | solution.py:397
  63.8 7.3 %collective-permute-start.7 = (bf16[336,256]{1,0:T(8,128)(2,1)S(1)}, bf16[336,256]{1,0:T(8,128)(2,1)S(1)}, u32[]{:S(2)}, u32[]{:S(2)}) collective-permute-start(bf16[336,256]{1,0:T(8,128)(2,1)S(1)} %collective-permute-done.5.refs_3_.refs_5_), channel_id=1, source_target_pairs={{0,2},{2,4},{4,6},{6,8},{8,10},{10,12},{12,14},{14,0},{1,3},{3,5},... | collective-permute-start | bytes 516104 | tf_op jit(solution)/shard_map/ppermute | solution.py:394
  65.7 7.3 %collective-permute-start.8 = (bf16[336,256]{1,0:T(8,128)(2,1)S(1)}, bf16[336,256]{1,0:T(8,128)(2,1)S(1)}, u32[]{:S(2)}, u32[]{:S(2)}) collective-permute-start(bf16[336,256]{1,0:T(8,128)(2,1)S(1)} %collective-permute-done.6.refs_4_.refs_6_), channel_id=1, source_target_pairs={{0,14},{2,0},{4,2},{6,4},{8,6},{10,8},{12,10},{14,12},{1,15},{3,1}... | collective-permute-start | bytes 516104 | tf_op jit(solution)/shard_map/ppermute | solution.py:397
  71.2 7.3 %collective-permute-start.9 = (bf16[336,256]{1,0:T(8,128)(2,1)S(1)}, bf16[336,256]{1,0:T(8,128)(2,1)S(1)}, u32[]{:S(2)}, u32[]{:S(2)}) collective-permute-start(bf16[336,256]{1,0:T(8,128)(2,1)S(1)} %collective-permute-done.7.refs_5_.refs_7_), channel_id=1, source_target_pairs={{0,2},{2,4},{4,6},{6,8},{8,10},{10,12},{12,14},{14,0},{1,3},{3,5},... | collective-permute-start | bytes 516104 | tf_op jit(solution)/shard_map/ppermute | solution.py:394
  73.4 42.2 %copy-start.2 = (bf16[1,4096,128]{2,1,0:T(8,128)(2,1)S(1)}, bf16[1,4096,128]{2,1,0:T(8,128)(2,1)}, u32[]{:S(2)}) copy-start(bf16[1,4096,128]{2,1,0:T(8,128)(2,1)} %param.15) | copy-start | bytes 3145732
  81.2 9.0 %collective-permute-start.10 = (bf16[320,512]{1,0:T(8,128)(2,1)S(1)}, bf16[320,512]{1,0:T(8,128)(2,1)S(1)}, u32[]{:S(2)}, u32[]{:S(2)}) collective-permute-start(bf16[320,512]{1,0:T(8,128)(2,1)S(1)} %hidden.1.refs_1_), channel_id=1, source_target_pairs={{0,2},{2,4},{4,6},{6,8},{8,10},{10,12},{12,14},{14,0},{1,3},{3,5},... | collective-permute-start | bytes 983048 | tf_op jit(solution)/shard_map/ppermute | solution.py:394
  83.1 9.0 %collective-permute-start.11 = (bf16[320,512]{1,0:T(8,128)(2,1)S(1)}, bf16[320,512]{1,0:T(8,128)(2,1)S(1)}, u32[]{:S(2)}, u32[]{:S(2)}) collective-permute-start(bf16[320,512]{1,0:T(8,128)(2,1)S(1)} %hidden.1.refs_1_), channel_id=1, source_target_pairs={{0,14},{2,0},{4,2},{6,4},{8,6},{10,8},{12,10},{14,12},{1,15},{3,1}... | collective-permute-start | bytes 983048 | tf_op jit(solution)/shard_map/ppermute | solution.py:397
  90.2 11.0 %collective-permute-start.12 = (bf16[320,512]{1,0:T(8,128)(2,1)S(1)}, bf16[320,512]{1,0:T(8,128)(2,1)S(1)}, u32[]{:S(2)}, u32[]{:S(2)}) collective-permute-start(bf16[320,512]{1,0:T(8,128)(2,1)S(1)} %collective-permute-done.10.refs_2_), channel_id=1, source_target_pairs={{0,2},{2,4},{4,6},{6,8},{8,10},{10,12},{12,14},{14,0},{1,3},{3,5},... | collective-permute-start | bytes 983048 | tf_op jit(solution)/shard_map/ppermute | solution.py:394
  92.2 11.0 %collective-permute-start.13 = (bf16[320,512]{1,0:T(8,128)(2,1)S(1)}, bf16[320,512]{1,0:T(8,128)(2,1)S(1)}, u32[]{:S(2)}, u32[]{:S(2)}) collective-permute-start(bf16[320,512]{1,0:T(8,128)(2,1)S(1)} %collective-permute-done.11.refs_3_), channel_id=1, source_target_pairs={{0,14},{2,0},{4,2},{6,4},{8,6},{10,8},{12,10},{14,12},{1,15},{3,1}... | collective-permute-start | bytes 983048 | tf_op jit(solution)/shard_map/ppermute | solution.py:397
  101.3 12.2 %collective-permute-start.14 = (bf16[320,512]{1,0:T(8,128)(2,1)S(1)}, bf16[320,512]{1,0:T(8,128)(2,1)S(1)}, u32[]{:S(2)}, u32[]{:S(2)}) collective-permute-start(bf16[320,512]{1,0:T(8,128)(2,1)S(1)} %collective-permute-done.12.refs_4_), channel_id=1, source_target_pairs={{0,2},{2,4},{4,6},{6,8},{8,10},{10,12},{12,14},{14,0},{1,3},{3,5},... | collective-permute-start | bytes 983048 | tf_op jit(solution)/shard_map/ppermute | solution.py:394
  103.2 12.4 %collective-permute-start.15 = (bf16[320,512]{1,0:T(8,128)(2,1)S(1)}, bf16[320,512]{1,0:T(8,128)(2,1)S(1)}, u32[]{:S(2)}, u32[]{:S(2)}) collective-permute-start(bf16[320,512]{1,0:T(8,128)(2,1)S(1)} %collective-permute-done.13.refs_5_), channel_id=1, source_target_pairs={{0,14},{2,0},{4,2},{6,4},{8,6},{10,8},{12,10},{14,12},{1,15},{3,1}... | collective-permute-start | bytes 983048 | tf_op jit(solution)/shard_map/ppermute | solution.py:397
  113.4 12.0 %collective-permute-start.16 = (bf16[320,512]{1,0:T(8,128)(2,1)S(1)}, bf16[320,512]{1,0:T(8,128)(2,1)S(1)}, u32[]{:S(2)}, u32[]{:S(2)}) collective-permute-start(bf16[320,512]{1,0:T(8,128)(2,1)S(1)} %collective-permute-done.14.refs_6_), channel_id=1, source_target_pairs={{0,2},{2,4},{4,6},{6,8},{8,10},{10,12},{12,14},{14,0},{1,3},{3,5},... | collective-permute-start | bytes 983048 | tf_op jit(solution)/shard_map/ppermute | solution.py:394
  126.0 16.4 %copy-start.3 = (f32[256,8]{1,0:T(8,128)S(1)}, f32[256,8]{1,0:T(8,128)}, u32[]{:S(2)}) copy-start(f32[256,8]{1,0:T(8,128)} %get-tuple-element.22.cols_ref) | copy-start | bytes 24580

commit v9 on v8

--- a/solution.py
+++ b/solution.py
@@ -149,7 +149,7 @@
 
 
 def chip_at(place_ref, offset, chips):
-    return lax.rem(place_ref[0] + (offset + chips), chips)
+    return lax.rem(place_ref[0] + offset * (1 - 2 * place_ref[1]) + chips, chips)
 
 
 def squares_kernel(*refs):
@@ -386,15 +386,21 @@
 
 def ring(value):
     chips = lax.axis_size("x")
-    onward = [(i, (i + 1) % chips) for i in range(chips)]
-    backward = [(i, (i - 1) % chips) for i in range(chips)]
+
+    def shift(step):
+        return [
+            (x * CORES + c, (x + step * (1 - 2 * c)) % chips * CORES + c)
+            for x in range(chips)
+            for c in range(CORES)
+        ]
+
     arrays = [(0, value)]
     before, after = value, value
     for step in range(1, chips // 2 + 1):
-        before = lax.ppermute(before, "x", onward)
+        before = lax.ppermute(before, ("x", "c"), shift(1))
         arrays.append((-step, before))
         if step < chips - step:
-            after = lax.ppermute(after, "x", backward)
+            after = lax.ppermute(after, ("x", "c"), shift(-1))
             arrays.append((step, after))
     return arrays
 

time: 173 us -> 168 us (0.971)
  waiting for transfers between devices: 28.8 us -> 18.9 us
  starting transfers between devices: 63.2 us -> 72.4 us
  blocking collectives: 69.2 us -> 65 us
    ppermute x14, waiting for transfers between devices: 28.8 us -> 18.9 us  [the longest x8 14.4 us: ring(): before = lax.ppermute(before, ('x', 'c'), shift(1))]
    ppermute x14, starting transfers between devices: 42.9 us -> 52.1 us  [the longest x8 40.3 us: ring(): before = lax.ppermute(before, ('x', 'c'), shift(1))]
    all_gather x1, blocking collectives: 14.3 us -> 9.72 us  [layer(): mixed = lax.all_gather(combine(blocks_exchange(result), cols), 'c', axis=0)]
where the time goes in v9:
time: 168 us; the launch traced here: 167 us
  starting transfers between devices  72.4 us (43%)
  blocking collectives  65 us (39%)
  waiting for transfers between devices  18.9 us (11%)
  Pallas kernels  10.6 us (6%)
    all_to_all x3, blocking collectives, exchange(): return lax.all_to_all(value, axis, split_axis=0, concat_axis=0, tiled=True)  53.4 us
    ppermute x8, starting transfers between devices, ring(): before = lax.ppermute(before, ('x', 'c'), shift(1))  40.3 us
    ppermute x3, starting transfers between devices, swap(): return lax.ppermute(value, 'c', [(0, 1), (1, 0)])  20.3 us
    ppermute x8, waiting for transfers between devices, ring(): before = lax.ppermute(before, ('x', 'c'), shift(1))  14.4 us
    ppermute x6, starting transfers between devices, ring(): after = lax.ppermute(after, ('x', 'c'), shift(-1))  11.8 us
    all_gather x1, blocking collectives, layer(): mixed = lax.all_gather(combine(blocks_exchange(result), cols), 'c', axis=0)  9.72 us
    ppermute x6, waiting for transfers between devices, ring(): after = lax.ppermute(after, ('x', 'c'), shift(-1))  4.48 us
  transfers between devices with their start and end apart: 17, of which 10 were waited for; matrix products, arithmetic and copies ran while one was open for 0% of the time, Pallas kernels for 3%

profile of v9, /device:TPU:1, one launch (start us, length us, event | category | flops | bytes accessed | tf_op | source)
XLA Modules:
  0.0 167.3 jit_solution(17722436866116433131)
XLA Ops:
  0.0 16.0 %collective-permute-start = (bf16[2048,256]{1,0:T(8,128)(2,1)}, bf16[2048,256]{1,0:T(8,128)(2,1)S(1)}, u32[]{:S(2)}, u32[]{:S(2)}) collective-permute-start(bf16[2048,256]{1,0:T(8,128)(2,1)} %bitcast.18), channel_id=1, source_target_pairs={{0,1},{1,0},{2,3},{3,2},{4,5},{5,4},{6,7},{7,6},{8,9},{9,8},{10,11... | collective-permute-start | bytes 3145736 | tf_op jit(solution)/shard_map/ppermute | solution.py:384
  16.0 1.9 %collective-permute-start.1 = (bf16[2048,256]{1,0:T(8,128)(2,1)}, bf16[2048,256]{1,0:T(8,128)(2,1)S(1)}, u32[]{:S(2)}, u32[]{:S(2)}) collective-permute-start(bf16[2048,256]{1,0:T(8,128)(2,1)} %bitcast.20), channel_id=1, source_target_pairs={{0,1},{1,0},{2,3},{3,2},{4,5},{5,4},{6,7},{7,6},{8,9},{9,8},{10,11... | collective-permute-start | bytes 3145736 | tf_op jit(solution)/shard_map/ppermute | solution.py:384
  18.0 2.4 %collective-permute-start.2 = (bf16[4096,128]{1,0:T(8,128)(2,1)}, bf16[4096,128]{1,0:T(8,128)(2,1)S(1)}, u32[]{:S(2)}, u32[]{:S(2)}) collective-permute-start(bf16[4096,128]{1,0:T(8,128)(2,1)} %bitcast.22), channel_id=1, source_target_pairs={{0,1},{1,0},{2,3},{3,2},{4,5},{5,4},{6,7},{7,6},{8,9},{9,8},{10,11... | collective-permute-start | bytes 3145736 | tf_op jit(solution)/shard_map/ppermute | solution.py:384
  21.2 1.9 %all-gather = bf16[544,128]{1,0:T(8,128)(2,1)S(1)} all-gather(bf16[272,128]{1,0:T(8,128)(2,1)S(1)} %prepare.1), channel_id=2, replica_groups=mesh['ep'=64,'x'=8,'c'=2] {'c'}, dimensions={0}, use_global_device_ids=true | all-gather | bytes 208896 | tf_op jit(solution)/shard_map/all_gather | solution.py:419
  23.2 1.8 %dispatch.1 = (bf16[512,256]{1,0:T(8,128)(2,1)S(1)}, f32[256,8]{1,0:T(8,128)}) custom-call(s32[2]{0:T(128)S(1)} %pad_add_fusion.refs_0_.place_ref, bf16[2,272,128]{2,1,0:T(8,128)(2,1)S(1)} %bitcast.16, s32[2,256]{1,0:T(2,128)} %bitcast.28, f32[2,256]{1,0:T(2,128)} %bitcast.29), custom_call_target="tpu_custom_call" | custom-call | tf_op jit(solution)/shard_map/dispatch/pallas_call | solution.py:97
  25.0 23.7 %all_to_all.15 = bf16[64,8,256]{2,1,0:T(8,128)(2,1)S(1)} all-to-all(bf16[64,8,256]{2,1,0:T(8,128)(2,1)S(1)} %bitcast.27), channel_id=1, replica_groups=mesh['ep'=64,'x'=8,'c'=2] {'ep'}, dimensions={0} | all-to-all | bytes 524288 | tf_op jit(solution)/shard_map/all_to_all | solution.py:375
  49.0 4.6 %collective-permute-start.3 = (bf16[336,256]{1,0:T(8,128)(2,1)S(1)}, bf16[336,256]{1,0:T(8,128)(2,1)S(1)}, u32[]{:S(2)}, u32[]{:S(2)}) collective-permute-start(bf16[336,256]{1,0:T(8,128)(2,1)S(1)} %arrange.1.refs_0_.refs_2_), channel_id=1, source_target_pairs={{0,2},{1,15},{2,4},{3,1},{4,6},{5,3},{6,8},{7,5},{8,10},{9,7},{10,... | collective-permute-start | bytes 516104 | tf_op jit(solution)/shard_map/ppermute | solution.py:400
  53.6 1.9 %collective-permute-start.4 = (bf16[336,256]{1,0:T(8,128)(2,1)S(1)}, bf16[336,256]{1,0:T(8,128)(2,1)S(1)}, u32[]{:S(2)}, u32[]{:S(2)}) collective-permute-start(bf16[336,256]{1,0:T(8,128)(2,1)S(1)} %arrange.1.refs_0_.refs_2_), channel_id=1, source_target_pairs={{0,14},{1,3},{2,0},{3,5},{4,2},{5,7},{6,4},{7,9},{8,6},{9,11},{10,... | collective-permute-start | bytes 516104 | tf_op jit(solution)/shard_map/ppermute | solution.py:403
  55.9 5.0 %collective-permute-start.5 = (bf16[336,256]{1,0:T(8,128)(2,1)S(1)}, bf16[336,256]{1,0:T(8,128)(2,1)S(1)}, u32[]{:S(2)}, u32[]{:S(2)}) collective-permute-start(bf16[336,256]{1,0:T(8,128)(2,1)S(1)} %collective-permute-done.3.refs_1_.refs_3_), channel_id=1, source_target_pairs={{0,2},{1,15},{2,4},{3,1},{4,6},{5,3},{6,8},{7,5},{8,10},{9,7},{10,... | collective-permute-start | bytes 516104 | tf_op jit(solution)/shard_map/ppermute | solution.py:400
  61.2 2.2 %collective-permute-start.6 = (bf16[336,256]{1,0:T(8,128)(2,1)S(1)}, bf16[336,256]{1,0:T(8,128)(2,1)S(1)}, u32[]{:S(2)}, u32[]{:S(2)}) collective-permute-start(bf16[336,256]{1,0:T(8,128)(2,1)S(1)} %collective-permute-done.4.refs_2_.refs_4_), channel_id=1, source_target_pairs={{0,14},{1,3},{2,0},{3,5},{4,2},{5,7},{6,4},{7,9},{8,6},{9,11},{10,... | collective-permute-start | bytes 516104 | tf_op jit(solution)/shard_map/ppermute | solution.py:403
  63.4 4.9 %collective-permute-start.7 = (bf16[336,256]{1,0:T(8,128)(2,1)S(1)}, bf16[336,256]{1,0:T(8,128)(2,1)S(1)}, u32[]{:S(2)}, u32[]{:S(2)}) collective-permute-start(bf16[336,256]{1,0:T(8,128)(2,1)S(1)} %collective-permute-done.5.refs_3_.refs_5_), channel_id=1, source_target_pairs={{0,2},{1,15},{2,4},{3,1},{4,6},{5,3},{6,8},{7,5},{8,10},{9,7},{10,... | collective-permute-start | bytes 516104 | tf_op jit(solution)/shard_map/ppermute | solution.py:400
  68.3 1.7 collective-permute-done.6.refs_4_.refs_6_
  70.0 1.9 %collective-permute-start.8 = (bf16[336,256]{1,0:T(8,128)(2,1)S(1)}, bf16[336,256]{1,0:T(8,128)(2,1)S(1)}, u32[]{:S(2)}, u32[]{:S(2)}) collective-permute-start(bf16[336,256]{1,0:T(8,128)(2,1)S(1)} %collective-permute-done.6.refs_4_.refs_6_), channel_id=1, source_target_pairs={{0,14},{1,3},{2,0},{3,5},{4,2},{5,7},{6,4},{7,9},{8,6},{9,11},{10,... | collective-permute-start | bytes 516104 | tf_op jit(solution)/shard_map/ppermute | solution.py:403
  71.9 4.9 %collective-permute-start.9 = (bf16[336,256]{1,0:T(8,128)(2,1)S(1)}, bf16[336,256]{1,0:T(8,128)(2,1)S(1)}, u32[]{:S(2)}, u32[]{:S(2)}) collective-permute-start(bf16[336,256]{1,0:T(8,128)(2,1)S(1)} %collective-permute-done.7.refs_5_.refs_7_), channel_id=1, source_target_pairs={{0,2},{1,15},{2,4},{3,1},{4,6},{5,3},{6,8},{7,5},{8,10},{9,7},{10,... | collective-permute-start | bytes 516104 | tf_op jit(solution)/shard_map/ppermute | solution.py:400
  76.8 2.0 %collective-permute-done.8.refs_6_.refs_8_ = bf16[336,256]{1,0:T(8,128)(2,1)S(1)} collective-permute-done((bf16[336,256]{1,0:T(8,128)(2,1)S(1)}, bf16[336,256]{1,0:T(8,128)(2,1)S(1)}, u32[]{:S(2)}, u32[]{:S(2)}) %collective-permute-start.8) | collective-permute-done | bytes 172064 | tf_op jit(solution)/shard_map/ppermute | solution.py:403
  80.2 2.7 %hidden.1.refs_1_ = bf16[320,512]{1,0:T(8,128)(2,1)S(1)} custom-call(s32[2]{0:T(128)S(1)} %pad_add_fusion.refs_0_.place_ref, f32[320,256]{1,0:T(8,128)S(1)} %squares.1.refs_1_, bf16[336,256]{1,0:T(8,128)(2,1)S(1)} %arrange.1.refs_0_.refs_2_, bf16[336,256]{1,0:T(8,128)(2,1)S(1)} %collective-permute-done.3.refs_1_.refs_3_, ...), custom_call_target="tpu_custom_call" | custom-call | tf_op jit(solution)/shard_map/hidden/pallas_call | solution.py:216
  82.9 5.3 %collective-permute-start.10 = (bf16[320,512]{1,0:T(8,128)(2,1)S(1)}, bf16[320,512]{1,0:T(8,128)(2,1)S(1)}, u32[]{:S(2)}, u32[]{:S(2)}) collective-permute-start(bf16[320,512]{1,0:T(8,128)(2,1)S(1)} %hidden.1.refs_1_), channel_id=1, source_target_pairs={{0,2},{1,15},{2,4},{3,1},{4,6},{5,3},{6,8},{7,5},{8,10},{9,7},{10,... | collective-permute-start | bytes 983048 | tf_op jit(solution)/shard_map/ppermute | solution.py:400
  88.2 1.9 %collective-permute-start.11 = (bf16[320,512]{1,0:T(8,128)(2,1)S(1)}, bf16[320,512]{1,0:T(8,128)(2,1)S(1)}, u32[]{:S(2)}, u32[]{:S(2)}) collective-permute-start(bf16[320,512]{1,0:T(8,128)(2,1)S(1)} %hidden.1.refs_1_), channel_id=1, source_target_pairs={{0,14},{1,3},{2,0},{3,5},{4,2},{5,7},{6,4},{7,9},{8,6},{9,11},{10,... | collective-permute-start | bytes 983048 | tf_op jit(solution)/shard_map/ppermute | solution.py:403
  90.2 2.1 %collective-permute-done.10.refs_2_ = bf16[320,512]{1,0:T(8,128)(2,1)S(1)} collective-permute-done((bf16[320,512]{1,0:T(8,128)(2,1)S(1)}, bf16[320,512]{1,0:T(8,128)(2,1)S(1)}, u32[]{:S(2)}, u32[]{:S(2)}) %collective-permute-start.10) | collective-permute-done | bytes 327712 | tf_op jit(solution)/shard_map/ppermute | solution.py:400
  92.2 5.0 %collective-permute-start.12 = (bf16[320,512]{1,0:T(8,128)(2,1)S(1)}, bf16[320,512]{1,0:T(8,128)(2,1)S(1)}, u32[]{:S(2)}, u32[]{:S(2)}) collective-permute-start(bf16[320,512]{1,0:T(8,128)(2,1)S(1)} %collective-permute-done.10.refs_2_), channel_id=1, source_target_pairs={{0,2},{1,15},{2,4},{3,1},{4,6},{5,3},{6,8},{7,5},{8,10},{9,7},{10,... | collective-permute-start | bytes 983048 | tf_op jit(solution)/shard_map/ppermute | solution.py:400
  97.8 1.9 %collective-permute-start.13 = (bf16[320,512]{1,0:T(8,128)(2,1)S(1)}, bf16[320,512]{1,0:T(8,128)(2,1)S(1)}, u32[]{:S(2)}, u32[]{:S(2)}) collective-permute-start(bf16[320,512]{1,0:T(8,128)(2,1)S(1)} %collective-permute-done.11.refs_3_), channel_id=1, source_target_pairs={{0,14},{1,3},{2,0},{3,5},{4,2},{5,7},{6,4},{7,9},{8,6},{9,11},{10,... | collective-permute-start | bytes 983048 | tf_op jit(solution)/shard_map/ppermute | solution.py:403
  99.7 4.0 %collective-permute-done.12.refs_4_ = bf16[320,512]{1,0:T(8,128)(2,1)S(1)} collective-permute-done((bf16[320,512]{1,0:T(8,128)(2,1)S(1)}, bf16[320,512]{1,0:T(8,128)(2,1)S(1)}, u32[]{:S(2)}, u32[]{:S(2)}) %collective-permute-start.12) | collective-permute-done | bytes 327712 | tf_op jit(solution)/shard_map/ppermute | solution.py:400
  103.7 5.3 %collective-permute-start.14 = (bf16[320,512]{1,0:T(8,128)(2,1)S(1)}, bf16[320,512]{1,0:T(8,128)(2,1)S(1)}, u32[]{:S(2)}, u32[]{:S(2)}) collective-permute-start(bf16[320,512]{1,0:T(8,128)(2,1)S(1)} %collective-permute-done.12.refs_4_), channel_id=1, source_target_pairs={{0,2},{1,15},{2,4},{3,1},{4,6},{5,3},{6,8},{7,5},{8,10},{9,7},{10,... | collective-permute-start | bytes 983048 | tf_op jit(solution)/shard_map/ppermute | solution.py:400
  109.1 1.9 %collective-permute-start.15 = (bf16[320,512]{1,0:T(8,128)(2,1)S(1)}, bf16[320,512]{1,0:T(8,128)(2,1)S(1)}, u32[]{:S(2)}, u32[]{:S(2)}) collective-permute-start(bf16[320,512]{1,0:T(8,128)(2,1)S(1)} %collective-permute-done.13.refs_5_), channel_id=1, source_target_pairs={{0,14},{1,3},{2,0},{3,5},{4,2},{5,7},{6,4},{7,9},{8,6},{9,11},{10,... | collective-permute-start | bytes 983048 | tf_op jit(solution)/shard_map/ppermute | solution.py:403
  111.0 3.7 %collective-permute-done.14.refs_6_ = bf16[320,512]{1,0:T(8,128)(2,1)S(1)} collective-permute-done((bf16[320,512]{1,0:T(8,128)(2,1)S(1)}, bf16[320,512]{1,0:T(8,128)(2,1)S(1)}, u32[]{:S(2)}, u32[]{:S(2)}) %collective-permute-start.14) | collective-permute-done | bytes 327712 | tf_op jit(solution)/shard_map/ppermute | solution.py:400
  114.7 5.3 %collective-permute-start.16 = (bf16[320,512]{1,0:T(8,128)(2,1)S(1)}, bf16[320,512]{1,0:T(8,128)(2,1)S(1)}, u32[]{:S(2)}, u32[]{:S(2)}) collective-permute-start(bf16[320,512]{1,0:T(8,128)(2,1)S(1)} %collective-permute-done.14.refs_6_), channel_id=1, source_target_pairs={{0,2},{1,15},{2,4},{3,1},{4,6},{5,3},{6,8},{7,5},{8,10},{9,7},{10,... | collective-permute-start | bytes 983048 | tf_op jit(solution)/shard_map/ppermute | solution.py:400
  120.0 1.7 %down_early.1 = (f32[320,256]{1,0:T(8,128)S(1)}, bf16[512,256]{1,0:T(8,128)(2,1)S(1)}) custom-call(s32[2]{0:T(128)S(1)} %pad_add_fusion.refs_0_.place_ref, bf16[320,512]{1,0:T(8,128)(2,1)S(1)} %hidden.1.refs_1_, bf16[320,512]{1,0:T(8,128)(2,1)S(1)} %collective-permute-done.10.refs_2_, bf16[320,512]{1,0:T(8,128)(2,1)S(1)} %collective-permute-done.11.refs_3_, ...), custom_call_target="tpu_custom_call" | custom-call | tf_op jit(solution)/shard_map/down_early/pallas_call | solution.py:260
  121.7 3.1 %collective-permute-done.16.refs_2_ = bf16[320,512]{1,0:T(8,128)(2,1)S(1)} collective-permute-done((bf16[320,512]{1,0:T(8,128)(2,1)S(1)}, bf16[320,512]{1,0:T(8,128)(2,1)S(1)}, u32[]{:S(2)}, u32[]{:S(2)}) %collective-permute-start.16) | collective-permute-done | bytes 327712 | tf_op jit(solution)/shard_map/ppermute | solution.py:400
  125.3 18.7 %all_to_all.16 = bf16[64,8,256]{2,1,0:T(8,128)(2,1)S(1)} all-to-all(bf16[64,8,256]{2,1,0:T(8,128)(2,1)S(1)} %bitcast.26), channel_id=1, replica_groups=mesh['ep'=64,'x'=8,'c'=2] {'ep'}, dimensions={0} | all-to-all | bytes 524288 | tf_op jit(solution)/shard_map/all_to_all | solution.py:375
  144.3 9.7 %all-gather.1 = f32[512,256]{1,0:T(8,128)S(1)} all-gather(f32[256,256]{1,0:T(8,128)S(1)} %combine.1), channel_id=3, replica_groups=mesh['ep'=64,'x'=8,'c'=2] {'c'}, dimensions={0}, use_global_device_ids=true | all-gather | bytes 786432 | tf_op jit(solution)/shard_map/all_gather | solution.py:439
  154.7 11.0 %all_to_all.17.sums_ref = f32[8,1,256]{2,1,0:T(1,128)S(1)} all-to-all(f32[8,1,256]{2,1,0:T(1,128)S(1)} %get-tuple-element.24), channel_id=1, replica_groups=mesh['ep'=64,'x'=8,'c'=2] {'x'}, dimensions={0} | all-to-all | bytes 16384 | tf_op jit(solution)/shard_map/all_to_all | solution.py:375
  165.8 1.6 final.1
  (26 shorter events, 5.4 us)
Async XLA Ops:
  0.0 48.7 %collective-permute-start = (bf16[2048,256]{1,0:T(8,128)(2,1)}, bf16[2048,256]{1,0:T(8,128)(2,1)S(1)}, u32[]{:S(2)}, u32[]{:S(2)}) collective-permute-start(bf16[2048,256]{1,0:T(8,128)(2,1)} %bitcast.18), channel_id=1, source_target_pairs={{0,1},{1,0},{2,3},{3,2},{4,5},{5,4},{6,7},{7,6},{8,9},{9,8},{10,11... | collective-permute-start | bytes 3145736 | tf_op jit(solution)/shard_map/ppermute | solution.py:384
  16.0 32.7 %collective-permute-start.1 = (bf16[2048,256]{1,0:T(8,128)(2,1)}, bf16[2048,256]{1,0:T(8,128)(2,1)S(1)}, u32[]{:S(2)}, u32[]{:S(2)}) collective-permute-start(bf16[2048,256]{1,0:T(8,128)(2,1)} %bitcast.20), channel_id=1, source_target_pairs={{0,1},{1,0},{2,3},{3,2},{4,5},{5,4},{6,7},{7,6},{8,9},{9,8},{10,11... | collective-permute-start | bytes 3145736 | tf_op jit(solution)/shard_map/ppermute | solution.py:384
  18.0 30.8 %collective-permute-start.2 = (bf16[4096,128]{1,0:T(8,128)(2,1)}, bf16[4096,128]{1,0:T(8,128)(2,1)S(1)}, u32[]{:S(2)}, u32[]{:S(2)}) collective-permute-start(bf16[4096,128]{1,0:T(8,128)(2,1)} %bitcast.22), channel_id=1, source_target_pairs={{0,1},{1,0},{2,3},{3,2},{4,5},{5,4},{6,7},{7,6},{8,9},{9,8},{10,11... | collective-permute-start | bytes 3145736 | tf_op jit(solution)/shard_map/ppermute | solution.py:384
  48.8 31.5 %copy-start = (bf16[1,2048,256]{2,1,0:T(8,128)(2,1)S(1)}, bf16[1,2048,256]{2,1,0:T(8,128)(2,1)}, u32[]{:S(2)}) copy-start(bf16[1,2048,256]{2,1,0:T(8,128)(2,1)} %param.13) | copy-start | bytes 3145732
  48.8 31.5 %copy-start.1 = (bf16[1,2048,256]{2,1,0:T(8,128)(2,1)S(1)}, bf16[1,2048,256]{2,1,0:T(8,128)(2,1)}, u32[]{:S(2)}) copy-start(bf16[1,2048,256]{2,1,0:T(8,128)(2,1)} %param.14) | copy-start | bytes 3145732
  49.0 7.0 %collective-permute-start.3 = (bf16[336,256]{1,0:T(8,128)(2,1)S(1)}, bf16[336,256]{1,0:T(8,128)(2,1)S(1)}, u32[]{:S(2)}, u32[]{:S(2)}) collective-permute-start(bf16[336,256]{1,0:T(8,128)(2,1)S(1)} %arrange.1.refs_0_.refs_2_), channel_id=1, source_target_pairs={{0,2},{1,15},{2,4},{3,1},{4,6},{5,3},{6,8},{7,5},{8,10},{9,7},{10,... | collective-permute-start | bytes 516104 | tf_op jit(solution)/shard_map/ppermute | solution.py:400
  53.6 7.6 %collective-permute-start.4 = (bf16[336,256]{1,0:T(8,128)(2,1)S(1)}, bf16[336,256]{1,0:T(8,128)(2,1)S(1)}, u32[]{:S(2)}, u32[]{:S(2)}) collective-permute-start(bf16[336,256]{1,0:T(8,128)(2,1)S(1)} %arrange.1.refs_0_.refs_2_), channel_id=1, source_target_pairs={{0,14},{1,3},{2,0},{3,5},{4,2},{5,7},{6,4},{7,9},{8,6},{9,11},{10,... | collective-permute-start | bytes 516104 | tf_op jit(solution)/shard_map/ppermute | solution.py:403
  55.9 7.5 %collective-permute-start.5 = (bf16[336,256]{1,0:T(8,128)(2,1)S(1)}, bf16[336,256]{1,0:T(8,128)(2,1)S(1)}, u32[]{:S(2)}, u32[]{:S(2)}) collective-permute-start(bf16[336,256]{1,0:T(8,128)(2,1)S(1)} %collective-permute-done.3.refs_1_.refs_3_), channel_id=1, source_target_pairs={{0,2},{1,15},{2,4},{3,1},{4,6},{5,3},{6,8},{7,5},{8,10},{9,7},{10,... | collective-permute-start | bytes 516104 | tf_op jit(solution)/shard_map/ppermute | solution.py:400
  61.2 8.8 %collective-permute-start.6 = (bf16[336,256]{1,0:T(8,128)(2,1)S(1)}, bf16[336,256]{1,0:T(8,128)(2,1)S(1)}, u32[]{:S(2)}, u32[]{:S(2)}) collective-permute-start(bf16[336,256]{1,0:T(8,128)(2,1)S(1)} %collective-permute-done.4.refs_2_.refs_4_), channel_id=1, source_target_pairs={{0,14},{1,3},{2,0},{3,5},{4,2},{5,7},{6,4},{7,9},{8,6},{9,11},{10,... | collective-permute-start | bytes 516104 | tf_op jit(solution)/shard_map/ppermute | solution.py:403
  63.4 8.5 %collective-permute-start.7 = (bf16[336,256]{1,0:T(8,128)(2,1)S(1)}, bf16[336,256]{1,0:T(8,128)(2,1)S(1)}, u32[]{:S(2)}, u32[]{:S(2)}) collective-permute-start(bf16[336,256]{1,0:T(8,128)(2,1)S(1)} %collective-permute-done.5.refs_3_.refs_5_), channel_id=1, source_target_pairs={{0,2},{1,15},{2,4},{3,1},{4,6},{5,3},{6,8},{7,5},{8,10},{9,7},{10,... | collective-permute-start | bytes 516104 | tf_op jit(solution)/shard_map/ppermute | solution.py:400
  70.0 8.8 %collective-permute-start.8 = (bf16[336,256]{1,0:T(8,128)(2,1)S(1)}, bf16[336,256]{1,0:T(8,128)(2,1)S(1)}, u32[]{:S(2)}, u32[]{:S(2)}) collective-permute-start(bf16[336,256]{1,0:T(8,128)(2,1)S(1)} %collective-permute-done.6.refs_4_.refs_6_), channel_id=1, source_target_pairs={{0,14},{1,3},{2,0},{3,5},{4,2},{5,7},{6,4},{7,9},{8,6},{9,11},{10,... | collective-permute-start | bytes 516104 | tf_op jit(solution)/shard_map/ppermute | solution.py:403
  71.9 8.3 %collective-permute-start.9 = (bf16[336,256]{1,0:T(8,128)(2,1)S(1)}, bf16[336,256]{1,0:T(8,128)(2,1)S(1)}, u32[]{:S(2)}, u32[]{:S(2)}) collective-permute-start(bf16[336,256]{1,0:T(8,128)(2,1)S(1)} %collective-permute-done.7.refs_5_.refs_7_), channel_id=1, source_target_pairs={{0,2},{1,15},{2,4},{3,1},{4,6},{5,3},{6,8},{7,5},{8,10},{9,7},{10,... | collective-permute-start | bytes 516104 | tf_op jit(solution)/shard_map/ppermute | solution.py:400
  79.0 41.0 %copy-start.2 = (bf16[1,4096,128]{2,1,0:T(8,128)(2,1)S(1)}, bf16[1,4096,128]{2,1,0:T(8,128)(2,1)}, u32[]{:S(2)}) copy-start(bf16[1,4096,128]{2,1,0:T(8,128)(2,1)} %param.15) | copy-start | bytes 3145732
  82.9 9.3 %collective-permute-start.10 = (bf16[320,512]{1,0:T(8,128)(2,1)S(1)}, bf16[320,512]{1,0:T(8,128)(2,1)S(1)}, u32[]{:S(2)}, u32[]{:S(2)}) collective-permute-start(bf16[320,512]{1,0:T(8,128)(2,1)S(1)} %hidden.1.refs_1_), channel_id=1, source_target_pairs={{0,2},{1,15},{2,4},{3,1},{4,6},{5,3},{6,8},{7,5},{8,10},{9,7},{10,... | collective-permute-start | bytes 983048 | tf_op jit(solution)/shard_map/ppermute | solution.py:400
  88.2 9.6 %collective-permute-start.11 = (bf16[320,512]{1,0:T(8,128)(2,1)S(1)}, bf16[320,512]{1,0:T(8,128)(2,1)S(1)}, u32[]{:S(2)}, u32[]{:S(2)}) collective-permute-start(bf16[320,512]{1,0:T(8,128)(2,1)S(1)} %hidden.1.refs_1_), channel_id=1, source_target_pairs={{0,14},{1,3},{2,0},{3,5},{4,2},{5,7},{6,4},{7,9},{8,6},{9,11},{10,... | collective-permute-start | bytes 983048 | tf_op jit(solution)/shard_map/ppermute | solution.py:403
  92.2 11.5 %collective-permute-start.12 = (bf16[320,512]{1,0:T(8,128)(2,1)S(1)}, bf16[320,512]{1,0:T(8,128)(2,1)S(1)}, u32[]{:S(2)}, u32[]{:S(2)}) collective-permute-start(bf16[320,512]{1,0:T(8,128)(2,1)S(1)} %collective-permute-done.10.refs_2_), channel_id=1, source_target_pairs={{0,2},{1,15},{2,4},{3,1},{4,6},{5,3},{6,8},{7,5},{8,10},{9,7},{10,... | collective-permute-start | bytes 983048 | tf_op jit(solution)/shard_map/ppermute | solution.py:400
  97.8 11.2 %collective-permute-start.13 = (bf16[320,512]{1,0:T(8,128)(2,1)S(1)}, bf16[320,512]{1,0:T(8,128)(2,1)S(1)}, u32[]{:S(2)}, u32[]{:S(2)}) collective-permute-start(bf16[320,512]{1,0:T(8,128)(2,1)S(1)} %collective-permute-done.11.refs_3_), channel_id=1, source_target_pairs={{0,14},{1,3},{2,0},{3,5},{4,2},{5,7},{6,4},{7,9},{8,6},{9,11},{10,... | collective-permute-start | bytes 983048 | tf_op jit(solution)/shard_map/ppermute | solution.py:403
  103.7 10.9 %collective-permute-start.14 = (bf16[320,512]{1,0:T(8,128)(2,1)S(1)}, bf16[320,512]{1,0:T(8,128)(2,1)S(1)}, u32[]{:S(2)}, u32[]{:S(2)}) collective-permute-start(bf16[320,512]{1,0:T(8,128)(2,1)S(1)} %collective-permute-done.12.refs_4_), channel_id=1, source_target_pairs={{0,2},{1,15},{2,4},{3,1},{4,6},{5,3},{6,8},{7,5},{8,10},{9,7},{10,... | collective-permute-start | bytes 983048 | tf_op jit(solution)/shard_map/ppermute | solution.py:400
  109.1 10.9 %collective-permute-start.15 = (bf16[320,512]{1,0:T(8,128)(2,1)S(1)}, bf16[320,512]{1,0:T(8,128)(2,1)S(1)}, u32[]{:S(2)}, u32[]{:S(2)}) collective-permute-start(bf16[320,512]{1,0:T(8,128)(2,1)S(1)} %collective-permute-done.13.refs_5_), channel_id=1, source_target_pairs={{0,14},{1,3},{2,0},{3,5},{4,2},{5,7},{6,4},{7,9},{8,6},{9,11},{10,... | collective-permute-start | bytes 983048 | tf_op jit(solution)/shard_map/ppermute | solution.py:403
  114.7 10.1 %collective-permute-start.16 = (bf16[320,512]{1,0:T(8,128)(2,1)S(1)}, bf16[320,512]{1,0:T(8,128)(2,1)S(1)}, u32[]{:S(2)}, u32[]{:S(2)}) collective-permute-start(bf16[320,512]{1,0:T(8,128)(2,1)S(1)} %collective-permute-done.14.refs_6_), channel_id=1, source_target_pairs={{0,2},{1,15},{2,4},{3,1},{4,6},{5,3},{6,8},{7,5},{8,10},{9,7},{10,... | collective-permute-start | bytes 983048 | tf_op jit(solution)/shard_map/ppermute | solution.py:400
  125.3 18.7 %copy-start.3 = (f32[256,8]{1,0:T(8,128)S(1)}, f32[256,8]{1,0:T(8,128)}, u32[]{:S(2)}) copy-start(f32[256,8]{1,0:T(8,128)} %get-tuple-element.22.cols_ref) | copy-start | bytes 24580

commit v10 on v9

--- a/solution.py
+++ b/solution.py
@@ -152,11 +152,18 @@
     return lax.rem(place_ref[0] + offset * (1 - 2 * place_ref[1]) + chips, chips)
 
 
+def blocks_of(refs):
+    blocks = []
+    for ref in refs:
+        blocks += [ref] if len(ref.shape) == 2 else [ref.at[i] for i in range(ref.shape[0])]
+    return blocks
+
+
 def squares_kernel(*refs):
     *feat_refs, out_ref = refs
     rows = out_ref.shape[0]
     total = jnp.zeros(out_ref.shape, jnp.float32)
-    for ref in feat_refs:
+    for ref in blocks_of(feat_refs):
         part = ref[0:rows, :].astype(jnp.float32)
         total = total + part * part
     out_ref[...] = total
@@ -172,17 +179,21 @@
     )(*arrays)
 
 
-def hidden_kernel(*refs, offsets):
+def hidden_kernel(*refs, offsets, count):
     chips = len(offsets)
     place_ref, squares_ref, *rest = refs
-    feat_refs, weight_refs, (out_ref, normed_ref) = rest[:chips], rest[chips:-2], rest[-2:]
+    feat_refs, weight_refs, (out_ref, normed_ref) = rest[:count], rest[count:-2], rest[-2:]
     rows, wide = squares_ref.shape
     units = weight_refs[0].shape[1]
-    part = feat_refs[-1][0:rows, :].astype(jnp.float32)
-    total = squares_ref[...] + part * part
+    total = squares_ref[...]
+    for ref in blocks_of(feat_refs[-1:]):
+        part = ref[0:rows, :].astype(jnp.float32)
+        total = total + part * part
     scale = lax.rsqrt(jnp.sum(total, axis=1, keepdims=True) / (chips * wide) + epsilon)
-    for offset, ref in zip(offsets, feat_refs):
-        begin = pl.multiple_of(chip_at(place_ref, offset, chips) * wide, wide)
+    sign = 1 - 2 * lax.rem(place_ref[0] + place_ref[1], 2)
+    for offset, ref in zip(offsets, blocks_of(feat_refs)):
+        chip = lax.rem(place_ref[0] + offset * sign + chips, chips)
+        begin = pl.multiple_of(chip * wide, wide)
         pieces = ref[rows:, :].astype(jnp.float32)
         gain = pieces[0:1, :] + pieces[1:2, :] + pieces[2:3, :]
         part = ref[0:rows, :].astype(jnp.float32)
@@ -204,20 +215,18 @@
             out_ref[:, (1 - c) * units : (2 - c) * units] = other
 
 
-def hidden_of(place, squares, features, weights):
-    offsets = [offset for offset, _ in features]
-    arrays = [array for _, array in features]
+def hidden_of(place, squares, offsets, arrays, weights):
     rows, wide = squares.shape
     units = weights[0].shape[1]
 
     def body(*refs):
-        hidden_kernel(*refs, offsets=offsets)
+        hidden_kernel(*refs, offsets=offsets, count=len(arrays))
 
     return pl.pallas_call(
         body,
         in_specs=[whole(pltpu.SMEM)] + [whole()] * (1 + len(arrays) + len(weights)),
         out_shape=jax.ShapeDtypeStruct((rows, CORES * units), jnp.bfloat16),
-        scratch_shapes=[pltpu.VMEM((rows, len(arrays) * wide), jnp.bfloat16)],
+        scratch_shapes=[pltpu.VMEM((rows, len(offsets) * wide), jnp.bfloat16)],
         compiler_params=params(16),
         name="hidden",
     )(place, squares, *arrays, *weights)
@@ -403,6 +412,27 @@
             after = lax.ppermute(after, ("x", "c"), shift(-1))
             arrays.append((step, after))
     return arrays
+
+
+def neighbours(value):
+    chips = lax.axis_size("x")
+
+    def partner(step):
+        return [
+            (x * CORES + c, (x + step * (1 - 2 * ((x + c) % 2))) % chips * CORES + c)
+            for x in range(chips)
+            for c in range(CORES)
+        ]
+
+    first = lax.ppermute(value, ("x", "c"), partner(1))
+    offsets, arrays = [0, 1], [value, first]
+    moving, side, low, high = jnp.stack([value, first]), -1, 1, 2
+    while len(offsets) < chips:
+        moving = lax.ppermute(moving, ("x", "c"), partner(side))
+        arrays.append(moving)
+        offsets += [side * low, side * high]
+        side, low, high = -side, low + 1, high + 1
+    return offsets, arrays
 
 
 def layer(
@@ -430,16 +460,16 @@
     for weight in (gate0, up0, down0):
         swapped.append(swap(weight))
     arrived, gate1, up1, down1 = lax.optimization_barrier((arrived, *swapped))
-    features = ring(arrange(arrived, both, half))
-    squares = squares_of([array for _, array in features[:-1]])
-    hidden = hidden_of(place, squares, features, (gate0, up0, gate1, up1))
+    offsets, features = neighbours(arrange(arrived, both, half))
+    squares = squares_of(features[:-1])
+    hidden = hidden_of(place, squares, offsets, features, (gate0, up0, gate1, up1))
     *early, (last, hidden) = ring(hidden)
     summed = down_early(place, early, last, down0, down1, chips)
     result = down_last(summed, hidden, half)
     mixed = lax.all_gather(combine(blocks_exchange(result), cols), "c", axis=0)
     mixed, sums = sums_of(place, mixed, chips)
     sums = exchange(sums, "x")
-    return final(mixed, sums, in_hbm(post_gain[None, :]))
+    return final(mixed, sums, post_gain[None, :])
 
 
 def solution(mesh):

time: 168 us -> 169 us (level)
  waiting for transfers between devices: 18.9 us -> 33.6 us
  starting transfers between devices: 72.4 us -> 59.2 us
    ppermute x8 -> x4, starting transfers between devices: 40.3 us -> 20.1 us  [ring(): before = lax.ppermute(before, ('x', 'c'), shift(1))]
    ppermute x0 -> x4, waiting for transfers between devices: none -> 19.4 us  [the longest x3 16.6 us: neighbours(): moving = lax.ppermute(moving, ('x', 'c'), partner(side))]
    ppermute x0 -> x4, starting transfers between devices: none -> 13 us  [the longest x3 8.32 us: neighbours(): moving = lax.ppermute(moving, ('x', 'c'), partner(side))]
    ppermute x6 -> x3, starting transfers between devices: 11.8 us -> 5.75 us  [ring(): after = lax.ppermute(after, ('x', 'c'), shift(-1))]
    ppermute x6 -> x3, waiting for transfers between devices: 4.48 us -> 0.81 us  [ring(): after = lax.ppermute(after, ('x', 'c'), shift(-1))]
    ppermute x8 -> x4, waiting for transfers between devices: 14.4 us -> 13.3 us  [ring(): before = lax.ppermute(before, ('x', 'c'), shift(1))]
  transfers between devices with their start and end apart: 17 -> 14, of which waited for: 10 -> 9; matrix products, arithmetic and copies ran while one was open for 0% -> 0% of each run, Pallas kernels for 3% -> 3%
where the time goes in v10:
time: 169 us; the launch traced here: 168 us
  blocking collectives  64.3 us (38%)
  starting transfers between devices  59.2 us (35%)
  waiting for transfers between devices  33.6 us (20%)
  Pallas kernels  9.91 us (6%)
    all_to_all x3, blocking collectives, exchange(): return lax.all_to_all(value, axis, split_axis=0, concat_axis=0, tiled=True)  53 us
    ppermute x3, starting transfers between devices, swap(): return lax.ppermute(value, 'c', [(0, 1), (1, 0)])  20.3 us
    ppermute x4, starting transfers between devices, ring(): before = lax.ppermute(before, ('x', 'c'), shift(1))  20.1 us
    ppermute x3, waiting for transfers between devices, neighbours(): moving = lax.ppermute(moving, ('x', 'c'), partner(side))  16.6 us
    ppermute x4, waiting for transfers between devices, ring(): before = lax.ppermute(before, ('x', 'c'), shift(1))  13.3 us
    all_gather x1, blocking collectives, layer(): mixed = lax.all_gather(combine(blocks_exchange(result), cols), 'c', axis=0)  9.44 us
    ppermute x3, starting transfers between devices, neighbours(): moving = lax.ppermute(moving, ('x', 'c'), partner(side))  8.32 us
    ppermute x3, starting transfers between devices, ring(): after = lax.ppermute(after, ('x', 'c'), shift(-1))  5.75 us
  transfers between devices with their start and end apart: 14, of which 9 were waited for; matrix products, arithmetic and copies ran while one was open for 0% of the time, Pallas kernels for 3%

profile of v10, /device:TPU:1, one launch (start us, length us, event | category | flops | bytes accessed | tf_op | source)
XLA Modules:
  0.0 168.0 jit_solution(11348609360248755629)
XLA Ops:
  0.0 16.0 %collective-permute-start = (bf16[2048,256]{1,0:T(8,128)(2,1)}, bf16[2048,256]{1,0:T(8,128)(2,1)S(1)}, u32[]{:S(2)}, u32[]{:S(2)}) collective-permute-start(bf16[2048,256]{1,0:T(8,128)(2,1)} %bitcast.22), channel_id=1, source_target_pairs={{0,1},{1,0},{2,3},{3,2},{4,5},{5,4},{6,7},{7,6},{8,9},{9,8},{10,11... | collective-permute-start | bytes 3145736 | tf_op jit(solution)/shard_map/ppermute | solution.py:393
  16.0 1.9 %collective-permute-start.1 = (bf16[2048,256]{1,0:T(8,128)(2,1)}, bf16[2048,256]{1,0:T(8,128)(2,1)S(1)}, u32[]{:S(2)}, u32[]{:S(2)}) collective-permute-start(bf16[2048,256]{1,0:T(8,128)(2,1)} %bitcast.24), channel_id=1, source_target_pairs={{0,1},{1,0},{2,3},{3,2},{4,5},{5,4},{6,7},{7,6},{8,9},{9,8},{10,11... | collective-permute-start | bytes 3145736 | tf_op jit(solution)/shard_map/ppermute | solution.py:393
  18.0 2.4 %collective-permute-start.2 = (bf16[4096,128]{1,0:T(8,128)(2,1)}, bf16[4096,128]{1,0:T(8,128)(2,1)S(1)}, u32[]{:S(2)}, u32[]{:S(2)}) collective-permute-start(bf16[4096,128]{1,0:T(8,128)(2,1)} %bitcast.26), channel_id=1, source_target_pairs={{0,1},{1,0},{2,3},{3,2},{4,5},{5,4},{6,7},{7,6},{8,9},{9,8},{10,11... | collective-permute-start | bytes 3145736 | tf_op jit(solution)/shard_map/ppermute | solution.py:393
  20.4 0.9 prepare.1
  21.2 1.9 %all-gather = bf16[544,128]{1,0:T(8,128)(2,1)S(1)} all-gather(bf16[272,128]{1,0:T(8,128)(2,1)S(1)} %prepare.1), channel_id=2, replica_groups=mesh['ep'=64,'x'=8,'c'=2] {'c'}, dimensions={0}, use_global_device_ids=true | all-gather | bytes 208896 | tf_op jit(solution)/shard_map/all_gather | solution.py:449
  23.2 1.8 %dispatch.1 = (bf16[512,256]{1,0:T(8,128)(2,1)S(1)}, f32[256,8]{1,0:T(8,128)}) custom-call(s32[2]{0:T(128)S(1)} %pad_add_fusion.refs_0_.place_ref, bf16[2,272,128]{2,1,0:T(8,128)(2,1)S(1)} %bitcast.20, s32[2,256]{1,0:T(2,128)} %bitcast.33, f32[2,256]{1,0:T(2,128)} %bitcast.34), custom_call_target="tpu_custom_call" | custom-call | tf_op jit(solution)/shard_map/dispatch/pallas_call | solution.py:97
  25.0 23.7 %all_to_all.15 = bf16[64,8,256]{2,1,0:T(8,128)(2,1)S(1)} all-to-all(bf16[64,8,256]{2,1,0:T(8,128)(2,1)S(1)} %bitcast.31), channel_id=1, replica_groups=mesh['ep'=64,'x'=8,'c'=2] {'ep'}, dimensions={0} | all-to-all | bytes 524288 | tf_op jit(solution)/shard_map/all_to_all | solution.py:384
  49.0 4.6 %collective-permute-start.3 = (bf16[336,256]{1,0:T(8,128)(2,1)S(1)}, bf16[336,256]{1,0:T(8,128)(2,1)S(1)}, u32[]{:S(2)}, u32[]{:S(2)}) collective-permute-start(bf16[336,256]{1,0:T(8,128)(2,1)S(1)} %arrange.1.refs_0_.refs_2_), channel_id=1, source_target_pairs={{0,2},{1,15},{2,0},{3,5},{4,6},{5,3},{6,4},{7,9},{8,10},{9,7},{10,... | collective-permute-start | bytes 516104 | tf_op jit(solution)/shard_map/ppermute | solution.py:427
  53.6 2.9 %collective-permute-done.3.refs_1_.refs_3_ = bf16[336,256]{1,0:T(8,128)(2,1)S(1)} collective-permute-done((bf16[336,256]{1,0:T(8,128)(2,1)S(1)}, bf16[336,256]{1,0:T(8,128)(2,1)S(1)}, u32[]{:S(2)}, u32[]{:S(2)}) %collective-permute-start.3) | collective-permute-done | bytes 172064 | tf_op jit(solution)/shard_map/ppermute | solution.py:427
  56.5 1.9 %collective-permute-start.4 = (bf16[2,336,256]{2,1,0:T(8,128)(2,1)S(1)}, bf16[2,336,256]{2,1,0:T(8,128)(2,1)S(1)}, u32[]{:S(2)}, u32[]{:S(2)}) collective-permute-start(bf16[2,336,256]{2,1,0:T(8,128)(2,1)S(1)} %pad_maximum_fusion), channel_id=1, source_target_pairs={{0,14},{1,3},{2,4},{3,1},{4,2},{5,7},{6,8},{7,5},{8,6},{9,11},{10,... | collective-permute-start | bytes 1032200 | tf_op jit(solution)/shard_map/ppermute | solution.py:431
  58.4 6.1 %collective-permute-done.4.refs_2_.refs_4_ = bf16[2,336,256]{2,1,0:T(8,128)(2,1)S(1)} collective-permute-done((bf16[2,336,256]{2,1,0:T(8,128)(2,1)S(1)}, bf16[2,336,256]{2,1,0:T(8,128)(2,1)S(1)}, u32[]{:S(2)}, u32[]{:S(2)}) %collective-permute-start.4) | collective-permute-done | bytes 344096 | tf_op jit(solution)/shard_map/ppermute | solution.py:431
  64.5 4.5 %collective-permute-start.5 = (bf16[2,336,256]{2,1,0:T(8,128)(2,1)S(1)}, bf16[2,336,256]{2,1,0:T(8,128)(2,1)S(1)}, u32[]{:S(2)}, u32[]{:S(2)}) collective-permute-start(bf16[2,336,256]{2,1,0:T(8,128)(2,1)S(1)} %collective-permute-done.4.refs_2_.refs_4_), channel_id=1, source_target_pairs={{0,2},{1,15},{2,0},{3,5},{4,6},{5,3},{6,4},{7,9},{8,10},{9,7},{10,... | collective-permute-start | bytes 1032200 | tf_op jit(solution)/shard_map/ppermute | solution.py:431
  69.0 4.7 %collective-permute-done.5.refs_3_.refs_5_ = bf16[2,336,256]{2,1,0:T(8,128)(2,1)S(1)} collective-permute-done((bf16[2,336,256]{2,1,0:T(8,128)(2,1)S(1)}, bf16[2,336,256]{2,1,0:T(8,128)(2,1)S(1)}, u32[]{:S(2)}, u32[]{:S(2)}) %collective-permute-start.5) | collective-permute-done | bytes 344096 | tf_op jit(solution)/shard_map/ppermute | solution.py:431
  73.7 1.9 %collective-permute-start.6 = (bf16[2,336,256]{2,1,0:T(8,128)(2,1)S(1)}, bf16[2,336,256]{2,1,0:T(8,128)(2,1)S(1)}, u32[]{:S(2)}, u32[]{:S(2)}) collective-permute-start(bf16[2,336,256]{2,1,0:T(8,128)(2,1)S(1)} %collective-permute-done.5.refs_3_.refs_5_), channel_id=1, source_target_pairs={{0,14},{1,3},{2,4},{3,1},{4,2},{5,7},{6,8},{7,5},{8,6},{9,11},{10,... | collective-permute-start | bytes 1032200 | tf_op jit(solution)/shard_map/ppermute | solution.py:431
  75.8 5.8 %collective-permute-done.6.refs_6_ = bf16[2,336,256]{2,1,0:T(8,128)(2,1)S(1)} collective-permute-done((bf16[2,336,256]{2,1,0:T(8,128)(2,1)S(1)}, bf16[2,336,256]{2,1,0:T(8,128)(2,1)S(1)}, u32[]{:S(2)}, u32[]{:S(2)}) %collective-permute-start.6) | collective-permute-done | bytes 344096 | tf_op jit(solution)/shard_map/ppermute | solution.py:431
  81.7 2.7 %hidden.1.refs_1_ = bf16[320,512]{1,0:T(8,128)(2,1)S(1)} custom-call(s32[2]{0:T(128)S(1)} %pad_add_fusion.refs_0_.place_ref, f32[320,256]{1,0:T(8,128)S(1)} %squares.1.refs_1_, bf16[336,256]{1,0:T(8,128)(2,1)S(1)} %arrange.1.refs_0_.refs_2_, bf16[336,256]{1,0:T(8,128)(2,1)S(1)} %collective-permute-done.3.refs_1_.refs_3_, ...), custom_call_target="tpu_custom_call" | custom-call | tf_op jit(solution)/shard_map/hidden/pallas_call | solution.py:225
  84.4 4.5 %collective-permute-start.7 = (bf16[320,512]{1,0:T(8,128)(2,1)S(1)}, bf16[320,512]{1,0:T(8,128)(2,1)S(1)}, u32[]{:S(2)}, u32[]{:S(2)}) collective-permute-start(bf16[320,512]{1,0:T(8,128)(2,1)S(1)} %hidden.1.refs_1_), channel_id=1, source_target_pairs={{0,2},{1,15},{2,4},{3,1},{4,6},{5,3},{6,8},{7,5},{8,10},{9,7},{10,... | collective-permute-start | bytes 983048 | tf_op jit(solution)/shard_map/ppermute | solution.py:409
  88.9 1.9 %collective-permute-start.8 = (bf16[320,512]{1,0:T(8,128)(2,1)S(1)}, bf16[320,512]{1,0:T(8,128)(2,1)S(1)}, u32[]{:S(2)}, u32[]{:S(2)}) collective-permute-start(bf16[320,512]{1,0:T(8,128)(2,1)S(1)} %hidden.1.refs_1_), channel_id=1, source_target_pairs={{0,14},{1,3},{2,0},{3,5},{4,2},{5,7},{6,4},{7,9},{8,6},{9,11},{10,... | collective-permute-start | bytes 983048 | tf_op jit(solution)/shard_map/ppermute | solution.py:412
  90.8 2.1 %collective-permute-done.7.refs_2_ = bf16[320,512]{1,0:T(8,128)(2,1)S(1)} collective-permute-done((bf16[320,512]{1,0:T(8,128)(2,1)S(1)}, bf16[320,512]{1,0:T(8,128)(2,1)S(1)}, u32[]{:S(2)}, u32[]{:S(2)}) %collective-permute-start.7) | collective-permute-done | bytes 327712 | tf_op jit(solution)/shard_map/ppermute | solution.py:409
  92.9 5.0 %collective-permute-start.9 = (bf16[320,512]{1,0:T(8,128)(2,1)S(1)}, bf16[320,512]{1,0:T(8,128)(2,1)S(1)}, u32[]{:S(2)}, u32[]{:S(2)}) collective-permute-start(bf16[320,512]{1,0:T(8,128)(2,1)S(1)} %collective-permute-done.7.refs_2_), channel_id=1, source_target_pairs={{0,2},{1,15},{2,4},{3,1},{4,6},{5,3},{6,8},{7,5},{8,10},{9,7},{10,... | collective-permute-start | bytes 983048 | tf_op jit(solution)/shard_map/ppermute | solution.py:409
  98.7 1.9 %collective-permute-start.10 = (bf16[320,512]{1,0:T(8,128)(2,1)S(1)}, bf16[320,512]{1,0:T(8,128)(2,1)S(1)}, u32[]{:S(2)}, u32[]{:S(2)}) collective-permute-start(bf16[320,512]{1,0:T(8,128)(2,1)S(1)} %collective-permute-done.8.refs_3_), channel_id=1, source_target_pairs={{0,14},{1,3},{2,0},{3,5},{4,2},{5,7},{6,4},{7,9},{8,6},{9,11},{10,... | collective-permute-start | bytes 983048 | tf_op jit(solution)/shard_map/ppermute | solution.py:412
  100.6 4.0 %collective-permute-done.9.refs_4_ = bf16[320,512]{1,0:T(8,128)(2,1)S(1)} collective-permute-done((bf16[320,512]{1,0:T(8,128)(2,1)S(1)}, bf16[320,512]{1,0:T(8,128)(2,1)S(1)}, u32[]{:S(2)}, u32[]{:S(2)}) %collective-permute-start.9) | collective-permute-done | bytes 327712 | tf_op jit(solution)/shard_map/ppermute | solution.py:409
  104.6 5.3 %collective-permute-start.11 = (bf16[320,512]{1,0:T(8,128)(2,1)S(1)}, bf16[320,512]{1,0:T(8,128)(2,1)S(1)}, u32[]{:S(2)}, u32[]{:S(2)}) collective-permute-start(bf16[320,512]{1,0:T(8,128)(2,1)S(1)} %collective-permute-done.9.refs_4_), channel_id=1, source_target_pairs={{0,2},{1,15},{2,4},{3,1},{4,6},{5,3},{6,8},{7,5},{8,10},{9,7},{10,... | collective-permute-start | bytes 983048 | tf_op jit(solution)/shard_map/ppermute | solution.py:409
  109.9 1.9 %collective-permute-start.12 = (bf16[320,512]{1,0:T(8,128)(2,1)S(1)}, bf16[320,512]{1,0:T(8,128)(2,1)S(1)}, u32[]{:S(2)}, u32[]{:S(2)}) collective-permute-start(bf16[320,512]{1,0:T(8,128)(2,1)S(1)} %collective-permute-done.10.refs_5_), channel_id=1, source_target_pairs={{0,14},{1,3},{2,0},{3,5},{4,2},{5,7},{6,4},{7,9},{8,6},{9,11},{10,... | collective-permute-start | bytes 983048 | tf_op jit(solution)/shard_map/ppermute | solution.py:412
  111.9 3.9 %collective-permute-done.11.refs_6_ = bf16[320,512]{1,0:T(8,128)(2,1)S(1)} collective-permute-done((bf16[320,512]{1,0:T(8,128)(2,1)S(1)}, bf16[320,512]{1,0:T(8,128)(2,1)S(1)}, u32[]{:S(2)}, u32[]{:S(2)}) %collective-permute-start.11) | collective-permute-done | bytes 327712 | tf_op jit(solution)/shard_map/ppermute | solution.py:409
  115.8 5.3 %collective-permute-start.13 = (bf16[320,512]{1,0:T(8,128)(2,1)S(1)}, bf16[320,512]{1,0:T(8,128)(2,1)S(1)}, u32[]{:S(2)}, u32[]{:S(2)}) collective-permute-start(bf16[320,512]{1,0:T(8,128)(2,1)S(1)} %collective-permute-done.11.refs_6_), channel_id=1, source_target_pairs={{0,2},{1,15},{2,4},{3,1},{4,6},{5,3},{6,8},{7,5},{8,10},{9,7},{10,... | collective-permute-start | bytes 983048 | tf_op jit(solution)/shard_map/ppermute | solution.py:409
  121.1 1.7 down_early.1
  122.8 3.3 %collective-permute-done.13.refs_2_ = bf16[320,512]{1,0:T(8,128)(2,1)S(1)} collective-permute-done((bf16[320,512]{1,0:T(8,128)(2,1)S(1)}, bf16[320,512]{1,0:T(8,128)(2,1)S(1)}, u32[]{:S(2)}, u32[]{:S(2)}) %collective-permute-start.13) | collective-permute-done | bytes 327712 | tf_op jit(solution)/shard_map/ppermute | solution.py:409
  126.6 20.3 %all_to_all.16 = bf16[64,8,256]{2,1,0:T(8,128)(2,1)S(1)} all-to-all(bf16[64,8,256]{2,1,0:T(8,128)(2,1)S(1)} %bitcast.30), channel_id=1, replica_groups=mesh['ep'=64,'x'=8,'c'=2] {'ep'}, dimensions={0} | all-to-all | bytes 524288 | tf_op jit(solution)/shard_map/all_to_all | solution.py:384
  147.4 9.4 %all-gather.1 = f32[512,256]{1,0:T(8,128)S(1)} all-gather(f32[256,256]{1,0:T(8,128)S(1)} %combine.1), channel_id=3, replica_groups=mesh['ep'=64,'x'=8,'c'=2] {'c'}, dimensions={0}, use_global_device_ids=true | all-gather | bytes 786432 | tf_op jit(solution)/shard_map/all_gather | solution.py:469
  157.5 8.9 %all_to_all.17.sums_ref = f32[8,1,256]{2,1,0:T(1,128)S(1)} all-to-all(f32[8,1,256]{2,1,0:T(1,128)S(1)} %get-tuple-element.24), channel_id=1, replica_groups=mesh['ep'=64,'x'=8,'c'=2] {'x'}, dimensions={0} | all-to-all | bytes 16384 | tf_op jit(solution)/shard_map/all_to_all | solution.py:384
  167.1 0.9 final.1
  (23 shorter events, 3.6 us)
Async XLA Ops:
  0.0 48.7 %collective-permute-start = (bf16[2048,256]{1,0:T(8,128)(2,1)}, bf16[2048,256]{1,0:T(8,128)(2,1)S(1)}, u32[]{:S(2)}, u32[]{:S(2)}) collective-permute-start(bf16[2048,256]{1,0:T(8,128)(2,1)} %bitcast.22), channel_id=1, source_target_pairs={{0,1},{1,0},{2,3},{3,2},{4,5},{5,4},{6,7},{7,6},{8,9},{9,8},{10,11... | collective-permute-start | bytes 3145736 | tf_op jit(solution)/shard_map/ppermute | solution.py:393
  16.0 32.7 %collective-permute-start.1 = (bf16[2048,256]{1,0:T(8,128)(2,1)}, bf16[2048,256]{1,0:T(8,128)(2,1)S(1)}, u32[]{:S(2)}, u32[]{:S(2)}) collective-permute-start(bf16[2048,256]{1,0:T(8,128)(2,1)} %bitcast.24), channel_id=1, source_target_pairs={{0,1},{1,0},{2,3},{3,2},{4,5},{5,4},{6,7},{7,6},{8,9},{9,8},{10,11... | collective-permute-start | bytes 3145736 | tf_op jit(solution)/shard_map/ppermute | solution.py:393
  18.0 30.8 %collective-permute-start.2 = (bf16[4096,128]{1,0:T(8,128)(2,1)}, bf16[4096,128]{1,0:T(8,128)(2,1)S(1)}, u32[]{:S(2)}, u32[]{:S(2)}) collective-permute-start(bf16[4096,128]{1,0:T(8,128)(2,1)} %bitcast.26), channel_id=1, source_target_pairs={{0,1},{1,0},{2,3},{3,2},{4,5},{5,4},{6,7},{7,6},{8,9},{9,8},{10,11... | collective-permute-start | bytes 3145736 | tf_op jit(solution)/shard_map/ppermute | solution.py:393
  48.7 32.9 %copy-start.1 = (bf16[1,2048,256]{2,1,0:T(8,128)(2,1)S(1)}, bf16[1,2048,256]{2,1,0:T(8,128)(2,1)}, u32[]{:S(2)}) copy-start(bf16[1,2048,256]{2,1,0:T(8,128)(2,1)} %param.14) | copy-start | bytes 3145732
  48.9 32.7 %copy-start = (bf16[1,2048,256]{2,1,0:T(8,128)(2,1)S(1)}, bf16[1,2048,256]{2,1,0:T(8,128)(2,1)}, u32[]{:S(2)}) copy-start(bf16[1,2048,256]{2,1,0:T(8,128)(2,1)} %param.13) | copy-start | bytes 3145732
  49.0 7.5 %collective-permute-start.3 = (bf16[336,256]{1,0:T(8,128)(2,1)S(1)}, bf16[336,256]{1,0:T(8,128)(2,1)S(1)}, u32[]{:S(2)}, u32[]{:S(2)}) collective-permute-start(bf16[336,256]{1,0:T(8,128)(2,1)S(1)} %arrange.1.refs_0_.refs_2_), channel_id=1, source_target_pairs={{0,2},{1,15},{2,0},{3,5},{4,6},{5,3},{6,4},{7,9},{8,10},{9,7},{10,... | collective-permute-start | bytes 516104 | tf_op jit(solution)/shard_map/ppermute | solution.py:427
  56.5 8.0 %collective-permute-start.4 = (bf16[2,336,256]{2,1,0:T(8,128)(2,1)S(1)}, bf16[2,336,256]{2,1,0:T(8,128)(2,1)S(1)}, u32[]{:S(2)}, u32[]{:S(2)}) collective-permute-start(bf16[2,336,256]{2,1,0:T(8,128)(2,1)S(1)} %pad_maximum_fusion), channel_id=1, source_target_pairs={{0,14},{1,3},{2,4},{3,1},{4,2},{5,7},{6,8},{7,5},{8,6},{9,11},{10,... | collective-permute-start | bytes 1032200 | tf_op jit(solution)/shard_map/ppermute | solution.py:431
  64.5 9.2 %collective-permute-start.5 = (bf16[2,336,256]{2,1,0:T(8,128)(2,1)S(1)}, bf16[2,336,256]{2,1,0:T(8,128)(2,1)S(1)}, u32[]{:S(2)}, u32[]{:S(2)}) collective-permute-start(bf16[2,336,256]{2,1,0:T(8,128)(2,1)S(1)} %collective-permute-done.4.refs_2_.refs_4_), channel_id=1, source_target_pairs={{0,2},{1,15},{2,0},{3,5},{4,6},{5,3},{6,4},{7,9},{8,10},{9,7},{10,... | collective-permute-start | bytes 1032200 | tf_op jit(solution)/shard_map/ppermute | solution.py:431
  73.7 8.0 %collective-permute-start.6 = (bf16[2,336,256]{2,1,0:T(8,128)(2,1)S(1)}, bf16[2,336,256]{2,1,0:T(8,128)(2,1)S(1)}, u32[]{:S(2)}, u32[]{:S(2)}) collective-permute-start(bf16[2,336,256]{2,1,0:T(8,128)(2,1)S(1)} %collective-permute-done.5.refs_3_.refs_5_), channel_id=1, source_target_pairs={{0,14},{1,3},{2,4},{3,1},{4,2},{5,7},{6,8},{7,5},{8,6},{9,11},{10,... | collective-permute-start | bytes 1032200 | tf_op jit(solution)/shard_map/ppermute | solution.py:431
  75.8 45.3 %copy-start.2 = (bf16[1,4096,128]{2,1,0:T(8,128)(2,1)S(1)}, bf16[1,4096,128]{2,1,0:T(8,128)(2,1)}, u32[]{:S(2)}) copy-start(bf16[1,4096,128]{2,1,0:T(8,128)(2,1)} %param.15) | copy-start | bytes 3145732
  84.4 8.5 %collective-permute-start.7 = (bf16[320,512]{1,0:T(8,128)(2,1)S(1)}, bf16[320,512]{1,0:T(8,128)(2,1)S(1)}, u32[]{:S(2)}, u32[]{:S(2)}) collective-permute-start(bf16[320,512]{1,0:T(8,128)(2,1)S(1)} %hidden.1.refs_1_), channel_id=1, source_target_pairs={{0,2},{1,15},{2,4},{3,1},{4,6},{5,3},{6,8},{7,5},{8,10},{9,7},{10,... | collective-permute-start | bytes 983048 | tf_op jit(solution)/shard_map/ppermute | solution.py:409
  88.9 9.8 %collective-permute-start.8 = (bf16[320,512]{1,0:T(8,128)(2,1)S(1)}, bf16[320,512]{1,0:T(8,128)(2,1)S(1)}, u32[]{:S(2)}, u32[]{:S(2)}) collective-permute-start(bf16[320,512]{1,0:T(8,128)(2,1)S(1)} %hidden.1.refs_1_), channel_id=1, source_target_pairs={{0,14},{1,3},{2,0},{3,5},{4,2},{5,7},{6,4},{7,9},{8,6},{9,11},{10,... | collective-permute-start | bytes 983048 | tf_op jit(solution)/shard_map/ppermute | solution.py:412
  92.9 11.7 %collective-permute-start.9 = (bf16[320,512]{1,0:T(8,128)(2,1)S(1)}, bf16[320,512]{1,0:T(8,128)(2,1)S(1)}, u32[]{:S(2)}, u32[]{:S(2)}) collective-permute-start(bf16[320,512]{1,0:T(8,128)(2,1)S(1)} %collective-permute-done.7.refs_2_), channel_id=1, source_target_pairs={{0,2},{1,15},{2,4},{3,1},{4,6},{5,3},{6,8},{7,5},{8,10},{9,7},{10,... | collective-permute-start | bytes 983048 | tf_op jit(solution)/shard_map/ppermute | solution.py:409
  98.7 11.2 %collective-permute-start.10 = (bf16[320,512]{1,0:T(8,128)(2,1)S(1)}, bf16[320,512]{1,0:T(8,128)(2,1)S(1)}, u32[]{:S(2)}, u32[]{:S(2)}) collective-permute-start(bf16[320,512]{1,0:T(8,128)(2,1)S(1)} %collective-permute-done.8.refs_3_), channel_id=1, source_target_pairs={{0,14},{1,3},{2,0},{3,5},{4,2},{5,7},{6,4},{7,9},{8,6},{9,11},{10,... | collective-permute-start | bytes 983048 | tf_op jit(solution)/shard_map/ppermute | solution.py:412
  104.6 11.2 %collective-permute-start.11 = (bf16[320,512]{1,0:T(8,128)(2,1)S(1)}, bf16[320,512]{1,0:T(8,128)(2,1)S(1)}, u32[]{:S(2)}, u32[]{:S(2)}) collective-permute-start(bf16[320,512]{1,0:T(8,128)(2,1)S(1)} %collective-permute-done.9.refs_4_), channel_id=1, source_target_pairs={{0,2},{1,15},{2,4},{3,1},{4,6},{5,3},{6,8},{7,5},{8,10},{9,7},{10,... | collective-permute-start | bytes 983048 | tf_op jit(solution)/shard_map/ppermute | solution.py:409
  109.9 11.2 %collective-permute-start.12 = (bf16[320,512]{1,0:T(8,128)(2,1)S(1)}, bf16[320,512]{1,0:T(8,128)(2,1)S(1)}, u32[]{:S(2)}, u32[]{:S(2)}) collective-permute-start(bf16[320,512]{1,0:T(8,128)(2,1)S(1)} %collective-permute-done.10.refs_5_), channel_id=1, source_target_pairs={{0,14},{1,3},{2,0},{3,5},{4,2},{5,7},{6,4},{7,9},{8,6},{9,11},{10,... | collective-permute-start | bytes 983048 | tf_op jit(solution)/shard_map/ppermute | solution.py:412
  115.8 10.3 %collective-permute-start.13 = (bf16[320,512]{1,0:T(8,128)(2,1)S(1)}, bf16[320,512]{1,0:T(8,128)(2,1)S(1)}, u32[]{:S(2)}, u32[]{:S(2)}) collective-permute-start(bf16[320,512]{1,0:T(8,128)(2,1)S(1)} %collective-permute-done.11.refs_6_), channel_id=1, source_target_pairs={{0,2},{1,15},{2,4},{3,1},{4,6},{5,3},{6,8},{7,5},{8,10},{9,7},{10,... | collective-permute-start | bytes 983048 | tf_op jit(solution)/shard_map/ppermute | solution.py:409
  126.6 20.4 %copy-start.3 = (f32[256,8]{1,0:T(8,128)S(1)}, f32[256,8]{1,0:T(8,128)}, u32[]{:S(2)}) copy-start(f32[256,8]{1,0:T(8,128)} %get-tuple-element.22.cols_ref) | copy-start | bytes 24580
  166.5 0.7 copy-start.4
